TPU v7x, 512 devices: a whole 4x8x8 slice. The times are simulated.
512 devices in a mesh: sp: 64 (over z, y), tp: 8 (over x, core).
Axes of the slice: x: 4, y: 8, z: 8, core: 2. Of those that a mesh axis runs over, the one named last changes fastest.
Arguments:
- target: bfloat16 [16384, 2048], P(('sp', 'tp')), may hold values from -6 to 6
- source: bfloat16 [16384, 2048], P(('sp', 'tp')), may hold values from -6 to 6
- target_gain: float32 [2, 2048], replicated, may hold values from 0.1 to 1.9
- source_gain: float32 [2, 2048], replicated, may hold values from 0.1 to 1.9
- query_gain: float32 [2, 64], replicated, may hold values from 0.75 to 2.75
- key_gain: float32 [2, 64], replicated, may hold values from 0.75 to 2.75
- query_weight: bfloat16 [2, 2048, 512], P(None, None, 'tp'), may hold values from -0.125 to 0.125
- key_weight: bfloat16 [2, 2048, 128], replicated, may hold values from -0.125 to 0.125
- value_weight: bfloat16 [2, 2048, 128], replicated, may hold values from -0.125 to 0.125
- out_weight: bfloat16 [2, 512, 2048], P(None, 'tp'), may hold values from -0.25 to 0.25
Outputs:
- decoded: bfloat16 [16384, 2048], P(('sp', 'tp'))
All inputs are finite; a program needn't handle non-finite values.
Results may differ from a plain program's by a relative error of at most 0.014.
Values may be sent and summed in bfloat16 or wider, within the bound.
No kernel may reach another device: no remote copies, remote signals or barrier semaphores. Data moves between devices by JAX's collectives and lax.ppermute only.
A program may use at most 64 MiB of HBM per device.

v0:
```python
import functools

import jax
import jax.numpy as jnp
from jax import lax
from jax.experimental import pallas as pl
from jax.experimental.pallas import tpu as pltpu
from jax.sharding import Mesh
from jax.sharding import PartitionSpec as P

ROWS = ("z", "y")
TP = ("x", "c")
ALL = ("z", "y", "x", "c")
EPS = 1e-06
LOG2E = 1.4426950408889634
F32 = jnp.float32
BF16 = jnp.bfloat16


def dot(a, b):
    return jnp.dot(a, b, preferred_element_type=F32)


def dot_t(a, b):
    return lax.dot_general(a, b, (((1,), (1,)), ((), ())), preferred_element_type=F32)


def rms(value):
    return lax.rsqrt(jnp.mean(value * value, axis=-1, keepdims=True) + EPS)


def head_norm(value, gain_row, head):
    rows, width = value.shape
    low = lax.broadcasted_iota(jnp.int32, (rows, 2 * head), 1) < head
    groups = []
    for start in range(0, width, 2 * head):
        part = value[:, start : start + 2 * head]
        square = part * part
        first = jnp.sum(jnp.where(low, square, 0.0), axis=-1, keepdims=True)
        second = jnp.sum(jnp.where(low, 0.0, square), axis=-1, keepdims=True)
        scale = lax.rsqrt(jnp.where(low, first, second) / head + EPS)
        groups.append(part * scale * gain_row)
    return groups


def doubled(row):
    return jnp.concatenate([row, row], axis=-1)


def source_kernel(source, gain, key_gain, key_weight, value_weight, out):
    layers, head = key_gain.shape
    value = source[...].astype(F32)
    scaled = value * rms(value)
    width = key_weight.shape[2]
    for layer in range(layers):
        normed = (scaled * gain[layer : layer + 1, :]).astype(BF16)
        keys = dot(normed, key_weight[layer])
        row = doubled(key_gain[layer : layer + 1, :])
        groups = head_norm(keys, row, head)
        for k, group in enumerate(groups):
            out[layer, :, k * 2 * head : (k + 1) * 2 * head] = group.astype(BF16)
        out[layer, :, width:] = dot(normed, value_weight[layer]).astype(BF16)


def project(normed, mine, other, row, head, place):
    x, core = place[0], place[1]
    model = normed.shape[1]
    own = jnp.concatenate(head_norm(dot_t(normed, mine.reshape(-1, model)), row, head), axis=1)
    far = jnp.concatenate(head_norm(dot_t(normed, other.reshape(-1, model)), row, head), axis=1)
    own = pltpu.roll(own, x * head, 1)
    far = pltpu.roll(far, x * head, 1)
    return jnp.where(core == 0, own, far), jnp.where(core == 0, far, own)


def store_groups(out, groups):
    width = groups[0].shape[1]
    for k, group in enumerate(groups):
        out[:, k * width : (k + 1) * width] = group.astype(BF16)


def query_kernel(layer, place, target, gain, query_gain, mine, other, out):
    head = query_gain.shape[1]
    value = target[...].astype(F32)
    normed = (value * rms(value) * gain[layer : layer + 1, :]).astype(BF16)
    row = doubled(query_gain[layer : layer + 1, :])
    store_groups(out, project(normed, mine[...], other[...], row, head, place))


def attended_halves(arrived, heads, head):
    total = arrived[0].astype(F32)
    for k in range(1, arrived.shape[0]):
        total = total + arrived[k].astype(F32)
    rows = total.shape[0]
    width = heads * head
    mass = total[:, width : width + heads] + total[:, width + heads : width + 2 * heads]
    low = lax.broadcasted_iota(jnp.int32, (rows, 2 * head), 1) < head
    groups = []
    for g in range(heads // 2):
        below = jnp.where(low, mass[:, 2 * g : 2 * g + 1], mass[:, 2 * g + 1 : 2 * g + 2])
        groups.append(total[:, 2 * g * head : 2 * (g + 1) * head] / below)
    half = len(groups) // 2
    return jnp.concatenate(groups[:half], axis=1), jnp.concatenate(groups[half:], axis=1)


def mixed(place, arrived, hidden, mine, other, heads, head):
    x, core = place[0], place[1]
    even, odd = attended_halves(arrived, heads, head)
    width = even.shape[1]
    back = (width - x * head) % width
    own = pltpu.roll(jnp.where(core == 0, even, odd), back, 1).astype(BF16)
    far = pltpu.roll(jnp.where(core == 0, odd, even), back, 1).astype(BF16)
    model = hidden.shape[1]
    branch = dot(own, mine[...].reshape(-1, model)) + dot(far, other[...].reshape(-1, model))
    return (hidden[...].astype(F32) + branch).astype(BF16)


def middle_kernel(layer, heads, place, arrived, hidden, gain, query_gain, out_mine, out_other, mine, other, hidden_out, out):
    head = query_gain.shape[1]
    now = mixed(place, arrived, hidden, out_mine, out_other, heads, head)
    hidden_out[...] = now
    value = now.astype(F32)
    normed = (value * rms(value) * gain[layer : layer + 1, :]).astype(BF16)
    row = doubled(query_gain[layer : layer + 1, :])
    store_groups(out, project(normed, mine[...], other[...], row, head, place))


def last_kernel(heads, head, place, arrived, hidden, out_mine, out_other, hidden_out):
    hidden_out[...] = mixed(place, arrived, hidden, out_mine, out_other, heads, head)


def attention_kernel(heads, head, tile, count, place, *refs):
    queries, (pairs, out, rhs, value_t, gathered) = refs[:count], refs[count:]
    blocks, each_rows, _ = pairs.shape
    keys = blocks * each_rows
    width = 2 * head
    everyone = jnp.concatenate([part[...].astype(F32) for part in queries], axis=0)
    columns = everyone.shape[0]
    factor = LOG2E * head**-0.5
    turned = jnp.transpose(everyone).astype(BF16)
    zero = jnp.zeros((head, columns), BF16)
    per = heads // 4
    for p in range(heads):
        kv = (p % 4) // 2
        rhs[p, kv * head : (kv + 1) * head, :] = turned[p * head : (p + 1) * head, :]
        rhs[p, (1 - kv) * head : (2 - kv) * head, :] = zero
    value_t[...] = jnp.transpose(pairs[:, :, width:].reshape(keys, width).astype(F32)).astype(BF16)
    for kv in range(2):

        def one_head(j, carry, kv=kv):
            p = (j // 2) * 4 + 2 * kv + j % 2
            right = rhs[p]
            mass = jnp.zeros((8, columns), F32)
            total = None
            for t in range(keys // tile):
                taken = slice(t * tile // each_rows, (t + 1) * tile // each_rows)
                score = dot(pairs[taken, :, :width].reshape(tile, width), right)
                weight = jnp.exp2(score * factor)
                mass = mass + jnp.sum(weight.reshape(tile // 8, 8, columns), axis=0)
                part = dot(value_t[:, t * tile : (t + 1) * tile], weight.astype(BF16))
                total = part if total is None else total + part
            gathered[pl.ds(pl.multiple_of(p * head, head), head), :] = total[kv * head : (kv + 1) * head, :]
            mass = jnp.sum(mass, axis=0, keepdims=True)
            top = mass.astype(BF16).astype(F32)
            gathered[pl.ds(heads * head + p, 1), :] = top
            gathered[pl.ds(heads * head + heads + p, 1), :] = mass - top
            return carry

        lax.fori_loop(0, 2 * per, one_head, 0)
    rest = heads * head + 2 * heads
    gathered[rest:, :] = jnp.zeros((gathered.shape[0] - rest, columns), F32)
    result = jnp.transpose(gathered[...]).astype(BF16)
    if count == 1:
        out[...] = result
        return
    each = columns // (2 * count)
    for r in range(count):
        for d in range(2):
            to = ((place[0] + r) % count) * 2 + (place[1] + d) % 2
            first = (2 * r + d) * each
            out[pl.ds(pl.multiple_of(to * each, each), each), :] = result[first : first + each, :]


def call(kernel, shapes, scratch=(), flops=1000000):
    one = not isinstance(shapes, (list, tuple))
    specs = pl.BlockSpec(memory_space=pltpu.VMEM)
    return pl.pallas_call(
        kernel,
        out_shape=shapes,
        out_specs=specs if one else [specs] * len(shapes),
        scratch_shapes=list(scratch),
        compiler_params=pltpu.CompilerParams(vmem_limit_bytes=40 * 1024 * 1024),
        cost_estimate=pl.CostEstimate(flops=flops, bytes_accessed=1000000, transcendentals=0),
    )


def whole(value):
    return pl.BlockSpec(value.shape, lambda i, n=value.ndim: (0,) * n)


def part_of(value, k, size):
    if value.ndim == 4:
        return pl.BlockSpec((value.shape[0], None, *value.shape[2:]), lambda i, k=k: (0, k, 0, 0))
    return pl.BlockSpec((value.shape[0], size, value.shape[2]), lambda i, k=k: (0, k, 0))


def with_place(kernel, shapes, operands, parts, flops, scratch=()):
    one = not isinstance(shapes, (list, tuple))
    place, *rest = operands
    specs = [pl.BlockSpec(memory_space=pltpu.SMEM)] + [whole(value) for value in rest]
    specs += [part_of(*part) for part in parts]
    return pl.pallas_call(
        kernel,
        grid=(1,),
        out_shape=shapes,
        in_specs=specs,
        out_specs=whole(shapes) if one else [whole(shape) for shape in shapes],
        scratch_shapes=list(scratch),
        compiler_params=pltpu.CompilerParams(vmem_limit_bytes=40 * 1024 * 1024),
        cost_estimate=pl.CostEstimate(flops=flops, bytes_accessed=1000000, transcendentals=0),
    )(place, *rest, *(part[0] for part in parts))


def to_all(value, axis):
    copies = jnp.broadcast_to(value, (lax.axis_size(axis), *value.shape))
    return lax.all_to_all(copies, axis, split_axis=0, concat_axis=0, tiled=True)


def shifted(value, axis, step):
    size = lax.axis_size(axis)
    return lax.ppermute(value, axis, [((k + step) % size, k) for k in range(size)])


def around(value):
    half = value.shape[0] // 2
    right, left = shifted(value, "x", 1), shifted(value, "x", -1)
    far = [shifted(right[:half], "x", 1), shifted(left[half:], "x", -1)]
    return jnp.concatenate([value, right, *far, left], axis=0).reshape(4, *value.shape)


def decoder(target, source, target_gain, source_gain, query_gain, key_gain, query_weight, key_weight, value_weight, out_weight):
    layers, _, head_columns = query_weight.shape
    head = query_gain.shape[1]
    heads = head_columns // head * lax.axis_size(TP)
    rows, model = target.shape
    group = rows * lax.axis_size(TP)
    shapes = jax.ShapeDtypeStruct
    place = jnp.stack([lax.axis_index("x"), lax.axis_index("c")])
    query_t = jnp.swapaxes(query_weight, 1, 2)
    width = heads * head
    wide = width + 128

    pairs = call(source_kernel, shapes((layers, rows, 4 * head), BF16), flops=200000000)(
        source, source_gain, key_gain, key_weight, value_weight
    )
    plane = to_all(pairs, ROWS)
    keys = plane.shape[0] * rows

    def both(stacked):
        return stacked, shifted(stacked, "c", 1)

    first = both(around(query_t[0]))
    rest = both(around(jnp.concatenate([out_weight[0], query_t[1], out_weight[1]], axis=0)))
    rest = [[(part, k, head) for part in rest] for k in range(3)]

    queries = with_place(
        functools.partial(query_kernel, 0),
        shapes((rows, width), BF16),
        (place, target, target_gain, query_gain),
        [(part, 0, head) for part in first],
        200000000,
    )
    chip = jnp.concatenate([queries, shifted(queries, "c", 1)], axis=0)
    everyone = [chip] + [shifted(chip, "x", k) for k in range(1, lax.axis_size("x"))]

    hidden = target
    for layer in range(layers):
        partial = with_place(
            functools.partial(attention_kernel, heads, head, 256, len(everyone)),
            shapes((group, wide), BF16),
            (place, *everyone),
            [(plane, layer, 1)],
            5000000000,
            scratch=[
                pltpu.VMEM((heads, 2 * head, group), BF16),
                pltpu.VMEM((2 * head, keys), BF16),
                pltpu.VMEM((wide, group), F32),
            ],
        )
        arrived = lax.all_to_all(partial.reshape(-1, rows, wide), TP, split_axis=0, concat_axis=0, tiled=True)
        if layer + 1 < layers:
            hidden, queries = with_place(
                functools.partial(middle_kernel, layer + 1, heads),
                [shapes((rows, model), BF16), shapes((rows, width), BF16)],
                (place, arrived, hidden, target_gain, query_gain),
                rest[0] + rest[1],
                400000000,
            )
            everyone = [to_all(queries, TP).reshape(group, width)]
        else:
            hidden = with_place(
                functools.partial(last_kernel, heads, head),
                shapes((rows, model), BF16),
                (place, arrived, hidden),
                rest[2],
                200000000,
            )
    return hidden


def solution(mesh):
    columns = mesh.shape["tp"]
    split = Mesh(mesh.devices.reshape(8, 8, columns // 2, 2), ALL)
    return jax.shard_map(
        decoder,
        mesh=split,
        in_specs=(P(ALL, None), P(ALL, None), P(), P(), P(), P(), P(None, None, TP), P(), P(), P(None, TP, None)),
        out_specs=P(ALL, None),
        check_vma=False,
    )
```

profile of v0, /device:TPU:1, one launch (start us, length us, event | category | flops | bytes accessed | tf_op | source)
XLA Modules:
  0.0 159.2 jit_solution(2171533709954664510)
XLA Ops:
  0.0 2.1 %slice_bitcast_fusion = (bf16[64,2048]{1,0:T(8,128)(2,1)S(1)}, bf16[64,2048]{1,0:T(8,128)(2,1)}, bf16[64,2048]{1,0:T(8,128)(2,1)S(1)}, bf16[64,2048]{1,0:T(8,128)(2,1)S(1)}) fusion(bf16[2,64,2048]{2,1,0:T(8,128)(2,1)} %bitcast.31, bf16[2,64,2048]{2,1,0:T(8,128)(2,1)} %param.19), kind=kLoop, calls=%fused_computation.1 | loop fusion | bytes 2097152 | tf_op jit(solution)/shard_map/squeeze | solution.py:262
  2.2 5.2 %collective-permute-start = (bf16[64,2048]{1,0:T(8,128)(2,1)}, bf16[64,2048]{1,0:T(8,128)(2,1)}, u32[]{:S(2)}, u32[]{:S(2)}) collective-permute-start(bf16[64,2048]{1,0:T(8,128)(2,1)} %get-tuple-element.12), channel_id=1, source_target_pairs={{2,0},{4,2},{6,4},{0,6},{3,1},{5,3},{7,5},{1,7},{10,8},{12,10},{14... | collective-permute-start | bytes 786440 | tf_op jit(solution)/shard_map/ppermute | solution.py:230
  7.4 1.9 %collective-permute-start.2 = (bf16[64,2048]{1,0:T(8,128)(2,1)}, bf16[64,2048]{1,0:T(8,128)(2,1)}, u32[]{:S(2)}, u32[]{:S(2)}) collective-permute-start(bf16[64,2048]{1,0:T(8,128)(2,1)} %get-tuple-element.12), channel_id=1, source_target_pairs={{6,0},{0,2},{2,4},{4,6},{7,1},{1,3},{3,5},{5,7},{14,8},{8,10},{10,... | collective-permute-start | bytes 786440 | tf_op jit(solution)/shard_map/ppermute | solution.py:230
  9.3 1.0 pad_maximum_fusion
  10.3 4.6 %collective-permute-start.9 = (bf16[192,2048]{1,0:T(8,128)(2,1)}, bf16[192,2048]{1,0:T(8,128)(2,1)}, u32[]{:S(2)}, u32[]{:S(2)}) collective-permute-start(bf16[192,2048]{1,0:T(8,128)(2,1)} %pad_maximum_fusion), channel_id=1, source_target_pairs={{2,0},{4,2},{6,4},{0,6},{3,1},{5,3},{7,5},{1,7},{10,8},{12,10},{14... | collective-permute-start | bytes 2359304 | tf_op jit(solution)/shard_map/ppermute | solution.py:230
  14.8 1.9 %collective-permute-start.11 = (bf16[192,2048]{1,0:T(8,128)(2,1)}, bf16[192,2048]{1,0:T(8,128)(2,1)}, u32[]{:S(2)}, u32[]{:S(2)}) collective-permute-start(bf16[192,2048]{1,0:T(8,128)(2,1)} %pad_maximum_fusion), channel_id=1, source_target_pairs={{6,0},{0,2},{2,4},{4,6},{7,1},{1,3},{3,5},{5,7},{14,8},{8,10},{10,... | collective-permute-start | bytes 2359304 | tf_op jit(solution)/shard_map/ppermute | solution.py:230
  17.3 1.6 broadcast_in_dim.6
  18.9 16.6 %all-to-all-start = ((bf16[64,2,32,256]{3,2,1,0:T(8,128)(2,1)}), bf16[64,2,32,256]{3,2,1,0:T(8,128)(2,1)}, u32[]{:S(2)}, u32[]{:S(2)}) async-start(bf16[64,2,32,256]{3,2,1,0:T(8,128)(2,1)} %broadcast_in_dim.6), calls=%async_computation | async-start | bytes 4194304 | tf_op jit(solution)/shard_map/all_to_all | solution.py:225
  35.5 1.0 constant_dynamic-update-slice_fusion.11
  36.5 1.8 %constant_dynamic-update-slice_fusion.10 = (bf16[768,2048]{1,0:T(8,128)(2,1)S(1)}, bf16[256,2048]{1,0:T(8,128)(2,1)}) fusion(bf16[768,2048]{1,0:T(8,128)(2,1)S(1)} %constant_dynamic-update-slice_fusion.11, bf16[2,64,2048]{2,1,0:T(8,128)(2,1)} %bitcast.32), kind=kLoop, calls=%fused_computation.16 | loop fusion | bytes 1048576
  38.3 1.0 slice.36
  39.3 4.6 %collective-permute-start.10 = (bf16[96,2048]{1,0:T(8,128)(2,1)S(1)}, bf16[96,2048]{1,0:T(8,128)(2,1)S(1)}, u32[]{:S(2)}, u32[]{:S(2)}) collective-permute-start(bf16[96,2048]{1,0:T(8,128)(2,1)S(1)} %slice.36), channel_id=1, source_target_pairs={{2,0},{4,2},{6,4},{0,6},{3,1},{5,3},{7,5},{1,7},{10,8},{12,10},{14... | collective-permute-start | bytes 1179656 | tf_op jit(solution)/shard_map/ppermute | solution.py:230
  43.9 1.0 constant_dynamic-update-slice_fusion.9
  44.8 1.0 slice.37
  45.9 2.1 %collective-permute-start.12 = (bf16[96,2048]{1,0:T(8,128)(2,1)S(1)}, bf16[96,2048]{1,0:T(8,128)(2,1)S(1)}, u32[]{:S(2)}, u32[]{:S(2)}) collective-permute-start(bf16[96,2048]{1,0:T(8,128)(2,1)S(1)} %slice.37), channel_id=1, source_target_pairs={{6,0},{0,2},{2,4},{4,6},{7,1},{1,3},{3,5},{5,7},{14,8},{8,10},{10,... | collective-permute-start | bytes 1179656 | tf_op jit(solution)/shard_map/ppermute | solution.py:230
  48.0 1.2 constant_dynamic-update-slice_fusion.8
  49.2 1.1 collective-permute-done.10
  50.3 7.3 %collective-permute-done.12 = bf16[96,2048]{1,0:T(8,128)(2,1)S(1)} collective-permute-done((bf16[96,2048]{1,0:T(8,128)(2,1)S(1)}, bf16[96,2048]{1,0:T(8,128)(2,1)S(1)}, u32[]{:S(2)}, u32[]{:S(2)}) %collective-permute-start.12) | collective-permute-done | bytes 393248 | tf_op jit(solution)/shard_map/ppermute | solution.py:230
  57.6 1.2 constant_dynamic-update-slice_fusion.5
  58.8 5.0 %collective-permute-start.13 = (bf16[4,192,2048]{2,1,0:T(8,128)(2,1)S(1)}, bf16[4,192,2048]{2,1,0:T(8,128)(2,1)}, u32[]{:S(2)}, u32[]{:S(2)}) collective-permute-start(bf16[4,192,2048]{2,1,0:T(8,128)(2,1)S(1)} %bitcast.24), channel_id=1, source_target_pairs={{1,0},{0,1},{3,2},{2,3},{5,4},{4,5},{7,6},{6,7},{9,8},{8,9},{11,10... | collective-permute-start | bytes 9437192 | tf_op jit(solution)/shard_map/ppermute | solution.py:230
  63.8 0.9 slice.33
  64.8 1.9 %collective-permute-start.1 = (bf16[32,2048]{1,0:T(8,128)(2,1)S(1)}, bf16[32,2048]{1,0:T(8,128)(2,1)S(1)}, u32[]{:S(2)}, u32[]{:S(2)}) collective-permute-start(bf16[32,2048]{1,0:T(8,128)(2,1)S(1)} %slice.33), channel_id=1, source_target_pairs={{2,0},{4,2},{6,4},{0,6},{3,1},{5,3},{7,5},{1,7},{10,8},{12,10},{14... | collective-permute-start | bytes 393224 | tf_op jit(solution)/shard_map/ppermute | solution.py:230
  66.7 0.9 slice.34
  67.6 3.4 %collective-permute-start.3 = (bf16[32,2048]{1,0:T(8,128)(2,1)S(1)}, bf16[32,2048]{1,0:T(8,128)(2,1)S(1)}, u32[]{:S(2)}, u32[]{:S(2)}) collective-permute-start(bf16[32,2048]{1,0:T(8,128)(2,1)S(1)} %slice.34), channel_id=1, source_target_pairs={{6,0},{0,2},{2,4},{4,6},{7,1},{1,3},{3,5},{5,7},{14,8},{8,10},{10,... | collective-permute-start | bytes 393224 | tf_op jit(solution)/shard_map/ppermute | solution.py:230
  71.0 1.7 %constant_dynamic-update-slice_fusion.3 = bf16[256,2048]{1,0:T(8,128)(2,1)} fusion(bf16[256,2048]{1,0:T(8,128)(2,1)} %get-tuple-element.14, bf16[64,2048]{1,0:T(8,128)(2,1)} %collective-permute-done), kind=kLoop, calls=%fused_computation.9 | loop fusion | bytes 524288
  72.7 0.7 constant_dynamic-update-slice_fusion.2
  73.4 2.5 %collective-permute-done.3 = bf16[32,2048]{1,0:T(8,128)(2,1)S(1)} collective-permute-done((bf16[32,2048]{1,0:T(8,128)(2,1)S(1)}, bf16[32,2048]{1,0:T(8,128)(2,1)S(1)}, u32[]{:S(2)}, u32[]{:S(2)}) %collective-permute-start.3) | collective-permute-done | bytes 131104 | tf_op jit(solution)/shard_map/ppermute | solution.py:230
  75.9 0.7 constant_dynamic-update-slice_fusion.1
  76.5 1.7 %constant_dynamic-update-slice_fusion = bf16[256,2048]{1,0:T(8,128)(2,1)} fusion(bf16[256,2048]{1,0:T(8,128)(2,1)} %constant_dynamic-update-slice_fusion.1, bf16[64,2048]{1,0:T(8,128)(2,1)} %collective-permute-done.2), kind=kLoop, calls=%fused_computation.6 | loop fusion | bytes 524288 | tf_op jit(solution)/shard_map/concatenate | solution.py:237
  78.2 2.7 %collective-permute-start.4 = (bf16[4,64,2048]{2,1,0:T(8,128)(2,1)}, bf16[4,64,2048]{2,1,0:T(8,128)(2,1)}, u32[]{:S(2)}, u32[]{:S(2)}) collective-permute-start(bf16[4,64,2048]{2,1,0:T(8,128)(2,1)} %bitcast.4.mine), channel_id=1, source_target_pairs={{1,0},{0,1},{3,2},{2,3},{5,4},{4,5},{7,6},{6,7},{9,8},{8,9},{11,10... | collective-permute-start | bytes 3145736 | tf_op jit(solution)/shard_map/ppermute | solution.py:230
  81.0 2.5 %collective-permute-done.4.other = bf16[4,64,2048]{2,1,0:T(8,128)(2,1)} collective-permute-done((bf16[4,64,2048]{2,1,0:T(8,128)(2,1)}, bf16[4,64,2048]{2,1,0:T(8,128)(2,1)}, u32[]{:S(2)}, u32[]{:S(2)}) %collective-permute-start.4) | collective-permute-done | bytes 1048608 | tf_op jit(solution)/shard_map/ppermute | solution.py:230
  83.5 2.5 %shard_map.100 = bf16[32,512]{1,0:T(8,128)(2,1)S(1)} custom-call(s32[2]{0:T(128)S(1)} %pad_add_fusion.place, bf16[32,2048]{1,0:T(8,128)(2,1)S(1)} %copy-done.2, f32[2,2048]{1,0:T(2,128)S(1)} %copy-done.6, f32[2,64]{1,0:T(2,128)S(1)} %copy-done.8, bf16[4,64,2048]{2,1,0:T(8,128)(2,1)} %bitcast.4.mine, bf16[4,64,2048]{2,1,0:T(8,128)(2,1)} %collective-permute-done.4.other), custom_call_target="tpu_custom_call" | custom-call | flops 200000000 | bytes 1000000 | tf_op jit(solution)/shard_map/pallas_call | solution.py:211
  86.0 2.3 %collective-permute-start.5 = (bf16[32,512]{1,0:T(8,128)(2,1)S(1)}, bf16[32,512]{1,0:T(8,128)(2,1)S(1)}, u32[]{:S(2)}, u32[]{:S(2)}) collective-permute-start(bf16[32,512]{1,0:T(8,128)(2,1)S(1)} %shard_map.100), channel_id=1, source_target_pairs={{1,0},{0,1},{3,2},{2,3},{5,4},{4,5},{7,6},{6,7},{9,8},{8,9},{11,10... | collective-permute-start | bytes 98312 | tf_op jit(solution)/shard_map/ppermute | solution.py:230
  88.3 0.8 collective-permute-done.5
  89.1 1.9 %collective-permute-start.6 = (bf16[64,512]{1,0:T(8,128)(2,1)S(1)}, bf16[64,512]{1,0:T(8,128)(2,1)S(1)}, u32[]{:S(2)}, u32[]{:S(2)}) collective-permute-start(bf16[64,512]{1,0:T(8,128)(2,1)S(1)} %pad_maximum_fusion.1.refs_0_), channel_id=1, source_target_pairs={{2,0},{4,2},{6,4},{0,6},{3,1},{5,3},{7,5},{1,7},{10,8},{12,10},{14... | collective-permute-start | bytes 196616 | tf_op jit(solution)/shard_map/ppermute | solution.py:230
  91.1 3.9 %collective-permute-start.7 = (bf16[64,512]{1,0:T(8,128)(2,1)S(1)}, bf16[64,512]{1,0:T(8,128)(2,1)S(1)}, u32[]{:S(2)}, u32[]{:S(2)}) collective-permute-start(bf16[64,512]{1,0:T(8,128)(2,1)S(1)} %pad_maximum_fusion.1.refs_0_), channel_id=1, source_target_pairs={{4,0},{6,2},{0,4},{2,6},{5,1},{7,3},{1,5},{3,7},{12,8},{14,10},{8,... | collective-permute-start | bytes 196616 | tf_op jit(solution)/shard_map/ppermute | solution.py:230
  95.0 1.9 %collective-permute-start.8 = (bf16[64,512]{1,0:T(8,128)(2,1)S(1)}, bf16[64,512]{1,0:T(8,128)(2,1)S(1)}, u32[]{:S(2)}, u32[]{:S(2)}) collective-permute-start(bf16[64,512]{1,0:T(8,128)(2,1)S(1)} %pad_maximum_fusion.1.refs_0_), channel_id=1, source_target_pairs={{6,0},{0,2},{2,4},{4,6},{7,1},{1,3},{3,5},{5,7},{14,8},{8,10},{10,... | collective-permute-start | bytes 196616 | tf_op jit(solution)/shard_map/ppermute | solution.py:230
  97.6 3.6 %collective-permute-done.8.refs_3_ = bf16[64,512]{1,0:T(8,128)(2,1)S(1)} collective-permute-done((bf16[64,512]{1,0:T(8,128)(2,1)S(1)}, bf16[64,512]{1,0:T(8,128)(2,1)S(1)}, u32[]{:S(2)}, u32[]{:S(2)}) %collective-permute-start.8) | collective-permute-done | bytes 65568 | tf_op jit(solution)/shard_map/ppermute | solution.py:230
  101.2 8.5 %shard_map.102 = bf16[256,640]{1,0:T(8,128)(2,1)S(1)} custom-call(s32[2]{0:T(128)S(1)} %pad_add_fusion.place, bf16[64,512]{1,0:T(8,128)(2,1)S(1)} %pad_maximum_fusion.1.refs_0_, bf16[64,512]{1,0:T(8,128)(2,1)S(1)} %collective-permute-done.6.refs_1_, bf16[64,512]{1,0:T(8,128)(2,1)S(1)} %collective-permute-done.7.refs_2_, ...), custom_call_target="tpu_custom_call" | custom-call | flops 5000000000 | bytes 1000000 | tf_op jit(solution)/shard_map/pallas_call | solution.py:211
  109.8 0.7 copy-done.4
  110.5 5.4 %all-to-all-start.1 = ((bf16[8,32,640]{2,1,0:T(8,128)(2,1)}), bf16[8,32,640]{2,1,0:T(8,128)(2,1)S(1)}, u32[]{:S(2)}, u32[]{:S(2)}) async-start(bf16[8,32,640]{2,1,0:T(8,128)(2,1)} %bitcast.28), calls=%async_computation.1 | async-start | bytes 655360 | tf_op jit(solution)/shard_map/all_to_all | solution.py:289
  115.9 7.1 %all-to-all-done.1.arrived = bf16[8,32,640]{2,1,0:T(8,128)(2,1)S(1)} async-done(((bf16[8,32,640]{2,1,0:T(8,128)(2,1)}), bf16[8,32,640]{2,1,0:T(8,128)(2,1)S(1)}, u32[]{:S(2)}, u32[]{:S(2)}) %all-to-all-start.1) | async-done | bytes 327712 | tf_op jit(solution)/shard_map/all_to_all | solution.py:289
  123.0 0.9 copy-done.3
  123.9 3.2 %shard_map.103 = (bf16[32,2048]{1,0:T(8,128)(2,1)S(1)}, bf16[32,512]{1,0:T(8,128)(2,1)S(1)}) custom-call(s32[2]{0:T(128)S(1)} %pad_add_fusion.place, bf16[8,32,640]{2,1,0:T(8,128)(2,1)S(1)} %all-to-all-done.1.arrived, bf16[32,2048]{1,0:T(8,128)(2,1)S(1)} %copy-done.3, f32[2,2048]{1,0:T(2,128)S(1)} %copy-done.6, f32[2,64]{1,0:T(2,128)S(1)} %copy-done.8, ...), custom_call_target="tpu_custom_call" | custom-call | flops 400000000 | bytes 1000000 | tf_op jit(solution)/shard_map/pallas_call | solution.py:211
  127.2 10.0 %all_to_all.20 = bf16[8,32,512]{2,1,0:T(8,128)(2,1)S(1)} all-to-all(bf16[8,32,512]{2,1,0:T(8,128)(2,1)S(1)} %broadcast_in_dim.7), channel_id=1, replica_groups=mesh['z'=8,'y'=8,'x'=4,'c'=2] {'x','c'}, dimensions={0} | all-to-all | bytes 524288 | tf_op jit(solution)/shard_map/all_to_all | solution.py:225
  137.2 8.5 %shard_map.104 = bf16[256,640]{1,0:T(8,128)(2,1)S(1)} custom-call(s32[2]{0:T(128)S(1)} %pad_add_fusion.place, bf16[256,512]{1,0:T(8,128)(2,1)S(1)} %bitcast.30, bf16[64,2,32,256]{3,2,1,0:T(8,128)(2,1)} %all-to-all-done.refs_4_.refs_1_), custom_call_target="tpu_custom_call" | custom-call | flops 5000000000 | bytes 1000000 | tf_op jit(solution)/shard_map/pallas_call | solution.py:211
  145.7 10.9 %all_to_all.21.arrived = bf16[8,32,640]{2,1,0:T(8,128)(2,1)S(1)} all-to-all(bf16[8,32,640]{2,1,0:T(8,128)(2,1)S(1)} %bitcast.29), channel_id=1, replica_groups=mesh['z'=8,'y'=8,'x'=4,'c'=2] {'x','c'}, dimensions={0} | all-to-all | bytes 655360 | tf_op jit(solution)/shard_map/all_to_all | solution.py:289
  156.6 2.6 %shard_map.105 = bf16[32,2048]{1,0:T(8,128)(2,1)} custom-call(s32[2]{0:T(128)S(1)} %pad_add_fusion.place, bf16[8,32,640]{2,1,0:T(8,128)(2,1)S(1)} %all_to_all.21.arrived, bf16[32,2048]{1,0:T(8,128)(2,1)S(1)} %get-tuple-element.8.hidden, bf16[4,192,2048]{2,1,0:T(8,128)(2,1)S(1)} %bitcast.27, bf16[4,192,2048]{2,1,0:T(8,128)(2,1)} %collective-permute-done.13.out_other.other), custom_call_target="tpu_custom_call" | custom-call | flops 200000000 | bytes 1000000 | tf_op jit(solution)/shard_map/pallas_call | solution.py:211
  (33 shorter events, 1.4 us)
Async XLA Ops:
  0.0 16.8 %copy-start.5 = (bf16[32,2048]{1,0:T(8,128)(2,1)S(1)}, bf16[32,2048]{1,0:T(8,128)(2,1)}, u32[]{:S(2)}) copy-start(bf16[32,2048]{1,0:T(8,128)(2,1)} %source.1) | copy-start | bytes 393220
  0.0 16.8 %copy-start.7 = (f32[2,2048]{1,0:T(2,128)S(1)}, f32[2,2048]{1,0:T(2,128)}, u32[]{:S(2)}) copy-start(f32[2,2048]{1,0:T(2,128)} %gain.4) | copy-start | bytes 49156
  0.0 16.8 %copy-start.9 = (f32[2,64]{1,0:T(2,128)S(1)}, f32[2,64]{1,0:T(2,128)}, u32[]{:S(2)}) copy-start(f32[2,64]{1,0:T(2,128)} %key_gain.1) | copy-start | bytes 1540
  0.0 16.8 %copy-start = (bf16[2,2048,128]{2,1,0:T(8,128)(2,1)S(1)}, bf16[2,2048,128]{2,1,0:T(8,128)(2,1)}, u32[]{:S(2)}) copy-start(bf16[2,2048,128]{2,1,0:T(8,128)(2,1)} %key_weight.1) | copy-start | bytes 3145732
  0.0 16.8 %copy-start.1 = (bf16[2,2048,128]{2,1,0:T(8,128)(2,1)S(1)}, bf16[2,2048,128]{2,1,0:T(8,128)(2,1)}, u32[]{:S(2)}) copy-start(bf16[2,2048,128]{2,1,0:T(8,128)(2,1)} %value_weight.1) | copy-start | bytes 3145732
  2.2 61.7 %collective-permute-start = (bf16[64,2048]{1,0:T(8,128)(2,1)}, bf16[64,2048]{1,0:T(8,128)(2,1)}, u32[]{:S(2)}, u32[]{:S(2)}) collective-permute-start(bf16[64,2048]{1,0:T(8,128)(2,1)} %get-tuple-element.12), channel_id=1, source_target_pairs={{2,0},{4,2},{6,4},{0,6},{3,1},{5,3},{7,5},{1,7},{10,8},{12,10},{14... | collective-permute-start | bytes 786440 | tf_op jit(solution)/shard_map/ppermute | solution.py:230
  7.4 59.3 %collective-permute-start.2 = (bf16[64,2048]{1,0:T(8,128)(2,1)}, bf16[64,2048]{1,0:T(8,128)(2,1)}, u32[]{:S(2)}, u32[]{:S(2)}) collective-permute-start(bf16[64,2048]{1,0:T(8,128)(2,1)} %get-tuple-element.12), channel_id=1, source_target_pairs={{6,0},{0,2},{2,4},{4,6},{7,1},{1,3},{3,5},{5,7},{14,8},{8,10},{10,... | collective-permute-start | bytes 786440 | tf_op jit(solution)/shard_map/ppermute | solution.py:230
  10.3 28.0 %collective-permute-start.9 = (bf16[192,2048]{1,0:T(8,128)(2,1)}, bf16[192,2048]{1,0:T(8,128)(2,1)}, u32[]{:S(2)}, u32[]{:S(2)}) collective-permute-start(bf16[192,2048]{1,0:T(8,128)(2,1)} %pad_maximum_fusion), channel_id=1, source_target_pairs={{2,0},{4,2},{6,4},{0,6},{3,1},{5,3},{7,5},{1,7},{10,8},{12,10},{14... | collective-permute-start | bytes 2359304 | tf_op jit(solution)/shard_map/ppermute | solution.py:230
  14.8 30.0 %collective-permute-start.11 = (bf16[192,2048]{1,0:T(8,128)(2,1)}, bf16[192,2048]{1,0:T(8,128)(2,1)}, u32[]{:S(2)}, u32[]{:S(2)}) collective-permute-start(bf16[192,2048]{1,0:T(8,128)(2,1)} %pad_maximum_fusion), channel_id=1, source_target_pairs={{6,0},{0,2},{2,4},{4,6},{7,1},{1,3},{3,5},{5,7},{14,8},{8,10},{10,... | collective-permute-start | bytes 2359304 | tf_op jit(solution)/shard_map/ppermute | solution.py:230
  18.9 82.3 %all-to-all-start = ((bf16[64,2,32,256]{3,2,1,0:T(8,128)(2,1)}), bf16[64,2,32,256]{3,2,1,0:T(8,128)(2,1)}, u32[]{:S(2)}, u32[]{:S(2)}) async-start(bf16[64,2,32,256]{3,2,1,0:T(8,128)(2,1)} %broadcast_in_dim.6), calls=%async_computation | async-start | bytes 4194304 | tf_op jit(solution)/shard_map/all_to_all | solution.py:225
  39.3 11.0 %collective-permute-start.10 = (bf16[96,2048]{1,0:T(8,128)(2,1)S(1)}, bf16[96,2048]{1,0:T(8,128)(2,1)S(1)}, u32[]{:S(2)}, u32[]{:S(2)}) collective-permute-start(bf16[96,2048]{1,0:T(8,128)(2,1)S(1)} %slice.36), channel_id=1, source_target_pairs={{2,0},{4,2},{6,4},{0,6},{3,1},{5,3},{7,5},{1,7},{10,8},{12,10},{14... | collective-permute-start | bytes 1179656 | tf_op jit(solution)/shard_map/ppermute | solution.py:230
  45.9 37.6 %copy-start.2 = (bf16[32,2048]{1,0:T(8,128)(2,1)S(1)}, bf16[32,2048]{1,0:T(8,128)(2,1)}, u32[]{:S(2)}) copy-start(bf16[32,2048]{1,0:T(8,128)(2,1)} %hidden.1) | copy-start | bytes 393220
  45.9 37.6 %copy-start.6 = (f32[2,2048]{1,0:T(2,128)S(1)}, f32[2,2048]{1,0:T(2,128)}, u32[]{:S(2)}) copy-start(f32[2,2048]{1,0:T(2,128)} %gain.5) | copy-start | bytes 49156
  45.9 37.6 %copy-start.8 = (f32[2,64]{1,0:T(2,128)S(1)}, f32[2,64]{1,0:T(2,128)}, u32[]{:S(2)}) copy-start(f32[2,64]{1,0:T(2,128)} %query_gain.3) | copy-start | bytes 1540
  45.9 11.7 %collective-permute-start.12 = (bf16[96,2048]{1,0:T(8,128)(2,1)S(1)}, bf16[96,2048]{1,0:T(8,128)(2,1)S(1)}, u32[]{:S(2)}, u32[]{:S(2)}) collective-permute-start(bf16[96,2048]{1,0:T(8,128)(2,1)S(1)} %slice.37), channel_id=1, source_target_pairs={{6,0},{0,2},{2,4},{4,6},{7,1},{1,3},{3,5},{5,7},{14,8},{8,10},{10,... | collective-permute-start | bytes 1179656 | tf_op jit(solution)/shard_map/ppermute | solution.py:230
  58.8 57.1 %collective-permute-start.13 = (bf16[4,192,2048]{2,1,0:T(8,128)(2,1)S(1)}, bf16[4,192,2048]{2,1,0:T(8,128)(2,1)}, u32[]{:S(2)}, u32[]{:S(2)}) collective-permute-start(bf16[4,192,2048]{2,1,0:T(8,128)(2,1)S(1)} %bitcast.24), channel_id=1, source_target_pairs={{1,0},{0,1},{3,2},{2,3},{5,4},{4,5},{7,6},{6,7},{9,8},{8,9},{11,10... | collective-permute-start | bytes 9437192 | tf_op jit(solution)/shard_map/ppermute | solution.py:230
  64.8 7.9 %collective-permute-start.1 = (bf16[32,2048]{1,0:T(8,128)(2,1)S(1)}, bf16[32,2048]{1,0:T(8,128)(2,1)S(1)}, u32[]{:S(2)}, u32[]{:S(2)}) collective-permute-start(bf16[32,2048]{1,0:T(8,128)(2,1)S(1)} %slice.33), channel_id=1, source_target_pairs={{2,0},{4,2},{6,4},{0,6},{3,1},{5,3},{7,5},{1,7},{10,8},{12,10},{14... | collective-permute-start | bytes 393224 | tf_op jit(solution)/shard_map/ppermute | solution.py:230
  67.6 8.2 %collective-permute-start.3 = (bf16[32,2048]{1,0:T(8,128)(2,1)S(1)}, bf16[32,2048]{1,0:T(8,128)(2,1)S(1)}, u32[]{:S(2)}, u32[]{:S(2)}) collective-permute-start(bf16[32,2048]{1,0:T(8,128)(2,1)S(1)} %slice.34), channel_id=1, source_target_pairs={{6,0},{0,2},{2,4},{4,6},{7,1},{1,3},{3,5},{5,7},{14,8},{8,10},{10,... | collective-permute-start | bytes 393224 | tf_op jit(solution)/shard_map/ppermute | solution.py:230
  78.2 5.3 %collective-permute-start.4 = (bf16[4,64,2048]{2,1,0:T(8,128)(2,1)}, bf16[4,64,2048]{2,1,0:T(8,128)(2,1)}, u32[]{:S(2)}, u32[]{:S(2)}) collective-permute-start(bf16[4,64,2048]{2,1,0:T(8,128)(2,1)} %bitcast.4.mine), channel_id=1, source_target_pairs={{1,0},{0,1},{3,2},{2,3},{5,4},{4,5},{7,6},{6,7},{9,8},{8,9},{11,10... | collective-permute-start | bytes 3145736 | tf_op jit(solution)/shard_map/ppermute | solution.py:230
  86.0 3.1 %collective-permute-start.5 = (bf16[32,512]{1,0:T(8,128)(2,1)S(1)}, bf16[32,512]{1,0:T(8,128)(2,1)S(1)}, u32[]{:S(2)}, u32[]{:S(2)}) collective-permute-start(bf16[32,512]{1,0:T(8,128)(2,1)S(1)} %shard_map.100), channel_id=1, source_target_pairs={{1,0},{0,1},{3,2},{2,3},{5,4},{4,5},{7,6},{6,7},{9,8},{8,9},{11,10... | collective-permute-start | bytes 98312 | tf_op jit(solution)/shard_map/ppermute | solution.py:230
  89.1 7.8 %collective-permute-start.6 = (bf16[64,512]{1,0:T(8,128)(2,1)S(1)}, bf16[64,512]{1,0:T(8,128)(2,1)S(1)}, u32[]{:S(2)}, u32[]{:S(2)}) collective-permute-start(bf16[64,512]{1,0:T(8,128)(2,1)S(1)} %pad_maximum_fusion.1.refs_0_), channel_id=1, source_target_pairs={{2,0},{4,2},{6,4},{0,6},{3,1},{5,3},{7,5},{1,7},{10,8},{12,10},{14... | collective-permute-start | bytes 196616 | tf_op jit(solution)/shard_map/ppermute | solution.py:230
  91.1 6.5 %collective-permute-start.7 = (bf16[64,512]{1,0:T(8,128)(2,1)S(1)}, bf16[64,512]{1,0:T(8,128)(2,1)S(1)}, u32[]{:S(2)}, u32[]{:S(2)}) collective-permute-start(bf16[64,512]{1,0:T(8,128)(2,1)S(1)} %pad_maximum_fusion.1.refs_0_), channel_id=1, source_target_pairs={{4,0},{6,2},{0,4},{2,6},{5,1},{7,3},{1,5},{3,7},{12,8},{14,10},{8,... | collective-permute-start | bytes 196616 | tf_op jit(solution)/shard_map/ppermute | solution.py:230
  95.0 6.2 %collective-permute-start.8 = (bf16[64,512]{1,0:T(8,128)(2,1)S(1)}, bf16[64,512]{1,0:T(8,128)(2,1)S(1)}, u32[]{:S(2)}, u32[]{:S(2)}) collective-permute-start(bf16[64,512]{1,0:T(8,128)(2,1)S(1)} %pad_maximum_fusion.1.refs_0_), channel_id=1, source_target_pairs={{6,0},{0,2},{2,4},{4,6},{7,1},{1,3},{3,5},{5,7},{14,8},{8,10},{10,... | collective-permute-start | bytes 196616 | tf_op jit(solution)/shard_map/ppermute | solution.py:230
  109.8 0.7 copy-start.4
  110.5 12.5 %all-to-all-start.1 = ((bf16[8,32,640]{2,1,0:T(8,128)(2,1)}), bf16[8,32,640]{2,1,0:T(8,128)(2,1)S(1)}, u32[]{:S(2)}, u32[]{:S(2)}) async-start(bf16[8,32,640]{2,1,0:T(8,128)(2,1)} %bitcast.28), calls=%async_computation.1 | async-start | bytes 655360 | tf_op jit(solution)/shard_map/all_to_all | solution.py:289
  123.0 0.9 copy-start.3
where the time goes:
time: 161 us; the launch traced here: 159 us
  starting transfers between devices  65.2 us (40%)
  Pallas kernels  26 us (16%)
  waiting for transfers between devices  25.6 us (16%)
  blocking collectives  20.9 us (13%)
  local copies, waits for them, and re-layouts  20.2 us (13%)
    ppermute x14, starting transfers between devices, shifted(): lax.ppermute(value, axis, [((k + step) % size, k) for k in range(size)])  43.2 us
    pallas_call x5, Pallas kernels, with_place(): pl.pallas_call(kernel, grid=(1,), out_shape=shapes, in_specs=specs, out_s...  25.5 us
    ppermute x14, waiting for transfers between devices, shifted(): lax.ppermute(value, axis, [((k + step) % size, k) for k in range(size)])  18.5 us
    all_to_all x1, starting transfers between devices, to_all(): return lax.all_to_all(copies, axis, split_axis=0, concat_axis=0, tiled=True)  16.6 us
    all_to_all x1, blocking collectives, decoder(): lax.all_to_all(partial.reshape(-1, rows, wide), TP, split_axis=0, concat_...  10.9 us
    all_to_all x1, blocking collectives, to_all(): return lax.all_to_all(copies, axis, split_axis=0, concat_axis=0, tiled=True)  10 us
    unnamed x29, local copies, waits for them, and re-layouts  9.67 us
    all_to_all x1, waiting for transfers between devices, decoder(): lax.all_to_all(partial.reshape(-1, rows, wide), TP, split_axis=0, concat_...  7.11 us
  transfers between devices with their start and end apart: 16, of which 8 were waited for; matrix products, arithmetic and copies ran while one was open for 11% of the time, Pallas kernels for 7%

commit v1 on v0

--- a/solution.py
+++ b/solution.py
@@ -62,13 +62,14 @@
         out[layer, :, width:] = dot(normed, value_weight[layer]).astype(BF16)
 
 
-def project(normed, mine, other, row, head, place):
+def project(normed, mine, other, row, head, place, turned=True):
     x, core = place[0], place[1]
     model = normed.shape[1]
     own = jnp.concatenate(head_norm(dot_t(normed, mine.reshape(-1, model)), row, head), axis=1)
     far = jnp.concatenate(head_norm(dot_t(normed, other.reshape(-1, model)), row, head), axis=1)
-    own = pltpu.roll(own, x * head, 1)
-    far = pltpu.roll(far, x * head, 1)
+    if turned:
+        own = pltpu.roll(own, x * head, 1)
+        far = pltpu.roll(far, x * head, 1)
     return jnp.where(core == 0, own, far), jnp.where(core == 0, far, own)
 
 
@@ -83,7 +84,7 @@
     value = target[...].astype(F32)
     normed = (value * rms(value) * gain[layer : layer + 1, :]).astype(BF16)
     row = doubled(query_gain[layer : layer + 1, :])
-    store_groups(out, project(normed, mine[...], other[...], row, head, place))
+    store_groups(out, project(normed, mine[...], other[...], row, head, place, turned=False))
 
 
 def attended_halves(arrived, heads, head):
@@ -180,19 +181,6 @@
             out[pl.ds(pl.multiple_of(to * each, each), each), :] = result[first : first + each, :]
 
 
-def call(kernel, shapes, scratch=(), flops=1000000):
-    one = not isinstance(shapes, (list, tuple))
-    specs = pl.BlockSpec(memory_space=pltpu.VMEM)
-    return pl.pallas_call(
-        kernel,
-        out_shape=shapes,
-        out_specs=specs if one else [specs] * len(shapes),
-        scratch_shapes=list(scratch),
-        compiler_params=pltpu.CompilerParams(vmem_limit_bytes=40 * 1024 * 1024),
-        cost_estimate=pl.CostEstimate(flops=flops, bytes_accessed=1000000, transcendentals=0),
-    )
-
-
 def whole(value):
     return pl.BlockSpec(value.shape, lambda i, n=value.ndim: (0,) * n)
 
@@ -206,7 +194,8 @@
 def with_place(kernel, shapes, operands, parts, flops, scratch=()):
     one = not isinstance(shapes, (list, tuple))
     place, *rest = operands
-    specs = [pl.BlockSpec(memory_space=pltpu.SMEM)] + [whole(value) for value in rest]
+    placed = [] if place is None else [place]
+    specs = [pl.BlockSpec(memory_space=pltpu.SMEM)] * len(placed) + [whole(value) for value in rest]
     specs += [part_of(*part) for part in parts]
     return pl.pallas_call(
         kernel,
@@ -217,7 +206,7 @@
         scratch_shapes=list(scratch),
         compiler_params=pltpu.CompilerParams(vmem_limit_bytes=40 * 1024 * 1024),
         cost_estimate=pl.CostEstimate(flops=flops, bytes_accessed=1000000, transcendentals=0),
-    )(place, *rest, *(part[0] for part in parts))
+    )(*placed, *rest, *(part[0] for part in parts))
 
 
 def to_all(value, axis):
@@ -249,8 +238,12 @@
     width = heads * head
     wide = width + 128
 
-    pairs = call(source_kernel, shapes((layers, rows, 4 * head), BF16), flops=200000000)(
-        source, source_gain, key_gain, key_weight, value_weight
+    pairs = with_place(
+        source_kernel,
+        shapes((layers, rows, 4 * head), BF16),
+        (None, source, source_gain, key_gain, key_weight, value_weight),
+        [],
+        200000000,
     )
     plane = to_all(pairs, ROWS)
     keys = plane.shape[0] * rows
@@ -258,7 +251,7 @@
     def both(stacked):
         return stacked, shifted(stacked, "c", 1)
 
-    first = both(around(query_t[0]))
+    first = both(to_all(query_t[0], "x"))
     rest = both(around(jnp.concatenate([out_weight[0], query_t[1], out_weight[1]], axis=0)))
     rest = [[(part, k, head) for part in rest] for k in range(3)]
 

time: 161 us -> 151 us (0.938)
  local copies, waits for them, and re-layouts: 20.2 us -> 12.3 us
    ppermute x14 -> x10, starting transfers between devices: 43.2 us -> 29.4 us  [shifted(): lax.ppermute(value, axis, [((k + step) % size, k) for k in range(size)])]
    all_to_all x1 -> x2, starting transfers between devices: 16.6 us -> 26.3 us  [to_all(): return lax.all_to_all(copies, axis, split_axis=0, concat_axis=0, tiled=True)]
    unnamed x29 -> x28, local copies, waits for them, and re-layouts: 9.67 us -> 4.9 us
    all_to_all x1, starting transfers between devices: 5.38 us -> 7.8 us  [decoder(): lax.all_to_all(partial.reshape(-1, rows, wide), TP, split_axis=0, concat_...]
    slice x4 -> x2, local copies, waits for them, and re-layouts: 3.87 us -> 2.05 us  [around(): far = [shifted(right[:half], 'x', 1), shifted(left[half:], 'x', -1)]]
    all_to_all x1 -> x2, waiting for transfers between devices: 0.01 us -> 1.71 us  [to_all(): return lax.all_to_all(copies, axis, split_axis=0, concat_axis=0, tiled=True)]
    concatenate x2 -> x1, local copies, waits for them, and re-layouts: 2.89 us -> 1.2 us  [around(): jnp.concatenate([value, right, *far, left], axis=0).reshape(4, *value.shape)]
    ppermute x14 -> x10, waiting for transfers between devices: 18.5 us -> 16.9 us  [shifted(): lax.ppermute(value, axis, [((k + step) % size, k) for k in range(size)])]
  transfers between devices with their start and end apart: 16 -> 13, of which waited for: 8 -> 8; matrix products, arithmetic and copies ran while one was open for 11% -> 6% of each run, Pallas kernels for 7% -> 8%
where the time goes in v1:
time: 151 us; the launch traced here: 150 us
  starting transfers between devices  63.6 us (42%)
  Pallas kernels  25.9 us (17%)
  waiting for transfers between devices  25.7 us (17%)
  blocking collectives  20.9 us (14%)
  local copies, waits for them, and re-layouts  12.3 us (8%)
    ppermute x10, starting transfers between devices, shifted(): lax.ppermute(value, axis, [((k + step) % size, k) for k in range(size)])  29.4 us
    all_to_all x2, starting transfers between devices, to_all(): return lax.all_to_all(copies, axis, split_axis=0, concat_axis=0, tiled=True)  26.3 us
    pallas_call x6, Pallas kernels, with_place(): pl.pallas_call(kernel, grid=(1,), out_shape=shapes, in_specs=specs, out_s...  25.9 us
    ppermute x10, waiting for transfers between devices, shifted(): lax.ppermute(value, axis, [((k + step) % size, k) for k in range(size)])  16.9 us
    all_to_all x1, blocking collectives, decoder(): lax.all_to_all(partial.reshape(-1, rows, wide), TP, split_axis=0, concat_...  10.9 us
    all_to_all x1, blocking collectives, to_all(): return lax.all_to_all(copies, axis, split_axis=0, concat_axis=0, tiled=True)  10 us
    all_to_all x1, starting transfers between devices, decoder(): lax.all_to_all(partial.reshape(-1, rows, wide), TP, split_axis=0, concat_...  7.8 us
    all_to_all x1, waiting for transfers between devices, decoder(): lax.all_to_all(partial.reshape(-1, rows, wide), TP, split_axis=0, concat_...  7.11 us
  transfers between devices with their start and end apart: 13, of which 8 were waited for; matrix products, arithmetic and copies ran while one was open for 6% of the time, Pallas kernels for 8%

profile of v1, /device:TPU:1, one launch (start us, length us, event | category | flops | bytes accessed | tf_op | source)
XLA Modules:
  0.0 149.7 jit_solution(4688588546961171891)
XLA Ops:
  0.0 1.4 slice_bitcast_fusion
  1.4 1.1 broadcast_in_dim.9
  2.6 4.8 %all-to-all-start = ((bf16[4,64,2048]{2,1,0:T(8,128)(2,1)}), bf16[4,64,2048]{2,1,0:T(8,128)(2,1)}, u32[]{:S(2)}, u32[]{:S(2)}) async-start(bf16[4,64,2048]{2,1,0:T(8,128)(2,1)} %broadcast_in_dim.9), calls=%async_computation | async-start | bytes 2097152 | tf_op jit(solution)/shard_map/all_to_all | solution.py:214
  7.4 0.9 pad_maximum_fusion
  8.4 4.6 %collective-permute-start.5 = (bf16[192,2048]{1,0:T(8,128)(2,1)}, bf16[192,2048]{1,0:T(8,128)(2,1)}, u32[]{:S(2)}, u32[]{:S(2)}) collective-permute-start(bf16[192,2048]{1,0:T(8,128)(2,1)} %pad_maximum_fusion), channel_id=1, source_target_pairs={{2,0},{4,2},{6,4},{0,6},{3,1},{5,3},{7,5},{1,7},{10,8},{12,10},{14... | collective-permute-start | bytes 2359304 | tf_op jit(solution)/shard_map/ppermute | solution.py:219
  13.0 1.9 %collective-permute-start.7 = (bf16[192,2048]{1,0:T(8,128)(2,1)}, bf16[192,2048]{1,0:T(8,128)(2,1)}, u32[]{:S(2)}, u32[]{:S(2)}) collective-permute-start(bf16[192,2048]{1,0:T(8,128)(2,1)} %pad_maximum_fusion), channel_id=1, source_target_pairs={{6,0},{0,2},{2,4},{4,6},{7,1},{1,3},{3,5},{5,7},{14,8},{8,10},{10,... | collective-permute-start | bytes 2359304 | tf_op jit(solution)/shard_map/ppermute | solution.py:219
  15.0 0.5 shard_map.101
  15.6 1.7 %all-to-all-done.mine = bf16[4,64,2048]{2,1,0:T(8,128)(2,1)} async-done(((bf16[4,64,2048]{2,1,0:T(8,128)(2,1)}), bf16[4,64,2048]{2,1,0:T(8,128)(2,1)}, u32[]{:S(2)}, u32[]{:S(2)}) %all-to-all-start) | async-done | bytes 1048608 | tf_op jit(solution)/shard_map/all_to_all | solution.py:214
  17.3 1.6 %broadcast_in_dim.10 = bf16[64,2,32,256]{3,2,1,0:T(8,128)(2,1)} broadcast(bf16[2,32,256]{2,1,0:T(8,128)(2,1)S(1)} %shard_map.101), dimensions={1,2,3} | broadcast | bytes 2129920 | tf_op jit(solution)/shard_map/broadcast_in_dim | solution.py:213
  18.9 21.5 %all-to-all-start.1 = ((bf16[64,2,32,256]{3,2,1,0:T(8,128)(2,1)}), bf16[64,2,32,256]{3,2,1,0:T(8,128)(2,1)}, u32[]{:S(2)}, u32[]{:S(2)}) async-start(bf16[64,2,32,256]{3,2,1,0:T(8,128)(2,1)} %broadcast_in_dim.10), calls=%async_computation.1 | async-start | bytes 4194304 | tf_op jit(solution)/shard_map/all_to_all | solution.py:214
  40.4 1.0 constant_dynamic-update-slice_fusion.5
  41.4 1.0 slice.26
  42.4 0.0 copy-start.2
  42.4 0.0 copy-start.6
  42.4 0.0 copy-start.8
  42.4 2.9 %collective-permute-start.6 = (bf16[96,2048]{1,0:T(8,128)(2,1)S(1)}, bf16[96,2048]{1,0:T(8,128)(2,1)S(1)}, u32[]{:S(2)}, u32[]{:S(2)}) collective-permute-start(bf16[96,2048]{1,0:T(8,128)(2,1)S(1)} %slice.26), channel_id=1, source_target_pairs={{2,0},{4,2},{6,4},{0,6},{3,1},{5,3},{7,5},{1,7},{10,8},{12,10},{14... | collective-permute-start | bytes 1179656 | tf_op jit(solution)/shard_map/ppermute | solution.py:219
  45.3 1.0 constant_dynamic-update-slice_fusion.4
  46.3 0.0 collective-permute-done.7
  46.3 1.0 slice.27
  47.4 2.5 %collective-permute-start.8 = (bf16[96,2048]{1,0:T(8,128)(2,1)S(1)}, bf16[96,2048]{1,0:T(8,128)(2,1)S(1)}, u32[]{:S(2)}, u32[]{:S(2)}) collective-permute-start(bf16[96,2048]{1,0:T(8,128)(2,1)S(1)} %slice.27), channel_id=1, source_target_pairs={{6,0},{0,2},{2,4},{4,6},{7,1},{1,3},{3,5},{5,7},{14,8},{8,10},{10,... | collective-permute-start | bytes 1179656 | tf_op jit(solution)/shard_map/ppermute | solution.py:219
  49.9 1.2 constant_dynamic-update-slice_fusion.3
  51.1 1.1 collective-permute-done.6
  52.1 5.7 %collective-permute-done.8 = bf16[96,2048]{1,0:T(8,128)(2,1)S(1)} collective-permute-done((bf16[96,2048]{1,0:T(8,128)(2,1)S(1)}, bf16[96,2048]{1,0:T(8,128)(2,1)S(1)}, u32[]{:S(2)}, u32[]{:S(2)}) %collective-permute-start.8) | collective-permute-done | bytes 393248 | tf_op jit(solution)/shard_map/ppermute | solution.py:219
  57.9 1.2 constant_dynamic-update-slice_fusion
  59.1 6.1 %collective-permute-start.9 = (bf16[4,192,2048]{2,1,0:T(8,128)(2,1)S(1)}, bf16[4,192,2048]{2,1,0:T(8,128)(2,1)}, u32[]{:S(2)}, u32[]{:S(2)}) collective-permute-start(bf16[4,192,2048]{2,1,0:T(8,128)(2,1)S(1)} %bitcast.21), channel_id=1, source_target_pairs={{1,0},{0,1},{3,2},{2,3},{5,4},{4,5},{7,6},{6,7},{9,8},{8,9},{11,10... | collective-permute-start | bytes 9437192 | tf_op jit(solution)/shard_map/ppermute | solution.py:219
  65.2 1.9 %collective-permute-start = (bf16[4,64,2048]{2,1,0:T(8,128)(2,1)}, bf16[4,64,2048]{2,1,0:T(8,128)(2,1)}, u32[]{:S(2)}, u32[]{:S(2)}) collective-permute-start(bf16[4,64,2048]{2,1,0:T(8,128)(2,1)} %all-to-all-done.mine), channel_id=1, source_target_pairs={{1,0},{0,1},{3,2},{2,3},{5,4},{4,5},{7,6},{6,7},{9,8},{8,9},{11,10... | collective-permute-start | bytes 3145736 | tf_op jit(solution)/shard_map/ppermute | solution.py:219
  67.1 0.1 pad_add_fusion.place
  67.2 4.9 %collective-permute-done.other = bf16[4,64,2048]{2,1,0:T(8,128)(2,1)} collective-permute-done((bf16[4,64,2048]{2,1,0:T(8,128)(2,1)}, bf16[4,64,2048]{2,1,0:T(8,128)(2,1)}, u32[]{:S(2)}, u32[]{:S(2)}) %collective-permute-start) | collective-permute-done | bytes 1048608 | tf_op jit(solution)/shard_map/ppermute | solution.py:219
  72.1 2.4 %shard_map.100 = bf16[32,512]{1,0:T(8,128)(2,1)S(1)} custom-call(s32[2]{0:T(128)S(1)} %pad_add_fusion.place, bf16[32,2048]{1,0:T(8,128)(2,1)S(1)} %copy-done.2, f32[2,2048]{1,0:T(2,128)S(1)} %copy-done.6, f32[2,64]{1,0:T(2,128)S(1)} %copy-done.8, bf16[4,64,2048]{2,1,0:T(8,128)(2,1)} %all-to-all-done.mine, bf16[4,64,2048]{2,1,0:T(8,128)(2,1)} %collective-permute-done.other), custom_call_target="tpu_custom_call" | custom-call | flops 200000000 | bytes 1000000 | tf_op jit(solution)/shard_map/pallas_call | solution.py:200
  74.5 2.3 %collective-permute-start.1 = (bf16[32,512]{1,0:T(8,128)(2,1)S(1)}, bf16[32,512]{1,0:T(8,128)(2,1)S(1)}, u32[]{:S(2)}, u32[]{:S(2)}) collective-permute-start(bf16[32,512]{1,0:T(8,128)(2,1)S(1)} %shard_map.100), channel_id=1, source_target_pairs={{1,0},{0,1},{3,2},{2,3},{5,4},{4,5},{7,6},{6,7},{9,8},{8,9},{11,10... | collective-permute-start | bytes 98312 | tf_op jit(solution)/shard_map/ppermute | solution.py:219
  76.8 0.8 collective-permute-done.1
  77.6 1.9 %collective-permute-start.2 = (bf16[64,512]{1,0:T(8,128)(2,1)S(1)}, bf16[64,512]{1,0:T(8,128)(2,1)S(1)}, u32[]{:S(2)}, u32[]{:S(2)}) collective-permute-start(bf16[64,512]{1,0:T(8,128)(2,1)S(1)} %pad_maximum_fusion.1.refs_0_), channel_id=1, source_target_pairs={{2,0},{4,2},{6,4},{0,6},{3,1},{5,3},{7,5},{1,7},{10,8},{12,10},{14... | collective-permute-start | bytes 196616 | tf_op jit(solution)/shard_map/ppermute | solution.py:219
  79.5 3.1 %collective-permute-start.3 = (bf16[64,512]{1,0:T(8,128)(2,1)S(1)}, bf16[64,512]{1,0:T(8,128)(2,1)S(1)}, u32[]{:S(2)}, u32[]{:S(2)}) collective-permute-start(bf16[64,512]{1,0:T(8,128)(2,1)S(1)} %pad_maximum_fusion.1.refs_0_), channel_id=1, source_target_pairs={{4,0},{6,2},{0,4},{2,6},{5,1},{7,3},{1,5},{3,7},{12,8},{14,10},{8,... | collective-permute-start | bytes 196616 | tf_op jit(solution)/shard_map/ppermute | solution.py:219
  82.6 2.2 %collective-permute-start.4 = (bf16[64,512]{1,0:T(8,128)(2,1)S(1)}, bf16[64,512]{1,0:T(8,128)(2,1)S(1)}, u32[]{:S(2)}, u32[]{:S(2)}) collective-permute-start(bf16[64,512]{1,0:T(8,128)(2,1)S(1)} %pad_maximum_fusion.1.refs_0_), channel_id=1, source_target_pairs={{6,0},{0,2},{2,4},{4,6},{7,1},{1,3},{3,5},{5,7},{14,8},{8,10},{10,... | collective-permute-start | bytes 196616 | tf_op jit(solution)/shard_map/ppermute | solution.py:219
  84.8 0.0 collective-permute-done.2.refs_1_
  84.8 1.6 %collective-permute-done.3.refs_2_ = bf16[64,512]{1,0:T(8,128)(2,1)S(1)} collective-permute-done((bf16[64,512]{1,0:T(8,128)(2,1)S(1)}, bf16[64,512]{1,0:T(8,128)(2,1)S(1)}, u32[]{:S(2)}, u32[]{:S(2)}) %collective-permute-start.3) | collective-permute-done | bytes 65568 | tf_op jit(solution)/shard_map/ppermute | solution.py:219
  86.4 2.8 %collective-permute-done.4.refs_3_ = bf16[64,512]{1,0:T(8,128)(2,1)S(1)} collective-permute-done((bf16[64,512]{1,0:T(8,128)(2,1)S(1)}, bf16[64,512]{1,0:T(8,128)(2,1)S(1)}, u32[]{:S(2)}, u32[]{:S(2)}) %collective-permute-start.4) | collective-permute-done | bytes 65568 | tf_op jit(solution)/shard_map/ppermute | solution.py:219
  89.3 8.6 %shard_map.102 = bf16[256,640]{1,0:T(8,128)(2,1)S(1)} custom-call(s32[2]{0:T(128)S(1)} %pad_add_fusion.place, bf16[64,512]{1,0:T(8,128)(2,1)S(1)} %pad_maximum_fusion.1.refs_0_, bf16[64,512]{1,0:T(8,128)(2,1)S(1)} %collective-permute-done.2.refs_1_, bf16[64,512]{1,0:T(8,128)(2,1)S(1)} %collective-permute-done.3.refs_2_, ...), custom_call_target="tpu_custom_call" | custom-call | flops 5000000000 | bytes 1000000 | tf_op jit(solution)/shard_map/pallas_call | solution.py:200
  97.8 0.7 copy-done.4
  98.6 7.8 %all-to-all-start.2 = ((bf16[8,32,640]{2,1,0:T(8,128)(2,1)}), bf16[8,32,640]{2,1,0:T(8,128)(2,1)S(1)}, u32[]{:S(2)}, u32[]{:S(2)}) async-start(bf16[8,32,640]{2,1,0:T(8,128)(2,1)} %bitcast.25), calls=%async_computation.2 | async-start | bytes 655360 | tf_op jit(solution)/shard_map/all_to_all | solution.py:282
  106.4 0.0 collective-permute-done.9.out_other.other
  106.4 7.1 %all-to-all-done.2.arrived = bf16[8,32,640]{2,1,0:T(8,128)(2,1)S(1)} async-done(((bf16[8,32,640]{2,1,0:T(8,128)(2,1)}), bf16[8,32,640]{2,1,0:T(8,128)(2,1)S(1)}, u32[]{:S(2)}, u32[]{:S(2)}) %all-to-all-start.2) | async-done | bytes 327712 | tf_op jit(solution)/shard_map/all_to_all | solution.py:282
  113.5 0.9 copy-done.3
  114.4 3.2 %shard_map.103 = (bf16[32,2048]{1,0:T(8,128)(2,1)S(1)}, bf16[32,512]{1,0:T(8,128)(2,1)S(1)}) custom-call(s32[2]{0:T(128)S(1)} %pad_add_fusion.place, bf16[8,32,640]{2,1,0:T(8,128)(2,1)S(1)} %all-to-all-done.2.arrived, bf16[32,2048]{1,0:T(8,128)(2,1)S(1)} %copy-done.3, f32[2,2048]{1,0:T(2,128)S(1)} %copy-done.6, f32[2,64]{1,0:T(2,128)S(1)} %copy-done.8, ...), custom_call_target="tpu_custom_call" | custom-call | flops 400000000 | bytes 1000000 | tf_op jit(solution)/shard_map/pallas_call | solution.py:200
  117.7 10.0 %all_to_all.25 = bf16[8,32,512]{2,1,0:T(8,128)(2,1)S(1)} all-to-all(bf16[8,32,512]{2,1,0:T(8,128)(2,1)S(1)} %broadcast_in_dim.11), channel_id=1, replica_groups=mesh['z'=8,'y'=8,'x'=4,'c'=2] {'x','c'}, dimensions={0} | all-to-all | bytes 524288 | tf_op jit(solution)/shard_map/all_to_all | solution.py:214
  127.7 8.5 %shard_map.104 = bf16[256,640]{1,0:T(8,128)(2,1)S(1)} custom-call(s32[2]{0:T(128)S(1)} %pad_add_fusion.place, bf16[256,512]{1,0:T(8,128)(2,1)S(1)} %bitcast.27, bf16[64,2,32,256]{3,2,1,0:T(8,128)(2,1)} %all-to-all-done.1.refs_4_.refs_1_), custom_call_target="tpu_custom_call" | custom-call | flops 5000000000 | bytes 1000000 | tf_op jit(solution)/shard_map/pallas_call | solution.py:200
  136.2 10.9 %all_to_all.26.arrived = bf16[8,32,640]{2,1,0:T(8,128)(2,1)S(1)} all-to-all(bf16[8,32,640]{2,1,0:T(8,128)(2,1)S(1)} %bitcast.26), channel_id=1, replica_groups=mesh['z'=8,'y'=8,'x'=4,'c'=2] {'x','c'}, dimensions={0} | all-to-all | bytes 655360 | tf_op jit(solution)/shard_map/all_to_all | solution.py:282
  147.1 2.6 %shard_map.105 = bf16[32,2048]{1,0:T(8,128)(2,1)} custom-call(s32[2]{0:T(128)S(1)} %pad_add_fusion.place, bf16[8,32,640]{2,1,0:T(8,128)(2,1)S(1)} %all_to_all.26.arrived, bf16[32,2048]{1,0:T(8,128)(2,1)S(1)} %get-tuple-element.8.hidden, bf16[4,192,2048]{2,1,0:T(8,128)(2,1)S(1)} %bitcast.24, bf16[4,192,2048]{2,1,0:T(8,128)(2,1)} %collective-permute-done.9.out_other.other), custom_call_target="tpu_custom_call" | custom-call | flops 200000000 | bytes 1000000 | tf_op jit(solution)/shard_map/pallas_call | solution.py:200
  (24 shorter events, 0.1 us)
Async XLA Ops:
  0.0 14.9 %copy-start = (bf16[2,2048,128]{2,1,0:T(8,128)(2,1)S(1)}, bf16[2,2048,128]{2,1,0:T(8,128)(2,1)}, u32[]{:S(2)}) copy-start(bf16[2,2048,128]{2,1,0:T(8,128)(2,1)} %key_weight.1) | copy-start | bytes 3145732
  0.0 14.9 %copy-start.1 = (bf16[2,2048,128]{2,1,0:T(8,128)(2,1)S(1)}, bf16[2,2048,128]{2,1,0:T(8,128)(2,1)}, u32[]{:S(2)}) copy-start(bf16[2,2048,128]{2,1,0:T(8,128)(2,1)} %value_weight.1) | copy-start | bytes 3145732
  0.0 15.0 %copy-start.5 = (bf16[32,2048]{1,0:T(8,128)(2,1)S(1)}, bf16[32,2048]{1,0:T(8,128)(2,1)}, u32[]{:S(2)}) copy-start(bf16[32,2048]{1,0:T(8,128)(2,1)} %source.1) | copy-start | bytes 393220
  0.0 15.0 %copy-start.7 = (f32[2,2048]{1,0:T(2,128)S(1)}, f32[2,2048]{1,0:T(2,128)}, u32[]{:S(2)}) copy-start(f32[2,2048]{1,0:T(2,128)} %gain.4) | copy-start | bytes 49156
  0.0 15.0 %copy-start.9 = (f32[2,64]{1,0:T(2,128)S(1)}, f32[2,64]{1,0:T(2,128)}, u32[]{:S(2)}) copy-start(f32[2,64]{1,0:T(2,128)} %key_gain.1) | copy-start | bytes 1540
  2.6 14.7 %all-to-all-start = ((bf16[4,64,2048]{2,1,0:T(8,128)(2,1)}), bf16[4,64,2048]{2,1,0:T(8,128)(2,1)}, u32[]{:S(2)}, u32[]{:S(2)}) async-start(bf16[4,64,2048]{2,1,0:T(8,128)(2,1)} %broadcast_in_dim.9), calls=%async_computation | async-start | bytes 2097152 | tf_op jit(solution)/shard_map/all_to_all | solution.py:214
  7.4 8.1 %copy-start.10 = (bf16[2,64,2048]{2,1,0:T(8,128)(2,1)S(1)}, bf16[2,64,2048]{2,1,0:T(8,128)(2,1)}, u32[]{:S(2)}) copy-start(bf16[2,64,2048]{2,1,0:T(8,128)(2,1)} %param.19) | copy-start | bytes 1572868
  8.4 33.0 %collective-permute-start.5 = (bf16[192,2048]{1,0:T(8,128)(2,1)}, bf16[192,2048]{1,0:T(8,128)(2,1)}, u32[]{:S(2)}, u32[]{:S(2)}) collective-permute-start(bf16[192,2048]{1,0:T(8,128)(2,1)} %pad_maximum_fusion), channel_id=1, source_target_pairs={{2,0},{4,2},{6,4},{0,6},{3,1},{5,3},{7,5},{1,7},{10,8},{12,10},{14... | collective-permute-start | bytes 2359304 | tf_op jit(solution)/shard_map/ppermute | solution.py:219
  13.0 33.3 %collective-permute-start.7 = (bf16[192,2048]{1,0:T(8,128)(2,1)}, bf16[192,2048]{1,0:T(8,128)(2,1)}, u32[]{:S(2)}, u32[]{:S(2)}) collective-permute-start(bf16[192,2048]{1,0:T(8,128)(2,1)} %pad_maximum_fusion), channel_id=1, source_target_pairs={{6,0},{0,2},{2,4},{4,6},{7,1},{1,3},{3,5},{5,7},{14,8},{8,10},{10,... | collective-permute-start | bytes 2359304 | tf_op jit(solution)/shard_map/ppermute | solution.py:219
  18.9 70.4 %all-to-all-start.1 = ((bf16[64,2,32,256]{3,2,1,0:T(8,128)(2,1)}), bf16[64,2,32,256]{3,2,1,0:T(8,128)(2,1)}, u32[]{:S(2)}, u32[]{:S(2)}) async-start(bf16[64,2,32,256]{3,2,1,0:T(8,128)(2,1)} %broadcast_in_dim.10), calls=%async_computation.1 | async-start | bytes 4194304 | tf_op jit(solution)/shard_map/all_to_all | solution.py:214
  42.4 29.7 %copy-start.2 = (bf16[32,2048]{1,0:T(8,128)(2,1)S(1)}, bf16[32,2048]{1,0:T(8,128)(2,1)}, u32[]{:S(2)}) copy-start(bf16[32,2048]{1,0:T(8,128)(2,1)} %hidden.1) | copy-start | bytes 393220
  42.4 29.7 %copy-start.6 = (f32[2,2048]{1,0:T(2,128)S(1)}, f32[2,2048]{1,0:T(2,128)}, u32[]{:S(2)}) copy-start(f32[2,2048]{1,0:T(2,128)} %gain.5) | copy-start | bytes 49156
  42.4 29.6 %copy-start.8 = (f32[2,64]{1,0:T(2,128)S(1)}, f32[2,64]{1,0:T(2,128)}, u32[]{:S(2)}) copy-start(f32[2,64]{1,0:T(2,128)} %query_gain.3) | copy-start | bytes 1540
  42.4 9.7 %collective-permute-start.6 = (bf16[96,2048]{1,0:T(8,128)(2,1)S(1)}, bf16[96,2048]{1,0:T(8,128)(2,1)S(1)}, u32[]{:S(2)}, u32[]{:S(2)}) collective-permute-start(bf16[96,2048]{1,0:T(8,128)(2,1)S(1)} %slice.26), channel_id=1, source_target_pairs={{2,0},{4,2},{6,4},{0,6},{3,1},{5,3},{7,5},{1,7},{10,8},{12,10},{14... | collective-permute-start | bytes 1179656 | tf_op jit(solution)/shard_map/ppermute | solution.py:219
  47.4 10.5 %collective-permute-start.8 = (bf16[96,2048]{1,0:T(8,128)(2,1)S(1)}, bf16[96,2048]{1,0:T(8,128)(2,1)S(1)}, u32[]{:S(2)}, u32[]{:S(2)}) collective-permute-start(bf16[96,2048]{1,0:T(8,128)(2,1)S(1)} %slice.27), channel_id=1, source_target_pairs={{6,0},{0,2},{2,4},{4,6},{7,1},{1,3},{3,5},{5,7},{14,8},{8,10},{10,... | collective-permute-start | bytes 1179656 | tf_op jit(solution)/shard_map/ppermute | solution.py:219
  59.1 47.3 %collective-permute-start.9 = (bf16[4,192,2048]{2,1,0:T(8,128)(2,1)S(1)}, bf16[4,192,2048]{2,1,0:T(8,128)(2,1)}, u32[]{:S(2)}, u32[]{:S(2)}) collective-permute-start(bf16[4,192,2048]{2,1,0:T(8,128)(2,1)S(1)} %bitcast.21), channel_id=1, source_target_pairs={{1,0},{0,1},{3,2},{2,3},{5,4},{4,5},{7,6},{6,7},{9,8},{8,9},{11,10... | collective-permute-start | bytes 9437192 | tf_op jit(solution)/shard_map/ppermute | solution.py:219
  65.2 6.9 %collective-permute-start = (bf16[4,64,2048]{2,1,0:T(8,128)(2,1)}, bf16[4,64,2048]{2,1,0:T(8,128)(2,1)}, u32[]{:S(2)}, u32[]{:S(2)}) collective-permute-start(bf16[4,64,2048]{2,1,0:T(8,128)(2,1)} %all-to-all-done.mine), channel_id=1, source_target_pairs={{1,0},{0,1},{3,2},{2,3},{5,4},{4,5},{7,6},{6,7},{9,8},{8,9},{11,10... | collective-permute-start | bytes 3145736 | tf_op jit(solution)/shard_map/ppermute | solution.py:219
  74.5 3.1 %collective-permute-start.1 = (bf16[32,512]{1,0:T(8,128)(2,1)S(1)}, bf16[32,512]{1,0:T(8,128)(2,1)S(1)}, u32[]{:S(2)}, u32[]{:S(2)}) collective-permute-start(bf16[32,512]{1,0:T(8,128)(2,1)S(1)} %shard_map.100), channel_id=1, source_target_pairs={{1,0},{0,1},{3,2},{2,3},{5,4},{4,5},{7,6},{6,7},{9,8},{8,9},{11,10... | collective-permute-start | bytes 98312 | tf_op jit(solution)/shard_map/ppermute | solution.py:219
  77.6 7.2 %collective-permute-start.2 = (bf16[64,512]{1,0:T(8,128)(2,1)S(1)}, bf16[64,512]{1,0:T(8,128)(2,1)S(1)}, u32[]{:S(2)}, u32[]{:S(2)}) collective-permute-start(bf16[64,512]{1,0:T(8,128)(2,1)S(1)} %pad_maximum_fusion.1.refs_0_), channel_id=1, source_target_pairs={{2,0},{4,2},{6,4},{0,6},{3,1},{5,3},{7,5},{1,7},{10,8},{12,10},{14... | collective-permute-start | bytes 196616 | tf_op jit(solution)/shard_map/ppermute | solution.py:219
  79.5 6.9 %collective-permute-start.3 = (bf16[64,512]{1,0:T(8,128)(2,1)S(1)}, bf16[64,512]{1,0:T(8,128)(2,1)S(1)}, u32[]{:S(2)}, u32[]{:S(2)}) collective-permute-start(bf16[64,512]{1,0:T(8,128)(2,1)S(1)} %pad_maximum_fusion.1.refs_0_), channel_id=1, source_target_pairs={{4,0},{6,2},{0,4},{2,6},{5,1},{7,3},{1,5},{3,7},{12,8},{14,10},{8,... | collective-permute-start | bytes 196616 | tf_op jit(solution)/shard_map/ppermute | solution.py:219
  82.6 6.7 %collective-permute-start.4 = (bf16[64,512]{1,0:T(8,128)(2,1)S(1)}, bf16[64,512]{1,0:T(8,128)(2,1)S(1)}, u32[]{:S(2)}, u32[]{:S(2)}) collective-permute-start(bf16[64,512]{1,0:T(8,128)(2,1)S(1)} %pad_maximum_fusion.1.refs_0_), channel_id=1, source_target_pairs={{6,0},{0,2},{2,4},{4,6},{7,1},{1,3},{3,5},{5,7},{14,8},{8,10},{10,... | collective-permute-start | bytes 196616 | tf_op jit(solution)/shard_map/ppermute | solution.py:219
  97.8 0.7 copy-start.4
  98.6 14.9 %all-to-all-start.2 = ((bf16[8,32,640]{2,1,0:T(8,128)(2,1)}), bf16[8,32,640]{2,1,0:T(8,128)(2,1)S(1)}, u32[]{:S(2)}, u32[]{:S(2)}) async-start(bf16[8,32,640]{2,1,0:T(8,128)(2,1)} %bitcast.25), calls=%async_computation.2 | async-start | bytes 655360 | tf_op jit(solution)/shard_map/all_to_all | solution.py:282
  113.5 0.9 copy-start.3

commit v2 on v1

--- a/solution.py
+++ b/solution.py
@@ -62,14 +62,13 @@
         out[layer, :, width:] = dot(normed, value_weight[layer]).astype(BF16)
 
 
-def project(normed, mine, other, row, head, place, turned=True):
+def project(normed, mine, other, row, head, place):
     x, core = place[0], place[1]
     model = normed.shape[1]
     own = jnp.concatenate(head_norm(dot_t(normed, mine.reshape(-1, model)), row, head), axis=1)
     far = jnp.concatenate(head_norm(dot_t(normed, other.reshape(-1, model)), row, head), axis=1)
-    if turned:
-        own = pltpu.roll(own, x * head, 1)
-        far = pltpu.roll(far, x * head, 1)
+    own = pltpu.roll(own, x * head, 1)
+    far = pltpu.roll(far, x * head, 1)
     return jnp.where(core == 0, own, far), jnp.where(core == 0, far, own)
 
 
@@ -84,7 +83,7 @@
     value = target[...].astype(F32)
     normed = (value * rms(value) * gain[layer : layer + 1, :]).astype(BF16)
     row = doubled(query_gain[layer : layer + 1, :])
-    store_groups(out, project(normed, mine[...], other[...], row, head, place, turned=False))
+    store_groups(out, project(normed, mine[...], other[...], row, head, place))
 
 
 def attended_halves(arrived, heads, head):
@@ -191,7 +190,7 @@
     return pl.BlockSpec((value.shape[0], size, value.shape[2]), lambda i, k=k: (0, k, 0))
 
 
-def with_place(kernel, shapes, operands, parts, flops, scratch=()):
+def with_place(kernel, shapes, operands, parts, flops, scratch=(), limit=40):
     one = not isinstance(shapes, (list, tuple))
     place, *rest = operands
     placed = [] if place is None else [place]
@@ -204,7 +203,7 @@
         in_specs=specs,
         out_specs=whole(shapes) if one else [whole(shape) for shape in shapes],
         scratch_shapes=list(scratch),
-        compiler_params=pltpu.CompilerParams(vmem_limit_bytes=40 * 1024 * 1024),
+        compiler_params=pltpu.CompilerParams(vmem_limit_bytes=limit * 1024 * 1024),
         cost_estimate=pl.CostEstimate(flops=flops, bytes_accessed=1000000, transcendentals=0),
     )(*placed, *rest, *(part[0] for part in parts))
 
@@ -244,6 +243,7 @@
         (None, source, source_gain, key_gain, key_weight, value_weight),
         [],
         200000000,
+        limit=63,
     )
     plane = to_all(pairs, ROWS)
     keys = plane.shape[0] * rows
@@ -251,7 +251,8 @@
     def both(stacked):
         return stacked, shifted(stacked, "c", 1)
 
-    first = both(to_all(query_t[0], "x"))
+    beside = [query_t[0]] + [shifted(query_t[0], "x", k) for k in range(1, lax.axis_size("x"))]
+    first = both(jnp.stack(beside))
     rest = both(around(jnp.concatenate([out_weight[0], query_t[1], out_weight[1]], axis=0)))
     rest = [[(part, k, head) for part in rest] for k in range(3)]
 
@@ -268,7 +269,7 @@
     hidden = target
     for layer in range(layers):
         partial = with_place(
-            functools.partial(attention_kernel, heads, head, 256, len(everyone)),
+            functools.partial(attention_kernel, heads, head, 512, len(everyone)),
             shapes((group, wide), BF16),
             (place, *everyone),
             [(plane, layer, 1)],

time: 151 us -> 160 us (1.060)
  waiting for transfers between devices: 25.7 us -> 35.5 us
  starting transfers between devices: 63.6 us -> 58.9 us
  local copies, waits for them, and re-layouts: 12.3 us -> 14.4 us
    ppermute x10 -> x13, waiting for transfers between devices: 16.9 us -> 28.4 us  [shifted(): lax.ppermute(value, axis, [((k + step) % size, k) for k in range(size)])]
    all_to_all x2 -> x1, starting transfers between devices: 26.3 us -> 16.6 us  [to_all(): return lax.all_to_all(copies, axis, split_axis=0, concat_axis=0, tiled=True)]
    ppermute x10 -> x13, starting transfers between devices: 29.4 us -> 37.3 us  [shifted(): lax.ppermute(value, axis, [((k + step) % size, k) for k in range(size)])]
    all_to_all x1, starting transfers between devices: 7.8 us -> 5.11 us  [decoder(): lax.all_to_all(partial.reshape(-1, rows, wide), TP, split_axis=0, concat_...]
    all_to_all x2 -> x1, waiting for transfers between devices: 1.71 us -> 0.01 us  [to_all(): return lax.all_to_all(copies, axis, split_axis=0, concat_axis=0, tiled=True)]
    unnamed x28 -> x20, local copies, waits for them, and re-layouts: 4.9 us -> 5.82 us
  transfers between devices with their start and end apart: 13 -> 15, of which waited for: 8 -> 10; matrix products, arithmetic and copies ran while one was open for 6% -> 7% of each run, Pallas kernels for 8% -> 8%
where the time goes in v2:
time: 160 us; the launch traced here: 158 us
  starting transfers between devices  58.9 us (37%)
  waiting for transfers between devices  35.5 us (22%)
  Pallas kernels  26.2 us (16%)
  blocking collectives  20.9 us (13%)
  local copies, waits for them, and re-layouts  14.4 us (9%)
  other arithmetic  2.24 us (1%)
    ppermute x13, starting transfers between devices, shifted(): lax.ppermute(value, axis, [((k + step) % size, k) for k in range(size)])  37.3 us
    ppermute x13, waiting for transfers between devices, shifted(): lax.ppermute(value, axis, [((k + step) % size, k) for k in range(size)])  28.4 us
    pallas_call x6, Pallas kernels, with_place(): pl.pallas_call(kernel, grid=(1,), out_shape=shapes, in_specs=specs, out_s...  26.2 us
    all_to_all x1, starting transfers between devices, to_all(): return lax.all_to_all(copies, axis, split_axis=0, concat_axis=0, tiled=True)  16.6 us
    all_to_all x1, blocking collectives, decoder(): lax.all_to_all(partial.reshape(-1, rows, wide), TP, split_axis=0, concat_...  10.9 us
    all_to_all x1, blocking collectives, to_all(): return lax.all_to_all(copies, axis, split_axis=0, concat_axis=0, tiled=True)  10 us
    all_to_all x1, waiting for transfers between devices, decoder(): lax.all_to_all(partial.reshape(-1, rows, wide), TP, split_axis=0, concat_...  7.11 us
    unnamed x20, local copies, waits for them, and re-layouts  5.82 us
  transfers between devices with their start and end apart: 15, of which 10 were waited for; matrix products, arithmetic and copies ran while one was open for 7% of the time, Pallas kernels for 8%

profile of v2, /device:TPU:1, one launch (start us, length us, event | category | flops | bytes accessed | tf_op | source)
XLA Modules:
  0.0 158.4 jit_solution(3882412665431339890)
XLA Ops:
  0.0 1.9 %slice_bitcast_fusion = (bf16[64,2048]{1,0:T(8,128)(2,1)S(1)}, bf16[64,2048]{1,0:T(8,128)(2,1)}, bf16[1,64,2048]{2,1,0:T(8,128)(2,1)}) fusion(bf16[2,64,2048]{2,1,0:T(8,128)(2,1)} %bitcast.31), kind=kLoop, calls=%fused_computation.2 | loop fusion | bytes 1310720 | tf_op jit(solution)/shard_map/squeeze | solution.py:256
  1.9 1.1 slice_bitcast_fusion.2
  3.0 0.9 pad_maximum_fusion.1
  3.9 5.2 %collective-permute-start.8 = (bf16[192,2048]{1,0:T(8,128)(2,1)}, bf16[192,2048]{1,0:T(8,128)(2,1)}, u32[]{:S(2)}, u32[]{:S(2)}) collective-permute-start(bf16[192,2048]{1,0:T(8,128)(2,1)} %pad_maximum_fusion.1), channel_id=1, source_target_pairs={{2,0},{4,2},{6,4},{0,6},{3,1},{5,3},{7,5},{1,7},{10,8},{12,10},{14... | collective-permute-start | bytes 2359304 | tf_op jit(solution)/shard_map/ppermute | solution.py:218
  9.1 1.9 %collective-permute-start.10 = (bf16[192,2048]{1,0:T(8,128)(2,1)}, bf16[192,2048]{1,0:T(8,128)(2,1)}, u32[]{:S(2)}, u32[]{:S(2)}) collective-permute-start(bf16[192,2048]{1,0:T(8,128)(2,1)} %pad_maximum_fusion.1), channel_id=1, source_target_pairs={{6,0},{0,2},{2,4},{4,6},{7,1},{1,3},{3,5},{5,7},{14,8},{8,10},{10,... | collective-permute-start | bytes 2359304 | tf_op jit(solution)/shard_map/ppermute | solution.py:218
  11.1 2.8 %shard_map.101 = bf16[2,32,256]{2,1,0:T(8,128)(2,1)} custom-call(bf16[32,2048]{1,0:T(8,128)(2,1)} %source.1, f32[2,2048]{1,0:T(2,128)} %gain.4, f32[2,64]{1,0:T(2,128)} %key_gain.1, bf16[2,2048,128]{2,1,0:T(8,128)(2,1)} %key_weight.1, bf16[2,2048,128]{2,1,0:T(8,128)(2,1)} %value_weight.1), custom_call_target="tpu_custom_call" | custom-call | flops 200000000 | bytes 1000000 | tf_op jit(solution)/shard_map/pallas_call | solution.py:199
  13.8 2.3 %broadcast_in_dim.6 = bf16[64,2,32,256]{3,2,1,0:T(8,128)(2,1)} broadcast(bf16[2,32,256]{2,1,0:T(8,128)(2,1)} %shard_map.101), dimensions={1,2,3} | broadcast | bytes 2129920 | tf_op jit(solution)/shard_map/broadcast_in_dim | solution.py:212
  16.2 16.6 %all-to-all-start = ((bf16[64,2,32,256]{3,2,1,0:T(8,128)(2,1)}), bf16[64,2,32,256]{3,2,1,0:T(8,128)(2,1)}, u32[]{:S(2)}, u32[]{:S(2)}) async-start(bf16[64,2,32,256]{3,2,1,0:T(8,128)(2,1)} %broadcast_in_dim.6), calls=%async_computation | async-start | bytes 4194304 | tf_op jit(solution)/shard_map/all_to_all | solution.py:213
  32.8 1.0 constant_dynamic-update-slice_fusion.6
  33.7 1.0 constant_dynamic-update-slice_fusion.5
  34.7 1.0 slice.29
  35.8 4.7 %collective-permute-start.9 = (bf16[96,2048]{1,0:T(8,128)(2,1)S(1)}, bf16[96,2048]{1,0:T(8,128)(2,1)S(1)}, u32[]{:S(2)}, u32[]{:S(2)}) collective-permute-start(bf16[96,2048]{1,0:T(8,128)(2,1)S(1)} %slice.29), channel_id=1, source_target_pairs={{2,0},{4,2},{6,4},{0,6},{3,1},{5,3},{7,5},{1,7},{10,8},{12,10},{14... | collective-permute-start | bytes 1179656 | tf_op jit(solution)/shard_map/ppermute | solution.py:218
  40.5 1.0 constant_dynamic-update-slice_fusion.4
  41.5 1.0 slice.30
  42.5 2.1 %collective-permute-start.11 = (bf16[96,2048]{1,0:T(8,128)(2,1)S(1)}, bf16[96,2048]{1,0:T(8,128)(2,1)S(1)}, u32[]{:S(2)}, u32[]{:S(2)}) collective-permute-start(bf16[96,2048]{1,0:T(8,128)(2,1)S(1)} %slice.30), channel_id=1, source_target_pairs={{6,0},{0,2},{2,4},{4,6},{7,1},{1,3},{3,5},{5,7},{14,8},{8,10},{10,... | collective-permute-start | bytes 1179656 | tf_op jit(solution)/shard_map/ppermute | solution.py:218
  44.6 1.2 constant_dynamic-update-slice_fusion.3
  45.8 1.6 %collective-permute-done.9 = bf16[96,2048]{1,0:T(8,128)(2,1)S(1)} collective-permute-done((bf16[96,2048]{1,0:T(8,128)(2,1)S(1)}, bf16[96,2048]{1,0:T(8,128)(2,1)S(1)}, u32[]{:S(2)}, u32[]{:S(2)}) %collective-permute-start.9) | collective-permute-done | bytes 393248 | tf_op jit(solution)/shard_map/ppermute | solution.py:218
  47.4 7.3 %collective-permute-done.11 = bf16[96,2048]{1,0:T(8,128)(2,1)S(1)} collective-permute-done((bf16[96,2048]{1,0:T(8,128)(2,1)S(1)}, bf16[96,2048]{1,0:T(8,128)(2,1)S(1)}, u32[]{:S(2)}, u32[]{:S(2)}) %collective-permute-start.11) | collective-permute-done | bytes 393248 | tf_op jit(solution)/shard_map/ppermute | solution.py:218
  54.8 1.2 constant_dynamic-update-slice_fusion
  56.0 4.5 %collective-permute-start.12 = (bf16[4,192,2048]{2,1,0:T(8,128)(2,1)S(1)}, bf16[4,192,2048]{2,1,0:T(8,128)(2,1)}, u32[]{:S(2)}, u32[]{:S(2)}) collective-permute-start(bf16[4,192,2048]{2,1,0:T(8,128)(2,1)S(1)} %bitcast.24), channel_id=1, source_target_pairs={{1,0},{0,1},{3,2},{2,3},{5,4},{4,5},{7,6},{6,7},{9,8},{8,9},{11,10... | collective-permute-start | bytes 9437192 | tf_op jit(solution)/shard_map/ppermute | solution.py:218
  60.4 1.9 %collective-permute-start = (bf16[64,2048]{1,0:T(8,128)(2,1)S(1)}, bf16[64,2048]{1,0:T(8,128)(2,1)S(1)}, u32[]{:S(2)}, u32[]{:S(2)}) collective-permute-start(bf16[64,2048]{1,0:T(8,128)(2,1)S(1)} %copy-done.6), channel_id=1, source_target_pairs={{2,0},{4,2},{6,4},{0,6},{3,1},{5,3},{7,5},{1,7},{10,8},{12,10},{14... | collective-permute-start | bytes 786440 | tf_op jit(solution)/shard_map/ppermute | solution.py:218
  62.4 2.5 %collective-permute-start.1 = (bf16[64,2048]{1,0:T(8,128)(2,1)S(1)}, bf16[64,2048]{1,0:T(8,128)(2,1)S(1)}, u32[]{:S(2)}, u32[]{:S(2)}) collective-permute-start(bf16[64,2048]{1,0:T(8,128)(2,1)S(1)} %copy-done.6), channel_id=1, source_target_pairs={{4,0},{6,2},{0,4},{2,6},{5,1},{7,3},{1,5},{3,7},{12,8},{14,10},{8,... | collective-permute-start | bytes 786440 | tf_op jit(solution)/shard_map/ppermute | solution.py:218
  64.8 2.8 %collective-permute-start.2 = (bf16[64,2048]{1,0:T(8,128)(2,1)S(1)}, bf16[64,2048]{1,0:T(8,128)(2,1)S(1)}, u32[]{:S(2)}, u32[]{:S(2)}) collective-permute-start(bf16[64,2048]{1,0:T(8,128)(2,1)S(1)} %copy-done.6), channel_id=1, source_target_pairs={{6,0},{0,2},{2,4},{4,6},{7,1},{1,3},{3,5},{5,7},{14,8},{8,10},{10,... | collective-permute-start | bytes 786440 | tf_op jit(solution)/shard_map/ppermute | solution.py:218
  67.7 2.6 %collective-permute-done = bf16[64,2048]{1,0:T(8,128)(2,1)S(1)} collective-permute-done((bf16[64,2048]{1,0:T(8,128)(2,1)S(1)}, bf16[64,2048]{1,0:T(8,128)(2,1)S(1)}, u32[]{:S(2)}, u32[]{:S(2)}) %collective-permute-start) | collective-permute-done | bytes 262176 | tf_op jit(solution)/shard_map/ppermute | solution.py:218
  70.3 3.5 %collective-permute-done.1 = bf16[64,2048]{1,0:T(8,128)(2,1)S(1)} collective-permute-done((bf16[64,2048]{1,0:T(8,128)(2,1)S(1)}, bf16[64,2048]{1,0:T(8,128)(2,1)S(1)}, u32[]{:S(2)}, u32[]{:S(2)}) %collective-permute-start.1) | collective-permute-done | bytes 262176 | tf_op jit(solution)/shard_map/ppermute | solution.py:218
  73.8 6.0 %collective-permute-done.2 = bf16[64,2048]{1,0:T(8,128)(2,1)S(1)} collective-permute-done((bf16[64,2048]{1,0:T(8,128)(2,1)S(1)}, bf16[64,2048]{1,0:T(8,128)(2,1)S(1)}, u32[]{:S(2)}, u32[]{:S(2)}) %collective-permute-start.2) | collective-permute-done | bytes 262176 | tf_op jit(solution)/shard_map/ppermute | solution.py:218
  79.7 1.2 pad_maximum_fusion.mine
  80.9 2.3 %collective-permute-start.3 = (bf16[4,64,2048]{2,1,0:T(8,128)(2,1)}, bf16[4,64,2048]{2,1,0:T(8,128)(2,1)}, u32[]{:S(2)}, u32[]{:S(2)}) collective-permute-start(bf16[4,64,2048]{2,1,0:T(8,128)(2,1)} %pad_maximum_fusion.mine), channel_id=1, source_target_pairs={{1,0},{0,1},{3,2},{2,3},{5,4},{4,5},{7,6},{6,7},{9,8},{8,9},{11,10... | collective-permute-start | bytes 3145736 | tf_op jit(solution)/shard_map/ppermute | solution.py:218
  83.2 0.1 pad_add_fusion.place
  83.3 2.5 %collective-permute-done.3.other = bf16[4,64,2048]{2,1,0:T(8,128)(2,1)} collective-permute-done((bf16[4,64,2048]{2,1,0:T(8,128)(2,1)}, bf16[4,64,2048]{2,1,0:T(8,128)(2,1)}, u32[]{:S(2)}, u32[]{:S(2)}) %collective-permute-start.3) | collective-permute-done | bytes 1048608 | tf_op jit(solution)/shard_map/ppermute | solution.py:218
  85.8 2.5 %shard_map.100 = bf16[32,512]{1,0:T(8,128)(2,1)S(1)} custom-call(s32[2]{0:T(128)S(1)} %pad_add_fusion.place, bf16[32,2048]{1,0:T(8,128)(2,1)S(1)} %copy-done, f32[2,2048]{1,0:T(2,128)S(1)} %copy-done.3, f32[2,64]{1,0:T(2,128)S(1)} %copy-done.4, bf16[4,64,2048]{2,1,0:T(8,128)(2,1)} %pad_maximum_fusion.mine, bf16[4,64,2048]{2,1,0:T(8,128)(2,1)} %collective-permute-done.3.other), custom_call_target="tpu_custom_call" | custom-call | flops 200000000 | bytes 1000000 | tf_op jit(solution)/shard_map/pallas_call | solution.py:199
  88.3 2.3 %collective-permute-start.4 = (bf16[32,512]{1,0:T(8,128)(2,1)S(1)}, bf16[32,512]{1,0:T(8,128)(2,1)S(1)}, u32[]{:S(2)}, u32[]{:S(2)}) collective-permute-start(bf16[32,512]{1,0:T(8,128)(2,1)S(1)} %shard_map.100), channel_id=1, source_target_pairs={{1,0},{0,1},{3,2},{2,3},{5,4},{4,5},{7,6},{6,7},{9,8},{8,9},{11,10... | collective-permute-start | bytes 98312 | tf_op jit(solution)/shard_map/ppermute | solution.py:218
  90.6 0.8 collective-permute-done.4
  91.5 2.2 %collective-permute-start.5 = (bf16[64,512]{1,0:T(8,128)(2,1)S(1)}, bf16[64,512]{1,0:T(8,128)(2,1)S(1)}, u32[]{:S(2)}, u32[]{:S(2)}) collective-permute-start(bf16[64,512]{1,0:T(8,128)(2,1)S(1)} %pad_maximum_fusion.2.refs_0_), channel_id=1, source_target_pairs={{2,0},{4,2},{6,4},{0,6},{3,1},{5,3},{7,5},{1,7},{10,8},{12,10},{14... | collective-permute-start | bytes 196616 | tf_op jit(solution)/shard_map/ppermute | solution.py:218
  93.7 2.5 %collective-permute-start.6 = (bf16[64,512]{1,0:T(8,128)(2,1)S(1)}, bf16[64,512]{1,0:T(8,128)(2,1)S(1)}, u32[]{:S(2)}, u32[]{:S(2)}) collective-permute-start(bf16[64,512]{1,0:T(8,128)(2,1)S(1)} %pad_maximum_fusion.2.refs_0_), channel_id=1, source_target_pairs={{4,0},{6,2},{0,4},{2,6},{5,1},{7,3},{1,5},{3,7},{12,8},{14,10},{8,... | collective-permute-start | bytes 196616 | tf_op jit(solution)/shard_map/ppermute | solution.py:218
  96.2 2.5 %collective-permute-start.7 = (bf16[64,512]{1,0:T(8,128)(2,1)S(1)}, bf16[64,512]{1,0:T(8,128)(2,1)S(1)}, u32[]{:S(2)}, u32[]{:S(2)}) collective-permute-start(bf16[64,512]{1,0:T(8,128)(2,1)S(1)} %pad_maximum_fusion.2.refs_0_), channel_id=1, source_target_pairs={{6,0},{0,2},{2,4},{4,6},{7,1},{1,3},{3,5},{5,7},{14,8},{8,10},{10,... | collective-permute-start | bytes 196616 | tf_op jit(solution)/shard_map/ppermute | solution.py:218
  98.7 1.5 collective-permute-done.6.refs_2_
  100.2 2.5 %collective-permute-done.7.refs_3_ = bf16[64,512]{1,0:T(8,128)(2,1)S(1)} collective-permute-done((bf16[64,512]{1,0:T(8,128)(2,1)S(1)}, bf16[64,512]{1,0:T(8,128)(2,1)S(1)}, u32[]{:S(2)}, u32[]{:S(2)}) %collective-permute-start.7) | collective-permute-done | bytes 65568 | tf_op jit(solution)/shard_map/ppermute | solution.py:218
  102.7 7.5 %shard_map.102 = bf16[256,640]{1,0:T(8,128)(2,1)S(1)} custom-call(s32[2]{0:T(128)S(1)} %pad_add_fusion.place, bf16[64,512]{1,0:T(8,128)(2,1)S(1)} %pad_maximum_fusion.2.refs_0_, bf16[64,512]{1,0:T(8,128)(2,1)S(1)} %collective-permute-done.5.refs_1_, bf16[64,512]{1,0:T(8,128)(2,1)S(1)} %collective-permute-done.6.refs_2_, ...), custom_call_target="tpu_custom_call" | custom-call | flops 5000000000 | bytes 1000000 | tf_op jit(solution)/shard_map/pallas_call | solution.py:199
  110.3 0.7 copy-done.2
  111.0 5.1 %all-to-all-start.1 = ((bf16[8,32,640]{2,1,0:T(8,128)(2,1)}), bf16[8,32,640]{2,1,0:T(8,128)(2,1)S(1)}, u32[]{:S(2)}, u32[]{:S(2)}) async-start(bf16[8,32,640]{2,1,0:T(8,128)(2,1)} %bitcast.28), calls=%async_computation.1 | async-start | bytes 655360 | tf_op jit(solution)/shard_map/all_to_all | solution.py:283
  116.1 7.1 %all-to-all-done.1.arrived = bf16[8,32,640]{2,1,0:T(8,128)(2,1)S(1)} async-done(((bf16[8,32,640]{2,1,0:T(8,128)(2,1)}), bf16[8,32,640]{2,1,0:T(8,128)(2,1)S(1)}, u32[]{:S(2)}, u32[]{:S(2)}) %all-to-all-start.1) | async-done | bytes 327712 | tf_op jit(solution)/shard_map/all_to_all | solution.py:283
  123.2 0.9 copy-done.1
  124.1 3.2 %shard_map.103 = (bf16[32,2048]{1,0:T(8,128)(2,1)S(1)}, bf16[32,512]{1,0:T(8,128)(2,1)S(1)}) custom-call(s32[2]{0:T(128)S(1)} %pad_add_fusion.place, bf16[8,32,640]{2,1,0:T(8,128)(2,1)S(1)} %all-to-all-done.1.arrived, bf16[32,2048]{1,0:T(8,128)(2,1)S(1)} %copy-done.1, f32[2,2048]{1,0:T(2,128)S(1)} %copy-done.3, f32[2,64]{1,0:T(2,128)S(1)} %copy-done.4, ...), custom_call_target="tpu_custom_call" | custom-call | flops 400000000 | bytes 1000000 | tf_op jit(solution)/shard_map/pallas_call | solution.py:199
  127.4 10.0 %all_to_all.20 = bf16[8,32,512]{2,1,0:T(8,128)(2,1)S(1)} all-to-all(bf16[8,32,512]{2,1,0:T(8,128)(2,1)S(1)} %broadcast_in_dim.7), channel_id=1, replica_groups=mesh['z'=8,'y'=8,'x'=4,'c'=2] {'x','c'}, dimensions={0} | all-to-all | bytes 524288 | tf_op jit(solution)/shard_map/all_to_all | solution.py:213
  137.4 7.5 %shard_map.104 = bf16[256,640]{1,0:T(8,128)(2,1)S(1)} custom-call(s32[2]{0:T(128)S(1)} %pad_add_fusion.place, bf16[256,512]{1,0:T(8,128)(2,1)S(1)} %bitcast.30, bf16[64,2,32,256]{3,2,1,0:T(8,128)(2,1)} %all-to-all-done.refs_4_.refs_1_), custom_call_target="tpu_custom_call" | custom-call | flops 5000000000 | bytes 1000000 | tf_op jit(solution)/shard_map/pallas_call | solution.py:199
  144.9 10.9 %all_to_all.21.arrived = bf16[8,32,640]{2,1,0:T(8,128)(2,1)S(1)} all-to-all(bf16[8,32,640]{2,1,0:T(8,128)(2,1)S(1)} %bitcast.29), channel_id=1, replica_groups=mesh['z'=8,'y'=8,'x'=4,'c'=2] {'x','c'}, dimensions={0} | all-to-all | bytes 655360 | tf_op jit(solution)/shard_map/all_to_all | solution.py:283
  155.8 2.6 %shard_map.105 = bf16[32,2048]{1,0:T(8,128)(2,1)} custom-call(s32[2]{0:T(128)S(1)} %pad_add_fusion.place, bf16[8,32,640]{2,1,0:T(8,128)(2,1)S(1)} %all_to_all.21.arrived, bf16[32,2048]{1,0:T(8,128)(2,1)S(1)} %get-tuple-element.8.hidden, bf16[4,192,2048]{2,1,0:T(8,128)(2,1)S(1)} %bitcast.27, bf16[4,192,2048]{2,1,0:T(8,128)(2,1)} %collective-permute-done.12.out_other.other), custom_call_target="tpu_custom_call" | custom-call | flops 200000000 | bytes 1000000 | tf_op jit(solution)/shard_map/pallas_call | solution.py:199
  (21 shorter events, 0.1 us)
Async XLA Ops:
  3.9 30.8 %collective-permute-start.8 = (bf16[192,2048]{1,0:T(8,128)(2,1)}, bf16[192,2048]{1,0:T(8,128)(2,1)}, u32[]{:S(2)}, u32[]{:S(2)}) collective-permute-start(bf16[192,2048]{1,0:T(8,128)(2,1)} %pad_maximum_fusion.1), channel_id=1, source_target_pairs={{2,0},{4,2},{6,4},{0,6},{3,1},{5,3},{7,5},{1,7},{10,8},{12,10},{14... | collective-permute-start | bytes 2359304 | tf_op jit(solution)/shard_map/ppermute | solution.py:218
  9.1 32.3 %collective-permute-start.10 = (bf16[192,2048]{1,0:T(8,128)(2,1)}, bf16[192,2048]{1,0:T(8,128)(2,1)}, u32[]{:S(2)}, u32[]{:S(2)}) collective-permute-start(bf16[192,2048]{1,0:T(8,128)(2,1)} %pad_maximum_fusion.1), channel_id=1, source_target_pairs={{6,0},{0,2},{2,4},{4,6},{7,1},{1,3},{3,5},{5,7},{14,8},{8,10},{10,... | collective-permute-start | bytes 2359304 | tf_op jit(solution)/shard_map/ppermute | solution.py:218
  16.2 86.5 %all-to-all-start = ((bf16[64,2,32,256]{3,2,1,0:T(8,128)(2,1)}), bf16[64,2,32,256]{3,2,1,0:T(8,128)(2,1)}, u32[]{:S(2)}, u32[]{:S(2)}) async-start(bf16[64,2,32,256]{3,2,1,0:T(8,128)(2,1)} %broadcast_in_dim.6), calls=%async_computation | async-start | bytes 4194304 | tf_op jit(solution)/shard_map/all_to_all | solution.py:213
  35.7 24.7 %copy-start.6 = (bf16[64,2048]{1,0:T(8,128)(2,1)S(1)}, bf16[64,2048]{1,0:T(8,128)(2,1)}, u32[]{:S(2)}) copy-start(bf16[64,2048]{1,0:T(8,128)(2,1)} %get-tuple-element.12) | copy-start | bytes 786436
  35.7 44.0 %copy-start.5 = (bf16[1,64,2048]{2,1,0:T(8,128)(2,1)S(1)}, bf16[1,64,2048]{2,1,0:T(8,128)(2,1)}, u32[]{:S(2)}) copy-start(bf16[1,64,2048]{2,1,0:T(8,128)(2,1)} %get-tuple-element.13) | copy-start | bytes 786436
  35.8 11.6 %collective-permute-start.9 = (bf16[96,2048]{1,0:T(8,128)(2,1)S(1)}, bf16[96,2048]{1,0:T(8,128)(2,1)S(1)}, u32[]{:S(2)}, u32[]{:S(2)}) collective-permute-start(bf16[96,2048]{1,0:T(8,128)(2,1)S(1)} %slice.29), channel_id=1, source_target_pairs={{2,0},{4,2},{6,4},{0,6},{3,1},{5,3},{7,5},{1,7},{10,8},{12,10},{14... | collective-permute-start | bytes 1179656 | tf_op jit(solution)/shard_map/ppermute | solution.py:218
  42.5 43.4 %copy-start = (bf16[32,2048]{1,0:T(8,128)(2,1)S(1)}, bf16[32,2048]{1,0:T(8,128)(2,1)}, u32[]{:S(2)}) copy-start(bf16[32,2048]{1,0:T(8,128)(2,1)} %hidden.1) | copy-start | bytes 393220
  42.5 43.3 %copy-start.3 = (f32[2,2048]{1,0:T(2,128)S(1)}, f32[2,2048]{1,0:T(2,128)}, u32[]{:S(2)}) copy-start(f32[2,2048]{1,0:T(2,128)} %gain.5) | copy-start | bytes 49156
  42.5 43.3 %copy-start.4 = (f32[2,64]{1,0:T(2,128)S(1)}, f32[2,64]{1,0:T(2,128)}, u32[]{:S(2)}) copy-start(f32[2,64]{1,0:T(2,128)} %query_gain.3) | copy-start | bytes 1540
  42.5 12.2 %collective-permute-start.11 = (bf16[96,2048]{1,0:T(8,128)(2,1)S(1)}, bf16[96,2048]{1,0:T(8,128)(2,1)S(1)}, u32[]{:S(2)}, u32[]{:S(2)}) collective-permute-start(bf16[96,2048]{1,0:T(8,128)(2,1)S(1)} %slice.30), channel_id=1, source_target_pairs={{6,0},{0,2},{2,4},{4,6},{7,1},{1,3},{3,5},{5,7},{14,8},{8,10},{10,... | collective-permute-start | bytes 1179656 | tf_op jit(solution)/shard_map/ppermute | solution.py:218
  56.0 60.1 %collective-permute-start.12 = (bf16[4,192,2048]{2,1,0:T(8,128)(2,1)S(1)}, bf16[4,192,2048]{2,1,0:T(8,128)(2,1)}, u32[]{:S(2)}, u32[]{:S(2)}) collective-permute-start(bf16[4,192,2048]{2,1,0:T(8,128)(2,1)S(1)} %bitcast.24), channel_id=1, source_target_pairs={{1,0},{0,1},{3,2},{2,3},{5,4},{4,5},{7,6},{6,7},{9,8},{8,9},{11,10... | collective-permute-start | bytes 9437192 | tf_op jit(solution)/shard_map/ppermute | solution.py:218
  60.4 9.8 %collective-permute-start = (bf16[64,2048]{1,0:T(8,128)(2,1)S(1)}, bf16[64,2048]{1,0:T(8,128)(2,1)S(1)}, u32[]{:S(2)}, u32[]{:S(2)}) collective-permute-start(bf16[64,2048]{1,0:T(8,128)(2,1)S(1)} %copy-done.6), channel_id=1, source_target_pairs={{2,0},{4,2},{6,4},{0,6},{3,1},{5,3},{7,5},{1,7},{10,8},{12,10},{14... | collective-permute-start | bytes 786440 | tf_op jit(solution)/shard_map/ppermute | solution.py:218
  62.4 11.4 %collective-permute-start.1 = (bf16[64,2048]{1,0:T(8,128)(2,1)S(1)}, bf16[64,2048]{1,0:T(8,128)(2,1)S(1)}, u32[]{:S(2)}, u32[]{:S(2)}) collective-permute-start(bf16[64,2048]{1,0:T(8,128)(2,1)S(1)} %copy-done.6), channel_id=1, source_target_pairs={{4,0},{6,2},{0,4},{2,6},{5,1},{7,3},{1,5},{3,7},{12,8},{14,10},{8,... | collective-permute-start | bytes 786440 | tf_op jit(solution)/shard_map/ppermute | solution.py:218
  64.8 14.9 %collective-permute-start.2 = (bf16[64,2048]{1,0:T(8,128)(2,1)S(1)}, bf16[64,2048]{1,0:T(8,128)(2,1)S(1)}, u32[]{:S(2)}, u32[]{:S(2)}) collective-permute-start(bf16[64,2048]{1,0:T(8,128)(2,1)S(1)} %copy-done.6), channel_id=1, source_target_pairs={{6,0},{0,2},{2,4},{4,6},{7,1},{1,3},{3,5},{5,7},{14,8},{8,10},{10,... | collective-permute-start | bytes 786440 | tf_op jit(solution)/shard_map/ppermute | solution.py:218
  80.9 4.9 %collective-permute-start.3 = (bf16[4,64,2048]{2,1,0:T(8,128)(2,1)}, bf16[4,64,2048]{2,1,0:T(8,128)(2,1)}, u32[]{:S(2)}, u32[]{:S(2)}) collective-permute-start(bf16[4,64,2048]{2,1,0:T(8,128)(2,1)} %pad_maximum_fusion.mine), channel_id=1, source_target_pairs={{1,0},{0,1},{3,2},{2,3},{5,4},{4,5},{7,6},{6,7},{9,8},{8,9},{11,10... | collective-permute-start | bytes 3145736 | tf_op jit(solution)/shard_map/ppermute | solution.py:218
  88.3 3.1 %collective-permute-start.4 = (bf16[32,512]{1,0:T(8,128)(2,1)S(1)}, bf16[32,512]{1,0:T(8,128)(2,1)S(1)}, u32[]{:S(2)}, u32[]{:S(2)}) collective-permute-start(bf16[32,512]{1,0:T(8,128)(2,1)S(1)} %shard_map.100), channel_id=1, source_target_pairs={{1,0},{0,1},{3,2},{2,3},{5,4},{4,5},{7,6},{6,7},{9,8},{8,9},{11,10... | collective-permute-start | bytes 98312 | tf_op jit(solution)/shard_map/ppermute | solution.py:218
  91.5 7.2 %collective-permute-start.5 = (bf16[64,512]{1,0:T(8,128)(2,1)S(1)}, bf16[64,512]{1,0:T(8,128)(2,1)S(1)}, u32[]{:S(2)}, u32[]{:S(2)}) collective-permute-start(bf16[64,512]{1,0:T(8,128)(2,1)S(1)} %pad_maximum_fusion.2.refs_0_), channel_id=1, source_target_pairs={{2,0},{4,2},{6,4},{0,6},{3,1},{5,3},{7,5},{1,7},{10,8},{12,10},{14... | collective-permute-start | bytes 196616 | tf_op jit(solution)/shard_map/ppermute | solution.py:218
  93.7 6.5 %collective-permute-start.6 = (bf16[64,512]{1,0:T(8,128)(2,1)S(1)}, bf16[64,512]{1,0:T(8,128)(2,1)S(1)}, u32[]{:S(2)}, u32[]{:S(2)}) collective-permute-start(bf16[64,512]{1,0:T(8,128)(2,1)S(1)} %pad_maximum_fusion.2.refs_0_), channel_id=1, source_target_pairs={{4,0},{6,2},{0,4},{2,6},{5,1},{7,3},{1,5},{3,7},{12,8},{14,10},{8,... | collective-permute-start | bytes 196616 | tf_op jit(solution)/shard_map/ppermute | solution.py:218
  96.2 6.5 %collective-permute-start.7 = (bf16[64,512]{1,0:T(8,128)(2,1)S(1)}, bf16[64,512]{1,0:T(8,128)(2,1)S(1)}, u32[]{:S(2)}, u32[]{:S(2)}) collective-permute-start(bf16[64,512]{1,0:T(8,128)(2,1)S(1)} %pad_maximum_fusion.2.refs_0_), channel_id=1, source_target_pairs={{6,0},{0,2},{2,4},{4,6},{7,1},{1,3},{3,5},{5,7},{14,8},{8,10},{10,... | collective-permute-start | bytes 196616 | tf_op jit(solution)/shard_map/ppermute | solution.py:218
  110.2 0.7 copy-start.2
  111.0 12.2 %all-to-all-start.1 = ((bf16[8,32,640]{2,1,0:T(8,128)(2,1)}), bf16[8,32,640]{2,1,0:T(8,128)(2,1)S(1)}, u32[]{:S(2)}, u32[]{:S(2)}) async-start(bf16[8,32,640]{2,1,0:T(8,128)(2,1)} %bitcast.28), calls=%async_computation.1 | async-start | bytes 655360 | tf_op jit(solution)/shard_map/all_to_all | solution.py:283
  123.2 0.9 copy-start.1

commit v3 on v2

--- a/solution.py
+++ b/solution.py
@@ -78,9 +78,9 @@
         out[:, k * width : (k + 1) * width] = group.astype(BF16)
 
 
-def query_kernel(layer, place, target, gain, query_gain, mine, other, out):
+def query_kernel(layer, place, target, beside, gain, query_gain, mine, other, out):
     head = query_gain.shape[1]
-    value = target[...].astype(F32)
+    value = jnp.concatenate([target[...].astype(F32), beside[...].astype(F32)], axis=0)
     normed = (value * rms(value) * gain[layer : layer + 1, :]).astype(BF16)
     row = doubled(query_gain[layer : layer + 1, :])
     store_groups(out, project(normed, mine[...], other[...], row, head, place))
@@ -165,7 +165,7 @@
             gathered[pl.ds(heads * head + heads + p, 1), :] = mass - top
             return carry
 
-        lax.fori_loop(0, 2 * per, one_head, 0)
+        lax.fori_loop(0, 2 * per, one_head, 0, unroll=True)
     rest = heads * head + 2 * heads
     gathered[rest:, :] = jnp.zeros((gathered.shape[0] - rest, columns), F32)
     result = jnp.transpose(gathered[...]).astype(BF16)
@@ -222,7 +222,7 @@
     half = value.shape[0] // 2
     right, left = shifted(value, "x", 1), shifted(value, "x", -1)
     far = [shifted(right[:half], "x", 1), shifted(left[half:], "x", -1)]
-    return jnp.concatenate([value, right, *far, left], axis=0).reshape(4, *value.shape)
+    return [value, right, *far, left]
 
 
 def decoder(target, source, target_gain, source_gain, query_gain, key_gain, query_weight, key_weight, value_weight, out_weight):
@@ -253,17 +253,15 @@
 
     beside = [query_t[0]] + [shifted(query_t[0], "x", k) for k in range(1, lax.axis_size("x"))]
     first = both(jnp.stack(beside))
-    rest = both(around(jnp.concatenate([out_weight[0], query_t[1], out_weight[1]], axis=0)))
-    rest = [[(part, k, head) for part in rest] for k in range(3)]
-
-    queries = with_place(
+    pieces = around(jnp.concatenate([out_weight[0], query_t[1], out_weight[1]], axis=0))
+
+    chip = with_place(
         functools.partial(query_kernel, 0),
-        shapes((rows, width), BF16),
-        (place, target, target_gain, query_gain),
+        shapes((2 * rows, width), BF16),
+        (place, target, shifted(target, "c", 1), target_gain, query_gain),
         [(part, 0, head) for part in first],
         200000000,
     )
-    chip = jnp.concatenate([queries, shifted(queries, "c", 1)], axis=0)
     everyone = [chip] + [shifted(chip, "x", k) for k in range(1, lax.axis_size("x"))]
 
     hidden = target
@@ -280,6 +278,11 @@
                 pltpu.VMEM((wide, group), F32),
             ],
         )
+        if layer == 0:
+            pieces, _ = lax.optimization_barrier((pieces, partial))
+            right = jnp.concatenate(pieces[2:4], axis=0)
+            rest = both(jnp.stack([pieces[0], pieces[1], right, pieces[4]]))
+            rest = [[(part, k, head) for part in rest] for k in range(3)]
         arrived = lax.all_to_all(partial.reshape(-1, rows, wide), TP, split_axis=0, concat_axis=0, tiled=True)
         if layer + 1 < layers:
             hidden, queries = with_place(

time: 160 us -> 133 us (0.83)
  waiting for transfers between devices: 35.5 us -> 11.9 us
  blocking collectives: 20.9 us -> 32.4 us
  local copies, waits for them, and re-layouts: 14.4 us -> 4.55 us
  Pallas kernels: 26.2 us -> 18 us
  starting transfers between devices: 58.9 us -> 61.1 us
  other arithmetic: 2.24 us -> 4.14 us
    ppermute x13, waiting for transfers between devices: 28.4 us -> 11.9 us  [shifted(): lax.ppermute(value, axis, [((k + step) % size, k) for k in range(size)])]
    all_to_all x1 -> x2, blocking collectives: 10.9 us -> 22.8 us  [decoder(): lax.all_to_all(partial.reshape(-1, rows, wide), TP, split_axis=0, concat_...]
    pallas_call x6, Pallas kernels: 26.2 us -> 18 us  [with_place(): pl.pallas_call(kernel, grid=(1,), out_shape=shapes, in_specs=specs, out_s...]
    all_to_all x1 -> x0, waiting for transfers between devices: 7.11 us -> none  [decoder(): lax.all_to_all(partial.reshape(-1, rows, wide), TP, split_axis=0, concat_...]
    ppermute x13, starting transfers between devices: 37.3 us -> 43.9 us  [shifted(): lax.ppermute(value, axis, [((k + step) % size, k) for k in range(size)])]
    unnamed x20 -> x10, local copies, waits for them, and re-layouts: 5.82 us -> 0.02 us
    all_to_all x1 -> x0, starting transfers between devices: 5.11 us -> none  [decoder(): lax.all_to_all(partial.reshape(-1, rows, wide), TP, split_axis=0, concat_...]
    another operation x0 -> x2, other arithmetic: none -> 2.98 us  [decoder(): rest = both(jnp.stack([pieces[0], pieces[1], right, pieces[4]]))]
  transfers between devices with their start and end apart: 15 -> 14, of which waited for: 10 -> 6; matrix products, arithmetic and copies ran while one was open for 7% -> 3% of each run, Pallas kernels for 8% -> 5%
where the time goes in v3:
time: 133 us; the launch traced here: 132 us
  starting transfers between devices  61.1 us (46%)
  blocking collectives  32.4 us (24%)
  Pallas kernels  18 us (14%)
  waiting for transfers between devices  11.9 us (9%)
  local copies, waits for them, and re-layouts  4.55 us (3%)
  other arithmetic  4.14 us (3%)
    ppermute x13, starting transfers between devices, shifted(): lax.ppermute(value, axis, [((k + step) % size, k) for k in range(size)])  43.9 us
    all_to_all x2, blocking collectives, decoder(): lax.all_to_all(partial.reshape(-1, rows, wide), TP, split_axis=0, concat_...  22.8 us
    pallas_call x6, Pallas kernels, with_place(): pl.pallas_call(kernel, grid=(1,), out_shape=shapes, in_specs=specs, out_s...  18 us
    all_to_all x1, starting transfers between devices, to_all(): return lax.all_to_all(copies, axis, split_axis=0, concat_axis=0, tiled=True)  17.3 us
    ppermute x13, waiting for transfers between devices, shifted(): lax.ppermute(value, axis, [((k + step) % size, k) for k in range(size)])  11.9 us
    all_to_all x1, blocking collectives, to_all(): return lax.all_to_all(copies, axis, split_axis=0, concat_axis=0, tiled=True)  9.62 us
    another operation x2, other arithmetic, decoder(): rest = both(jnp.stack([pieces[0], pieces[1], right, pieces[4]]))  2.98 us
  transfers between devices with their start and end apart: 14, of which 6 were waited for; matrix products, arithmetic and copies ran while one was open for 3% of the time, Pallas kernels for 5%

profile of v3, /device:TPU:1, one launch (start us, length us, event | category | flops | bytes accessed | tf_op | source)
XLA Modules:
  0.0 132.4 jit_solution(13612453004648356832)
XLA Ops:
  0.0 2.7 %shard_map.101 = bf16[2,32,256]{2,1,0:T(8,128)(2,1)} custom-call(bf16[32,2048]{1,0:T(8,128)(2,1)} %source.1, f32[2,2048]{1,0:T(2,128)} %gain.4, f32[2,64]{1,0:T(2,128)} %key_gain.1, bf16[2,2048,128]{2,1,0:T(8,128)(2,1)} %key_weight.1, bf16[2,2048,128]{2,1,0:T(8,128)(2,1)} %value_weight.1), custom_call_target="tpu_custom_call" | custom-call | flops 200000000 | bytes 1000000 | tf_op jit(solution)/shard_map/pallas_call | solution.py:199
  2.7 2.3 %broadcast_in_dim.6 = bf16[64,2,32,256]{3,2,1,0:T(8,128)(2,1)} broadcast(bf16[2,32,256]{2,1,0:T(8,128)(2,1)} %shard_map.101), dimensions={1,2,3} | broadcast | bytes 2129920 | tf_op jit(solution)/shard_map/broadcast_in_dim | solution.py:212
  5.1 17.3 %all-to-all-start = ((bf16[64,2,32,256]{3,2,1,0:T(8,128)(2,1)}), bf16[64,2,32,256]{3,2,1,0:T(8,128)(2,1)S(1)}, u32[]{:S(2)}, u32[]{:S(2)}) async-start(bf16[64,2,32,256]{3,2,1,0:T(8,128)(2,1)} %broadcast_in_dim.6), calls=%async_computation | async-start | bytes 4194304 | tf_op jit(solution)/shard_map/all_to_all | solution.py:213
  22.4 0.0 copy-start.4
  22.4 0.1 slice_bitcast_fusion
  22.5 3.3 %collective-permute-start.3 = (bf16[64,2048]{1,0:T(8,128)(2,1)S(1)}, bf16[64,2048]{1,0:T(8,128)(2,1)S(1)}, u32[]{:S(2)}, u32[]{:S(2)}) collective-permute-start(bf16[64,2048]{1,0:T(8,128)(2,1)S(1)} %get-tuple-element.22), channel_id=1, source_target_pairs={{6,0},{0,2},{2,4},{4,6},{7,1},{1,3},{3,5},{5,7},{14,8},{8,10},{10,... | collective-permute-start | bytes 786440 | tf_op jit(solution)/shard_map/ppermute | solution.py:218
  25.7 4.4 %collective-permute-start.2 = (bf16[64,2048]{1,0:T(8,128)(2,1)S(1)}, bf16[64,2048]{1,0:T(8,128)(2,1)S(1)}, u32[]{:S(2)}, u32[]{:S(2)}) collective-permute-start(bf16[64,2048]{1,0:T(8,128)(2,1)S(1)} %get-tuple-element.22), channel_id=1, source_target_pairs={{4,0},{6,2},{0,4},{2,6},{5,1},{7,3},{1,5},{3,7},{12,8},{14,10},{8,... | collective-permute-start | bytes 786440 | tf_op jit(solution)/shard_map/ppermute | solution.py:218
  30.1 3.1 %collective-permute-start.1 = (bf16[64,2048]{1,0:T(8,128)(2,1)S(1)}, bf16[64,2048]{1,0:T(8,128)(2,1)S(1)}, u32[]{:S(2)}, u32[]{:S(2)}) collective-permute-start(bf16[64,2048]{1,0:T(8,128)(2,1)S(1)} %get-tuple-element.22), channel_id=1, source_target_pairs={{2,0},{4,2},{6,4},{0,6},{3,1},{5,3},{7,5},{1,7},{10,8},{12,10},{14... | collective-permute-start | bytes 786440 | tf_op jit(solution)/shard_map/ppermute | solution.py:218
  33.2 0.0 collective-permute-done.3
  33.2 6.0 %collective-permute-done.2 = bf16[64,2048]{1,0:T(8,128)(2,1)S(1)} collective-permute-done((bf16[64,2048]{1,0:T(8,128)(2,1)S(1)}, bf16[64,2048]{1,0:T(8,128)(2,1)S(1)}, u32[]{:S(2)}, u32[]{:S(2)}) %collective-permute-start.2) | collective-permute-done | bytes 262176 | tf_op jit(solution)/shard_map/ppermute | solution.py:218
  39.2 1.2 collective-permute-done.1
  40.5 0.1 pad_maximum_fusion.1.mine
  40.6 4.0 %collective-permute-start.4 = (bf16[4,64,2048]{2,1,0:T(8,128)(2,1)S(1)}, bf16[4,64,2048]{2,1,0:T(8,128)(2,1)}, u32[]{:S(2)}, u32[]{:S(2)}) collective-permute-start(bf16[4,64,2048]{2,1,0:T(8,128)(2,1)S(1)} %pad_maximum_fusion.1.mine), channel_id=1, source_target_pairs={{1,0},{0,1},{3,2},{2,3},{5,4},{4,5},{7,6},{6,7},{9,8},{8,9},{11,10... | collective-permute-start | bytes 3145736 | tf_op jit(solution)/shard_map/ppermute | solution.py:218
  44.6 0.0 copy-done.4
  44.7 1.0 pad_maximum_fusion.2
  45.6 4.0 %collective-permute-start.10 = (bf16[192,2048]{1,0:T(8,128)(2,1)}, bf16[192,2048]{1,0:T(8,128)(2,1)}, u32[]{:S(2)}, u32[]{:S(2)}) collective-permute-start(bf16[192,2048]{1,0:T(8,128)(2,1)} %pad_maximum_fusion.2), channel_id=1, source_target_pairs={{6,0},{0,2},{2,4},{4,6},{7,1},{1,3},{3,5},{5,7},{14,8},{8,10},{10,... | collective-permute-start | bytes 2359304 | tf_op jit(solution)/shard_map/ppermute | solution.py:218
  49.7 2.4 %collective-permute-start.8 = (bf16[192,2048]{1,0:T(8,128)(2,1)}, bf16[192,2048]{1,0:T(8,128)(2,1)}, u32[]{:S(2)}, u32[]{:S(2)}) collective-permute-start(bf16[192,2048]{1,0:T(8,128)(2,1)} %pad_maximum_fusion.2), channel_id=1, source_target_pairs={{2,0},{4,2},{6,4},{0,6},{3,1},{5,3},{7,5},{1,7},{10,8},{12,10},{14... | collective-permute-start | bytes 2359304 | tf_op jit(solution)/shard_map/ppermute | solution.py:218
  52.1 2.5 %collective-permute-start = (bf16[32,2048]{1,0:T(8,128)(2,1)S(1)}, bf16[32,2048]{1,0:T(8,128)(2,1)S(1)}, u32[]{:S(2)}, u32[]{:S(2)}) collective-permute-start(bf16[32,2048]{1,0:T(8,128)(2,1)S(1)} %copy-done), channel_id=1, source_target_pairs={{1,0},{0,1},{3,2},{2,3},{5,4},{4,5},{7,6},{6,7},{9,8},{8,9},{11,10... | collective-permute-start | bytes 393224 | tf_op jit(solution)/shard_map/ppermute | solution.py:218
  54.6 0.1 pad_add_fusion.place
  54.7 0.9 collective-permute-done.beside
  55.6 0.0 collective-permute-done.4.other
  55.6 2.3 %shard_map.100.refs_0_ = bf16[64,512]{1,0:T(8,128)(2,1)S(1)} custom-call(s32[2]{0:T(128)S(1)} %pad_add_fusion.place, bf16[32,2048]{1,0:T(8,128)(2,1)S(1)} %copy-done, bf16[32,2048]{1,0:T(8,128)(2,1)S(1)} %collective-permute-done.beside, f32[2,2048]{1,0:T(2,128)S(1)} %copy-done.1, f32[2,64]{1,0:T(2,128)S(1)} %copy-done.2, ...), custom_call_target="tpu_custom_call" | custom-call | flops 200000000 | bytes 1000000 | tf_op jit(solution)/shard_map/pallas_call | solution.py:199
  57.9 2.8 %collective-permute-start.7 = (bf16[64,512]{1,0:T(8,128)(2,1)S(1)}, bf16[64,512]{1,0:T(8,128)(2,1)S(1)}, u32[]{:S(2)}, u32[]{:S(2)}) collective-permute-start(bf16[64,512]{1,0:T(8,128)(2,1)S(1)} %shard_map.100.refs_0_), channel_id=1, source_target_pairs={{6,0},{0,2},{2,4},{4,6},{7,1},{1,3},{3,5},{5,7},{14,8},{8,10},{10,... | collective-permute-start | bytes 196616 | tf_op jit(solution)/shard_map/ppermute | solution.py:218
  60.7 3.3 %collective-permute-start.6 = (bf16[64,512]{1,0:T(8,128)(2,1)S(1)}, bf16[64,512]{1,0:T(8,128)(2,1)S(1)}, u32[]{:S(2)}, u32[]{:S(2)}) collective-permute-start(bf16[64,512]{1,0:T(8,128)(2,1)S(1)} %shard_map.100.refs_0_), channel_id=1, source_target_pairs={{4,0},{6,2},{0,4},{2,6},{5,1},{7,3},{1,5},{3,7},{12,8},{14,10},{8,... | collective-permute-start | bytes 196616 | tf_op jit(solution)/shard_map/ppermute | solution.py:218
  64.1 3.2 %collective-permute-start.5 = (bf16[64,512]{1,0:T(8,128)(2,1)S(1)}, bf16[64,512]{1,0:T(8,128)(2,1)S(1)}, u32[]{:S(2)}, u32[]{:S(2)}) collective-permute-start(bf16[64,512]{1,0:T(8,128)(2,1)S(1)} %shard_map.100.refs_0_), channel_id=1, source_target_pairs={{2,0},{4,2},{6,4},{0,6},{3,1},{5,3},{7,5},{1,7},{10,8},{12,10},{14... | collective-permute-start | bytes 196616 | tf_op jit(solution)/shard_map/ppermute | solution.py:218
  67.3 0.9 collective-permute-done.10
  68.1 1.0 slice.30
  69.1 2.8 %collective-permute-start.11 = (bf16[96,2048]{1,0:T(8,128)(2,1)S(1)}, bf16[96,2048]{1,0:T(8,128)(2,1)}, u32[]{:S(2)}, u32[]{:S(2)}) collective-permute-start(bf16[96,2048]{1,0:T(8,128)(2,1)S(1)} %slice.30), channel_id=1, source_target_pairs={{6,0},{0,2},{2,4},{4,6},{7,1},{1,3},{3,5},{5,7},{14,8},{8,10},{10,... | collective-permute-start | bytes 1179656 | tf_op jit(solution)/shard_map/ppermute | solution.py:218
  72.0 0.0 collective-permute-done.8
  72.0 1.0 slice.29
  73.0 3.7 %collective-permute-start.9 = (bf16[96,2048]{1,0:T(8,128)(2,1)S(1)}, bf16[96,2048]{1,0:T(8,128)(2,1)}, u32[]{:S(2)}, u32[]{:S(2)}) collective-permute-start(bf16[96,2048]{1,0:T(8,128)(2,1)S(1)} %slice.29), channel_id=1, source_target_pairs={{2,0},{4,2},{6,4},{0,6},{3,1},{5,3},{7,5},{1,7},{10,8},{12,10},{14... | collective-permute-start | bytes 1179656 | tf_op jit(solution)/shard_map/ppermute | solution.py:218
  76.7 0.0 collective-permute-done.7.refs_3_
  76.7 0.0 collective-permute-done.6.refs_2_
  76.7 0.0 collective-permute-done.5.refs_1_
  76.7 0.0 all-to-all-done.refs_4_.refs_1_
  76.7 4.5 %shard_map.102 = bf16[256,640]{1,0:T(8,128)(2,1)S(1)} custom-call(s32[2]{0:T(128)S(1)} %pad_add_fusion.place, bf16[64,512]{1,0:T(8,128)(2,1)S(1)} %shard_map.100.refs_0_, bf16[64,512]{1,0:T(8,128)(2,1)S(1)} %collective-permute-done.5.refs_1_, bf16[64,512]{1,0:T(8,128)(2,1)S(1)} %collective-permute-done.6.refs_2_, ...), custom_call_target="tpu_custom_call" | custom-call | flops 5000000000 | bytes 1000000 | tf_op jit(solution)/shard_map/pallas_call | solution.py:199
  81.2 0.5 collective-permute-done.11
  81.7 2.4 %collective-permute-done.9 = bf16[96,2048]{1,0:T(8,128)(2,1)} collective-permute-done((bf16[96,2048]{1,0:T(8,128)(2,1)S(1)}, bf16[96,2048]{1,0:T(8,128)(2,1)}, u32[]{:S(2)}, u32[]{:S(2)}) %collective-permute-start.9) | collective-permute-done | bytes 393248 | tf_op jit(solution)/shard_map/ppermute | solution.py:218
  84.1 1.2 maximum_bitcast_fusion
  85.2 1.8 %pad_maximum_fusion.out_mine.mine = bf16[4,192,2048]{2,1,0:T(8,128)(2,1)S(1)} fusion(bf16[1,192,2048]{2,1,0:T(8,128)(2,1)} %bitcast.14, bf16[1,192,2048]{2,1,0:T(8,128)(2,1)S(1)} %maximum_bitcast_fusion, bf16[1,192,2048]{2,1,0:T(8,128)(2,1)} %bitcast.12, bf16[1,192,2048]{2,1,0:T(8,128)(2,1)} %bitcast.11), kind=kLoop, calls=%fused_computation | loop fusion | flops 4718592 | bytes 6291456 | tf_op jit(solution)/shard_map/stack | solution.py:284
  87.1 4.4 %collective-permute-start.12 = (bf16[4,192,2048]{2,1,0:T(8,128)(2,1)S(1)}, bf16[4,192,2048]{2,1,0:T(8,128)(2,1)S(1)}, u32[]{:S(2)}, u32[]{:S(2)}) collective-permute-start(bf16[4,192,2048]{2,1,0:T(8,128)(2,1)S(1)} %pad_maximum_fusion.out_mine.mine), channel_id=1, source_target_pairs={{1,0},{0,1},{3,2},{2,3},{5,4},{4,5},{7,6},{6,7},{9,8},{8,9},{11,10... | collective-permute-start | bytes 9437192 | tf_op jit(solution)/shard_map/ppermute | solution.py:218
  91.4 11.9 %all_to_all.20.arrived = bf16[8,32,640]{2,1,0:T(8,128)(2,1)S(1)} all-to-all(bf16[8,32,640]{2,1,0:T(8,128)(2,1)S(1)} %bitcast.22), channel_id=1, replica_groups=mesh['z'=8,'y'=8,'x'=4,'c'=2] {'x','c'}, dimensions={0} | all-to-all | bytes 655360 | tf_op jit(solution)/shard_map/all_to_all | solution.py:286
  103.3 0.0 collective-permute-done.12.out_other.other
  103.3 2.2 %shard_map.103 = (bf16[32,2048]{1,0:T(8,128)(2,1)S(1)}, bf16[32,512]{1,0:T(8,128)(2,1)S(1)}) custom-call(s32[2]{0:T(128)S(1)} %pad_add_fusion.place, bf16[8,32,640]{2,1,0:T(8,128)(2,1)S(1)} %all_to_all.20.arrived, bf16[32,2048]{1,0:T(8,128)(2,1)S(1)} %copy-done, f32[2,2048]{1,0:T(2,128)S(1)} %copy-done.1, f32[2,64]{1,0:T(2,128)S(1)} %copy-done.2, ...), custom_call_target="tpu_custom_call" | custom-call | flops 400000000 | bytes 1000000 | tf_op jit(solution)/shard_map/pallas_call | solution.py:199
  105.5 9.6 %all_to_all.21 = bf16[8,32,512]{2,1,0:T(8,128)(2,1)S(1)} all-to-all(bf16[8,32,512]{2,1,0:T(8,128)(2,1)S(1)} %broadcast_in_dim.7), channel_id=1, replica_groups=mesh['z'=8,'y'=8,'x'=4,'c'=2] {'x','c'}, dimensions={0} | all-to-all | bytes 524288 | tf_op jit(solution)/shard_map/all_to_all | solution.py:213
  115.2 4.5 %shard_map.104 = bf16[256,640]{1,0:T(8,128)(2,1)S(1)} custom-call(s32[2]{0:T(128)S(1)} %pad_add_fusion.place, bf16[256,512]{1,0:T(8,128)(2,1)S(1)} %bitcast.24, bf16[64,2,32,256]{3,2,1,0:T(8,128)(2,1)S(1)} %all-to-all-done.refs_4_.refs_1_), custom_call_target="tpu_custom_call" | custom-call | flops 5000000000 | bytes 1000000 | tf_op jit(solution)/shard_map/pallas_call | solution.py:199
  119.6 10.9 %all_to_all.22.arrived = bf16[8,32,640]{2,1,0:T(8,128)(2,1)S(1)} all-to-all(bf16[8,32,640]{2,1,0:T(8,128)(2,1)S(1)} %bitcast.23), channel_id=1, replica_groups=mesh['z'=8,'y'=8,'x'=4,'c'=2] {'x','c'}, dimensions={0} | all-to-all | bytes 655360 | tf_op jit(solution)/shard_map/all_to_all | solution.py:286
  130.5 1.9 %shard_map.105 = bf16[32,2048]{1,0:T(8,128)(2,1)} custom-call(s32[2]{0:T(128)S(1)} %pad_add_fusion.place, bf16[8,32,640]{2,1,0:T(8,128)(2,1)S(1)} %all_to_all.22.arrived, bf16[32,2048]{1,0:T(8,128)(2,1)S(1)} %get-tuple-element.18.hidden, bf16[4,192,2048]{2,1,0:T(8,128)(2,1)S(1)} %pad_maximum_fusion.out_mine.mine, ...), custom_call_target="tpu_custom_call" | custom-call | flops 200000000 | bytes 1000000 | tf_op jit(solution)/shard_map/pallas_call | solution.py:199
  (10 shorter events, 0.1 us)
Async XLA Ops:
  5.1 17.3 %copy-start.3 = (bf16[2,2048,64]{1,2,0:T(8,128)(2,1)S(1)}, bf16[2,2048,64]{1,2,0:T(8,128)(2,1)}, u32[]{:S(2)}) copy-start(bf16[2,2048,64]{1,2,0:T(8,128)(2,1)} %param.16) | copy-start | bytes 1572868
  5.1 71.6 %all-to-all-start = ((bf16[64,2,32,256]{3,2,1,0:T(8,128)(2,1)}), bf16[64,2,32,256]{3,2,1,0:T(8,128)(2,1)S(1)}, u32[]{:S(2)}, u32[]{:S(2)}) async-start(bf16[64,2,32,256]{3,2,1,0:T(8,128)(2,1)} %broadcast_in_dim.6), calls=%async_computation | async-start | bytes 4194304 | tf_op jit(solution)/shard_map/all_to_all | solution.py:213
  22.4 22.2 %copy-start.4 = (bf16[2,64,2048]{2,1,0:T(8,128)(2,1)S(1)}, bf16[2,64,2048]{2,1,0:T(8,128)(2,1)}, u32[]{:S(2)}) copy-start(bf16[2,64,2048]{2,1,0:T(8,128)(2,1)} %param.19) | copy-start | bytes 1572868
  22.5 10.7 %collective-permute-start.3 = (bf16[64,2048]{1,0:T(8,128)(2,1)S(1)}, bf16[64,2048]{1,0:T(8,128)(2,1)S(1)}, u32[]{:S(2)}, u32[]{:S(2)}) collective-permute-start(bf16[64,2048]{1,0:T(8,128)(2,1)S(1)} %get-tuple-element.22), channel_id=1, source_target_pairs={{6,0},{0,2},{2,4},{4,6},{7,1},{1,3},{3,5},{5,7},{14,8},{8,10},{10,... | collective-permute-start | bytes 786440 | tf_op jit(solution)/shard_map/ppermute | solution.py:218
  25.7 13.5 %collective-permute-start.2 = (bf16[64,2048]{1,0:T(8,128)(2,1)S(1)}, bf16[64,2048]{1,0:T(8,128)(2,1)S(1)}, u32[]{:S(2)}, u32[]{:S(2)}) collective-permute-start(bf16[64,2048]{1,0:T(8,128)(2,1)S(1)} %get-tuple-element.22), channel_id=1, source_target_pairs={{4,0},{6,2},{0,4},{2,6},{5,1},{7,3},{1,5},{3,7},{12,8},{14,10},{8,... | collective-permute-start | bytes 786440 | tf_op jit(solution)/shard_map/ppermute | solution.py:218
  30.1 10.4 %collective-permute-start.1 = (bf16[64,2048]{1,0:T(8,128)(2,1)S(1)}, bf16[64,2048]{1,0:T(8,128)(2,1)S(1)}, u32[]{:S(2)}, u32[]{:S(2)}) collective-permute-start(bf16[64,2048]{1,0:T(8,128)(2,1)S(1)} %get-tuple-element.22), channel_id=1, source_target_pairs={{2,0},{4,2},{6,4},{0,6},{3,1},{5,3},{7,5},{1,7},{10,8},{12,10},{14... | collective-permute-start | bytes 786440 | tf_op jit(solution)/shard_map/ppermute | solution.py:218
  40.4 11.7 %copy-start = (bf16[32,2048]{1,0:T(8,128)(2,1)S(1)}, bf16[32,2048]{1,0:T(8,128)(2,1)}, u32[]{:S(2)}) copy-start(bf16[32,2048]{1,0:T(8,128)(2,1)} %hidden.1) | copy-start | bytes 393220
  40.4 15.1 %copy-start.1 = (f32[2,2048]{1,0:T(2,128)S(1)}, f32[2,2048]{1,0:T(2,128)}, u32[]{:S(2)}) copy-start(f32[2,2048]{1,0:T(2,128)} %gain.5) | copy-start | bytes 49156
  40.5 15.1 %copy-start.2 = (f32[2,64]{1,0:T(2,128)S(1)}, f32[2,64]{1,0:T(2,128)}, u32[]{:S(2)}) copy-start(f32[2,64]{1,0:T(2,128)} %query_gain.3) | copy-start | bytes 1540
  40.6 15.0 %collective-permute-start.4 = (bf16[4,64,2048]{2,1,0:T(8,128)(2,1)S(1)}, bf16[4,64,2048]{2,1,0:T(8,128)(2,1)}, u32[]{:S(2)}, u32[]{:S(2)}) collective-permute-start(bf16[4,64,2048]{2,1,0:T(8,128)(2,1)S(1)} %pad_maximum_fusion.1.mine), channel_id=1, source_target_pairs={{1,0},{0,1},{3,2},{2,3},{5,4},{4,5},{7,6},{6,7},{9,8},{8,9},{11,10... | collective-permute-start | bytes 3145736 | tf_op jit(solution)/shard_map/ppermute | solution.py:218
  45.6 22.5 %collective-permute-start.10 = (bf16[192,2048]{1,0:T(8,128)(2,1)}, bf16[192,2048]{1,0:T(8,128)(2,1)}, u32[]{:S(2)}, u32[]{:S(2)}) collective-permute-start(bf16[192,2048]{1,0:T(8,128)(2,1)} %pad_maximum_fusion.2), channel_id=1, source_target_pairs={{6,0},{0,2},{2,4},{4,6},{7,1},{1,3},{3,5},{5,7},{14,8},{8,10},{10,... | collective-permute-start | bytes 2359304 | tf_op jit(solution)/shard_map/ppermute | solution.py:218
  49.7 22.3 %collective-permute-start.8 = (bf16[192,2048]{1,0:T(8,128)(2,1)}, bf16[192,2048]{1,0:T(8,128)(2,1)}, u32[]{:S(2)}, u32[]{:S(2)}) collective-permute-start(bf16[192,2048]{1,0:T(8,128)(2,1)} %pad_maximum_fusion.2), channel_id=1, source_target_pairs={{2,0},{4,2},{6,4},{0,6},{3,1},{5,3},{7,5},{1,7},{10,8},{12,10},{14... | collective-permute-start | bytes 2359304 | tf_op jit(solution)/shard_map/ppermute | solution.py:218
  52.1 3.5 %collective-permute-start = (bf16[32,2048]{1,0:T(8,128)(2,1)S(1)}, bf16[32,2048]{1,0:T(8,128)(2,1)S(1)}, u32[]{:S(2)}, u32[]{:S(2)}) collective-permute-start(bf16[32,2048]{1,0:T(8,128)(2,1)S(1)} %copy-done), channel_id=1, source_target_pairs={{1,0},{0,1},{3,2},{2,3},{5,4},{4,5},{7,6},{6,7},{9,8},{8,9},{11,10... | collective-permute-start | bytes 393224 | tf_op jit(solution)/shard_map/ppermute | solution.py:218
  57.9 18.8 %collective-permute-start.7 = (bf16[64,512]{1,0:T(8,128)(2,1)S(1)}, bf16[64,512]{1,0:T(8,128)(2,1)S(1)}, u32[]{:S(2)}, u32[]{:S(2)}) collective-permute-start(bf16[64,512]{1,0:T(8,128)(2,1)S(1)} %shard_map.100.refs_0_), channel_id=1, source_target_pairs={{6,0},{0,2},{2,4},{4,6},{7,1},{1,3},{3,5},{5,7},{14,8},{8,10},{10,... | collective-permute-start | bytes 196616 | tf_op jit(solution)/shard_map/ppermute | solution.py:218
  60.7 16.0 %collective-permute-start.6 = (bf16[64,512]{1,0:T(8,128)(2,1)S(1)}, bf16[64,512]{1,0:T(8,128)(2,1)S(1)}, u32[]{:S(2)}, u32[]{:S(2)}) collective-permute-start(bf16[64,512]{1,0:T(8,128)(2,1)S(1)} %shard_map.100.refs_0_), channel_id=1, source_target_pairs={{4,0},{6,2},{0,4},{2,6},{5,1},{7,3},{1,5},{3,7},{12,8},{14,10},{8,... | collective-permute-start | bytes 196616 | tf_op jit(solution)/shard_map/ppermute | solution.py:218
  64.1 12.6 %collective-permute-start.5 = (bf16[64,512]{1,0:T(8,128)(2,1)S(1)}, bf16[64,512]{1,0:T(8,128)(2,1)S(1)}, u32[]{:S(2)}, u32[]{:S(2)}) collective-permute-start(bf16[64,512]{1,0:T(8,128)(2,1)S(1)} %shard_map.100.refs_0_), channel_id=1, source_target_pairs={{2,0},{4,2},{6,4},{0,6},{3,1},{5,3},{7,5},{1,7},{10,8},{12,10},{14... | collective-permute-start | bytes 196616 | tf_op jit(solution)/shard_map/ppermute | solution.py:218
  69.1 12.5 %collective-permute-start.11 = (bf16[96,2048]{1,0:T(8,128)(2,1)S(1)}, bf16[96,2048]{1,0:T(8,128)(2,1)}, u32[]{:S(2)}, u32[]{:S(2)}) collective-permute-start(bf16[96,2048]{1,0:T(8,128)(2,1)S(1)} %slice.30), channel_id=1, source_target_pairs={{6,0},{0,2},{2,4},{4,6},{7,1},{1,3},{3,5},{5,7},{14,8},{8,10},{10,... | collective-permute-start | bytes 1179656 | tf_op jit(solution)/shard_map/ppermute | solution.py:218
  73.0 11.1 %collective-permute-start.9 = (bf16[96,2048]{1,0:T(8,128)(2,1)S(1)}, bf16[96,2048]{1,0:T(8,128)(2,1)}, u32[]{:S(2)}, u32[]{:S(2)}) collective-permute-start(bf16[96,2048]{1,0:T(8,128)(2,1)S(1)} %slice.29), channel_id=1, source_target_pairs={{2,0},{4,2},{6,4},{0,6},{3,1},{5,3},{7,5},{1,7},{10,8},{12,10},{14... | collective-permute-start | bytes 1179656 | tf_op jit(solution)/shard_map/ppermute | solution.py:218
  87.1 16.3 %collective-permute-start.12 = (bf16[4,192,2048]{2,1,0:T(8,128)(2,1)S(1)}, bf16[4,192,2048]{2,1,0:T(8,128)(2,1)S(1)}, u32[]{:S(2)}, u32[]{:S(2)}) collective-permute-start(bf16[4,192,2048]{2,1,0:T(8,128)(2,1)S(1)} %pad_maximum_fusion.out_mine.mine), channel_id=1, source_target_pairs={{1,0},{0,1},{3,2},{2,3},{5,4},{4,5},{7,6},{6,7},{9,8},{8,9},{11,10... | collective-permute-start | bytes 9437192 | tf_op jit(solution)/shard_map/ppermute | solution.py:218

commit v4 on v3

--- a/solution.py
+++ b/solution.py
@@ -128,51 +128,61 @@
     hidden_out[...] = mixed(place, arrived, hidden, out_mine, out_other, heads, head)
 
 
-def attention_kernel(heads, head, tile, count, place, *refs):
-    queries, (pairs, out, rhs, value_t, gathered) = refs[:count], refs[count:]
-    blocks, each_rows, _ = pairs.shape
-    keys = blocks * each_rows
+def attention_kernel(heads, head, tile, counts, place, *refs):
+    count, shards = counts
+    queries, planes, (out, rhs, value_t, gathered) = refs[:count], refs[count : count + shards], refs[count + shards :]
+    blocks, each_rows, _ = planes[0].shape
+    shard = blocks * each_rows
     width = 2 * head
-    everyone = jnp.concatenate([part[...].astype(F32) for part in queries], axis=0)
-    columns = everyone.shape[0]
+    everyone = jnp.concatenate([part[...].astype(F32).reshape(-1, heads * head) for part in queries], axis=0)
+    rows = everyone.shape[0]
+    groups, _, columns = rhs.shape
+    pack = columns // rows
     factor = LOG2E * head**-0.5
     turned = jnp.transpose(everyone).astype(BF16)
     zero = jnp.zeros((head, columns), BF16)
-    per = heads // 4
-    for p in range(heads):
-        kv = (p % 4) // 2
-        rhs[p, kv * head : (kv + 1) * head, :] = turned[p * head : (p + 1) * head, :]
-        rhs[p, (1 - kv) * head : (2 - kv) * head, :] = zero
-    value_t[...] = jnp.transpose(pairs[:, :, width:].reshape(keys, width).astype(F32)).astype(BF16)
-    for kv in range(2):
-
-        def one_head(j, carry, kv=kv):
-            p = (j // 2) * 4 + 2 * kv + j % 2
-            right = rhs[p]
-            mass = jnp.zeros((8, columns), F32)
-            total = None
-            for t in range(keys // tile):
+
+    def key_head(group):
+        return group * pack % 4 // 2
+
+    for group in range(groups):
+        kv = key_head(group)
+        for k in range(pack):
+            p = group * pack + k
+            rhs[group, kv * head : (kv + 1) * head, k * rows : (k + 1) * rows] = turned[p * head : (p + 1) * head, :]
+        rhs[group, (1 - kv) * head : (2 - kv) * head, :] = zero
+    for n, pairs in enumerate(planes):
+        flat = pairs[:, :, width:].reshape(shard, width).astype(F32)
+        value_t[:, n * shard : (n + 1) * shard] = jnp.transpose(flat).astype(BF16)
+    for group in range(groups):
+        kv = key_head(group)
+        right = rhs[group]
+        mass = jnp.zeros((8, columns), F32)
+        total = None
+        for n, pairs in enumerate(planes):
+            for t in range(shard // tile):
                 taken = slice(t * tile // each_rows, (t + 1) * tile // each_rows)
                 score = dot(pairs[taken, :, :width].reshape(tile, width), right)
                 weight = jnp.exp2(score * factor)
                 mass = mass + jnp.sum(weight.reshape(tile // 8, 8, columns), axis=0)
-                part = dot(value_t[:, t * tile : (t + 1) * tile], weight.astype(BF16))
+                first = n * shard + t * tile
+                part = dot(value_t[:, first : first + tile], weight.astype(BF16))
                 total = part if total is None else total + part
-            gathered[pl.ds(pl.multiple_of(p * head, head), head), :] = total[kv * head : (kv + 1) * head, :]
-            mass = jnp.sum(mass, axis=0, keepdims=True)
-            top = mass.astype(BF16).astype(F32)
-            gathered[pl.ds(heads * head + p, 1), :] = top
-            gathered[pl.ds(heads * head + heads + p, 1), :] = mass - top
-            return carry
-
-        lax.fori_loop(0, 2 * per, one_head, 0, unroll=True)
+        mass = jnp.sum(mass, axis=0, keepdims=True)
+        top = mass.astype(BF16).astype(F32)
+        for k in range(pack):
+            p = group * pack + k
+            here = slice(k * rows, (k + 1) * rows)
+            gathered[p * head : (p + 1) * head, :] = total[kv * head : (kv + 1) * head, here]
+            gathered[heads * head + p : heads * head + p + 1, :] = top[:, here]
+            gathered[heads * head + heads + p : heads * head + heads + p + 1, :] = (mass - top)[:, here]
     rest = heads * head + 2 * heads
-    gathered[rest:, :] = jnp.zeros((gathered.shape[0] - rest, columns), F32)
+    gathered[rest:, :] = jnp.zeros((gathered.shape[0] - rest, rows), F32)
     result = jnp.transpose(gathered[...]).astype(BF16)
     if count == 1:
         out[...] = result
         return
-    each = columns // (2 * count)
+    each = rows // (2 * count)
     for r in range(count):
         for d in range(2):
             to = ((place[0] + r) % count) * 2 + (place[1] + d) % 2
@@ -190,7 +200,7 @@
     return pl.BlockSpec((value.shape[0], size, value.shape[2]), lambda i, k=k: (0, k, 0))
 
 
-def with_place(kernel, shapes, operands, parts, flops, scratch=(), limit=40):
+def with_place(kernel, shapes, operands, parts, flops, scratch=(), limit=24):
     one = not isinstance(shapes, (list, tuple))
     place, *rest = operands
     placed = [] if place is None else [place]
@@ -264,44 +274,47 @@
     )
     everyone = [chip] + [shifted(chip, "x", k) for k in range(1, lax.axis_size("x"))]
 
-    hidden = target
-    for layer in range(layers):
-        partial = with_place(
-            functools.partial(attention_kernel, heads, head, 512, len(everyone)),
-            shapes((group, wide), BF16),
+    def attend(everyone, parts, members):
+        columns = group
+        return with_place(
+            functools.partial(attention_kernel, heads, head, 512, (len(everyone), len(parts))),
+            shapes((members * rows, wide), BF16),
             (place, *everyone),
-            [(plane, layer, 1)],
+            parts,
             5000000000,
             scratch=[
-                pltpu.VMEM((heads, 2 * head, group), BF16),
-                pltpu.VMEM((2 * head, keys), BF16),
-                pltpu.VMEM((wide, group), F32),
+                pltpu.VMEM((heads * members * rows // columns, 2 * head, columns), BF16),
+                pltpu.VMEM((2 * head, len(parts) * keys), BF16),
+                pltpu.VMEM((wide, members * rows), F32),
             ],
+            limit=52,
         )
-        if layer == 0:
-            pieces, _ = lax.optimization_barrier((pieces, partial))
-            right = jnp.concatenate(pieces[2:4], axis=0)
-            rest = both(jnp.stack([pieces[0], pieces[1], right, pieces[4]]))
-            rest = [[(part, k, head) for part in rest] for k in range(3)]
-        arrived = lax.all_to_all(partial.reshape(-1, rows, wide), TP, split_axis=0, concat_axis=0, tiled=True)
-        if layer + 1 < layers:
-            hidden, queries = with_place(
-                functools.partial(middle_kernel, layer + 1, heads),
-                [shapes((rows, model), BF16), shapes((rows, width), BF16)],
-                (place, arrived, hidden, target_gain, query_gain),
-                rest[0] + rest[1],
-                400000000,
-            )
-            everyone = [to_all(queries, TP).reshape(group, width)]
-        else:
-            hidden = with_place(
-                functools.partial(last_kernel, heads, head),
-                shapes((rows, model), BF16),
-                (place, arrived, hidden),
-                rest[2],
-                200000000,
-            )
-    return hidden
+
+    def returned(partial, axis):
+        return lax.all_to_all(partial.reshape(-1, rows, wide), axis, split_axis=0, concat_axis=0, tiled=True)
+
+    partial = attend(everyone, [(plane, 0, 1)], lax.axis_size(TP))
+    pieces, second, _ = lax.optimization_barrier((pieces, plane, partial))
+    far = jnp.concatenate(pieces[2:4], axis=0)
+    rest = both(jnp.stack([pieces[0], pieces[1], far, pieces[4]]))
+    rest = [[(part, k, head) for part in rest] for k in range(3)]
+    shared = shifted(second[:, 1:2], "c", 1)
+    arrived = returned(partial, TP)
+    hidden, queries = with_place(
+        functools.partial(middle_kernel, 1, heads),
+        [shapes((rows, model), BF16), shapes((rows, width), BF16)],
+        (place, arrived, target, target_gain, query_gain),
+        rest[0] + rest[1],
+        400000000,
+    )
+    partial = attend([to_all(queries, "x")], [(plane, 1, 1), (shared, 0, 1)], lax.axis_size("x"))
+    return with_place(
+        functools.partial(last_kernel, heads, head),
+        shapes((rows, model), BF16),
+        (place, returned(partial, "x"), hidden),
+        rest[2],
+        200000000,
+    )
 
 
 def solution(mesh):

time: 133 us -> 134 us (level); the launches traced: 132 us -> 132 us
  blocking collectives: 32.4 us -> 19.7 us
  starting transfers between devices: 61.1 us -> 66.9 us
  waiting for transfers between devices: 11.9 us -> 15.9 us
  local copies, waits for them, and re-layouts: 4.55 us -> 7.47 us
  other arithmetic: 4.14 us -> 1.89 us
  Pallas kernels: 18 us -> 19.6 us
    all_to_all x3 -> x2, blocking collectives: 32.4 us -> 19.7 us  [returned(): lax.all_to_all(partial.reshape(-1, rows, wide), axis, split_axis=0, conca...]
    all_to_all x1 -> x2, waiting for transfers between devices: 0.01 us -> 4.6 us  [to_all(): return lax.all_to_all(copies, axis, split_axis=0, concat_axis=0, tiled=True)]
    all_to_all x1 -> x2, starting transfers between devices: 17.3 us -> 21 us  [to_all(): return lax.all_to_all(copies, axis, split_axis=0, concat_axis=0, tiled=True)]
    slice x0 -> x1, local copies, waits for them, and re-layouts: none -> 2.26 us  [decoder(): shared = shifted(second[:, 1:2], 'c', 1)]
    ppermute x13 -> x14, starting transfers between devices: 43.9 us -> 45.9 us  [shifted(): lax.ppermute(value, axis, [((k + step) % size, k) for k in range(size)])]
    pallas_call x6, Pallas kernels: 18 us -> 19.6 us  [with_place(): pl.pallas_call(kernel, grid=(1,), out_shape=shapes, in_specs=specs, out_s...]
    another operation x2, other arithmetic: 2.98 us -> 1.63 us  [decoder(): rest = both(jnp.stack([pieces[0], pieces[1], far, pieces[4]]))]
    ppermute x13 -> x14, waiting for transfers between devices: 11.9 us -> 11.3 us  [shifted(): lax.ppermute(value, axis, [((k + step) % size, k) for k in range(size)])]
  transfers between devices with their start and end apart: 14 -> 16, of which waited for: 6 -> 6; matrix products, arithmetic and copies ran while one was open for 3% -> 4% of each run, Pallas kernels for 5% -> 7%
where the time goes in v4:
time: 134 us; the launch traced here: 132 us
  starting transfers between devices  66.9 us (50%)
  blocking collectives  19.7 us (15%)
  Pallas kernels  19.6 us (15%)
  waiting for transfers between devices  15.9 us (12%)
  local copies, waits for them, and re-layouts  7.47 us (6%)
  other arithmetic  1.89 us (1%)
    ppermute x14, starting transfers between devices, shifted(): lax.ppermute(value, axis, [((k + step) % size, k) for k in range(size)])  45.9 us
    all_to_all x2, starting transfers between devices, to_all(): return lax.all_to_all(copies, axis, split_axis=0, concat_axis=0, tiled=True)  21 us
    all_to_all x2, blocking collectives, returned(): lax.all_to_all(partial.reshape(-1, rows, wide), axis, split_axis=0, conca...  19.7 us
    pallas_call x6, Pallas kernels, with_place(): pl.pallas_call(kernel, grid=(1,), out_shape=shapes, in_specs=specs, out_s...  19.6 us
    ppermute x14, waiting for transfers between devices, shifted(): lax.ppermute(value, axis, [((k + step) % size, k) for k in range(size)])  11.3 us
    all_to_all x2, waiting for transfers between devices, to_all(): return lax.all_to_all(copies, axis, split_axis=0, concat_axis=0, tiled=True)  4.6 us
    broadcast_in_dim x2, local copies, waits for them, and re-layouts, to_all(): copies = jnp.broadcast_to(value, (lax.axis_size(axis), *value.shape))  3.02 us
  transfers between devices with their start and end apart: 16, of which 6 were waited for; matrix products, arithmetic and copies ran while one was open for 4% of the time, Pallas kernels for 7%

profile of v4, /device:TPU:1, one launch (start us, length us, event | category | flops | bytes accessed | tf_op | source)
XLA Modules:
  0.0 131.9 jit_solution(7572674142225848799)
XLA Ops:
  0.0 2.7 %shard_map.101 = bf16[2,32,256]{2,1,0:T(8,128)(2,1)} custom-call(bf16[32,2048]{1,0:T(8,128)(2,1)} %source.1, f32[2,2048]{1,0:T(2,128)} %gain.4, f32[2,64]{1,0:T(2,128)} %key_gain.1, bf16[2,2048,128]{2,1,0:T(8,128)(2,1)} %key_weight.1, bf16[2,2048,128]{2,1,0:T(8,128)(2,1)} %value_weight.1), custom_call_target="tpu_custom_call" | custom-call | flops 200000000 | bytes 1000000 | tf_op jit(solution)/shard_map/pallas_call | solution.py:209
  2.7 2.4 %broadcast_in_dim.6 = bf16[64,2,32,256]{3,2,1,0:T(8,128)(2,1)} broadcast(bf16[2,32,256]{2,1,0:T(8,128)(2,1)} %shard_map.101), dimensions={1,2,3} | broadcast | bytes 2129920 | tf_op jit(solution)/shard_map/broadcast_in_dim | solution.py:222
  5.1 17.5 %all-to-all-start = ((bf16[64,2,32,256]{3,2,1,0:T(8,128)(2,1)}), bf16[64,2,32,256]{3,2,1,0:T(8,128)(2,1)}, u32[]{:S(2)}, u32[]{:S(2)}) async-start(bf16[64,2,32,256]{3,2,1,0:T(8,128)(2,1)} %broadcast_in_dim.6), calls=%async_computation | async-start | bytes 4194304 | tf_op jit(solution)/shard_map/all_to_all | solution.py:223
  22.6 0.0 copy-start.8
  22.7 0.1 slice_bitcast_fusion
  22.7 3.3 %collective-permute-start.3 = (bf16[64,2048]{1,0:T(8,128)(2,1)S(1)}, bf16[64,2048]{1,0:T(8,128)(2,1)S(1)}, u32[]{:S(2)}, u32[]{:S(2)}) collective-permute-start(bf16[64,2048]{1,0:T(8,128)(2,1)S(1)} %get-tuple-element.24), channel_id=1, source_target_pairs={{6,0},{0,2},{2,4},{4,6},{7,1},{1,3},{3,5},{5,7},{14,8},{8,10},{10,... | collective-permute-start | bytes 786440 | tf_op jit(solution)/shard_map/ppermute | solution.py:228
  26.0 4.4 %collective-permute-start.2 = (bf16[64,2048]{1,0:T(8,128)(2,1)S(1)}, bf16[64,2048]{1,0:T(8,128)(2,1)S(1)}, u32[]{:S(2)}, u32[]{:S(2)}) collective-permute-start(bf16[64,2048]{1,0:T(8,128)(2,1)S(1)} %get-tuple-element.24), channel_id=1, source_target_pairs={{4,0},{6,2},{0,4},{2,6},{5,1},{7,3},{1,5},{3,7},{12,8},{14,10},{8,... | collective-permute-start | bytes 786440 | tf_op jit(solution)/shard_map/ppermute | solution.py:228
  30.4 3.1 %collective-permute-start.1 = (bf16[64,2048]{1,0:T(8,128)(2,1)S(1)}, bf16[64,2048]{1,0:T(8,128)(2,1)S(1)}, u32[]{:S(2)}, u32[]{:S(2)}) collective-permute-start(bf16[64,2048]{1,0:T(8,128)(2,1)S(1)} %get-tuple-element.24), channel_id=1, source_target_pairs={{2,0},{4,2},{6,4},{0,6},{3,1},{5,3},{7,5},{1,7},{10,8},{12,10},{14... | collective-permute-start | bytes 786440 | tf_op jit(solution)/shard_map/ppermute | solution.py:228
  33.4 0.0 collective-permute-done.3
  33.4 6.1 %collective-permute-done.2 = bf16[64,2048]{1,0:T(8,128)(2,1)S(1)} collective-permute-done((bf16[64,2048]{1,0:T(8,128)(2,1)S(1)}, bf16[64,2048]{1,0:T(8,128)(2,1)S(1)}, u32[]{:S(2)}, u32[]{:S(2)}) %collective-permute-start.2) | collective-permute-done | bytes 262176 | tf_op jit(solution)/shard_map/ppermute | solution.py:228
  39.6 1.2 collective-permute-done.1
  40.8 0.1 pad_maximum_fusion.1.mine
  41.0 3.9 %collective-permute-start.4 = (bf16[4,64,2048]{2,1,0:T(8,128)(2,1)S(1)}, bf16[4,64,2048]{2,1,0:T(8,128)(2,1)S(1)}, u32[]{:S(2)}, u32[]{:S(2)}) collective-permute-start(bf16[4,64,2048]{2,1,0:T(8,128)(2,1)S(1)} %pad_maximum_fusion.1.mine), channel_id=1, source_target_pairs={{1,0},{0,1},{3,2},{2,3},{5,4},{4,5},{7,6},{6,7},{9,8},{8,9},{11,10... | collective-permute-start | bytes 3145736 | tf_op jit(solution)/shard_map/ppermute | solution.py:228
  44.9 0.1 pad_maximum_fusion.2
  45.0 4.0 %collective-permute-start.10 = (bf16[192,2048]{1,0:T(8,128)(2,1)S(1)}, bf16[192,2048]{1,0:T(8,128)(2,1)}, u32[]{:S(2)}, u32[]{:S(2)}) collective-permute-start(bf16[192,2048]{1,0:T(8,128)(2,1)S(1)} %pad_maximum_fusion.2), channel_id=1, source_target_pairs={{6,0},{0,2},{2,4},{4,6},{7,1},{1,3},{3,5},{5,7},{14,8},{8,10},{10,... | collective-permute-start | bytes 2359304 | tf_op jit(solution)/shard_map/ppermute | solution.py:228
  49.0 2.4 %collective-permute-start.8 = (bf16[192,2048]{1,0:T(8,128)(2,1)S(1)}, bf16[192,2048]{1,0:T(8,128)(2,1)}, u32[]{:S(2)}, u32[]{:S(2)}) collective-permute-start(bf16[192,2048]{1,0:T(8,128)(2,1)S(1)} %pad_maximum_fusion.2), channel_id=1, source_target_pairs={{2,0},{4,2},{6,4},{0,6},{3,1},{5,3},{7,5},{1,7},{10,8},{12,10},{14... | collective-permute-start | bytes 2359304 | tf_op jit(solution)/shard_map/ppermute | solution.py:228
  51.5 2.5 %collective-permute-start = (bf16[32,2048]{1,0:T(8,128)(2,1)S(1)}, bf16[32,2048]{1,0:T(8,128)(2,1)S(1)}, u32[]{:S(2)}, u32[]{:S(2)}) collective-permute-start(bf16[32,2048]{1,0:T(8,128)(2,1)S(1)} %copy-done.2), channel_id=1, source_target_pairs={{1,0},{0,1},{3,2},{2,3},{5,4},{4,5},{7,6},{6,7},{9,8},{8,9},{11,10... | collective-permute-start | bytes 393224 | tf_op jit(solution)/shard_map/ppermute | solution.py:228
  54.0 0.1 pad_add_fusion.place
  54.1 0.9 collective-permute-done.beside
  55.0 0.0 collective-permute-done.4.other
  55.0 1.6 %shard_map.100.refs_0_ = bf16[64,512]{1,0:T(8,128)(2,1)S(1)} custom-call(s32[2]{0:T(128)S(1)} %pad_add_fusion.place, bf16[32,2048]{1,0:T(8,128)(2,1)S(1)} %copy-done.2, bf16[32,2048]{1,0:T(8,128)(2,1)S(1)} %collective-permute-done.beside, f32[2,2048]{1,0:T(2,128)S(1)} %copy-done.3, f32[2,64]{1,0:T(2,128)S(1)} %copy-done.4, ...), custom_call_target="tpu_custom_call" | custom-call | flops 200000000 | bytes 1000000 | tf_op jit(solution)/shard_map/pallas_call | solution.py:209
  56.5 2.9 %collective-permute-start.7 = (bf16[64,512]{1,0:T(8,128)(2,1)S(1)}, bf16[64,512]{1,0:T(8,128)(2,1)S(1)}, u32[]{:S(2)}, u32[]{:S(2)}) collective-permute-start(bf16[64,512]{1,0:T(8,128)(2,1)S(1)} %shard_map.100.refs_0_), channel_id=1, source_target_pairs={{6,0},{0,2},{2,4},{4,6},{7,1},{1,3},{3,5},{5,7},{14,8},{8,10},{10,... | collective-permute-start | bytes 196616 | tf_op jit(solution)/shard_map/ppermute | solution.py:228
  59.5 3.2 %collective-permute-start.6 = (bf16[64,512]{1,0:T(8,128)(2,1)S(1)}, bf16[64,512]{1,0:T(8,128)(2,1)S(1)}, u32[]{:S(2)}, u32[]{:S(2)}) collective-permute-start(bf16[64,512]{1,0:T(8,128)(2,1)S(1)} %shard_map.100.refs_0_), channel_id=1, source_target_pairs={{4,0},{6,2},{0,4},{2,6},{5,1},{7,3},{1,5},{3,7},{12,8},{14,10},{8,... | collective-permute-start | bytes 196616 | tf_op jit(solution)/shard_map/ppermute | solution.py:228
  62.7 3.2 %collective-permute-start.5 = (bf16[64,512]{1,0:T(8,128)(2,1)S(1)}, bf16[64,512]{1,0:T(8,128)(2,1)S(1)}, u32[]{:S(2)}, u32[]{:S(2)}) collective-permute-start(bf16[64,512]{1,0:T(8,128)(2,1)S(1)} %shard_map.100.refs_0_), channel_id=1, source_target_pairs={{2,0},{4,2},{6,4},{0,6},{3,1},{5,3},{7,5},{1,7},{10,8},{12,10},{14... | collective-permute-start | bytes 196616 | tf_op jit(solution)/shard_map/ppermute | solution.py:228
  65.9 1.3 %collective-permute-done.10 = bf16[192,2048]{1,0:T(8,128)(2,1)} collective-permute-done((bf16[192,2048]{1,0:T(8,128)(2,1)S(1)}, bf16[192,2048]{1,0:T(8,128)(2,1)}, u32[]{:S(2)}, u32[]{:S(2)}) %collective-permute-start.10) | collective-permute-done | bytes 786464 | tf_op jit(solution)/shard_map/ppermute | solution.py:228
  67.3 1.0 slice.34
  68.3 2.7 %collective-permute-start.11 = (bf16[96,2048]{1,0:T(8,128)(2,1)S(1)}, bf16[96,2048]{1,0:T(8,128)(2,1)S(1)}, u32[]{:S(2)}, u32[]{:S(2)}) collective-permute-start(bf16[96,2048]{1,0:T(8,128)(2,1)S(1)} %slice.34), channel_id=1, source_target_pairs={{6,0},{0,2},{2,4},{4,6},{7,1},{1,3},{3,5},{5,7},{14,8},{8,10},{10,... | collective-permute-start | bytes 1179656 | tf_op jit(solution)/shard_map/ppermute | solution.py:228
  71.0 0.0 collective-permute-done.8
  71.0 1.0 slice.33
  72.1 3.8 %collective-permute-start.9 = (bf16[96,2048]{1,0:T(8,128)(2,1)S(1)}, bf16[96,2048]{1,0:T(8,128)(2,1)S(1)}, u32[]{:S(2)}, u32[]{:S(2)}) collective-permute-start(bf16[96,2048]{1,0:T(8,128)(2,1)S(1)} %slice.33), channel_id=1, source_target_pairs={{2,0},{4,2},{6,4},{0,6},{3,1},{5,3},{7,5},{1,7},{10,8},{12,10},{14... | collective-permute-start | bytes 1179656 | tf_op jit(solution)/shard_map/ppermute | solution.py:228
  75.9 0.0 collective-permute-done.5.refs_1_
  75.9 0.0 all-to-all-done.refs_4_.refs_1_
  75.9 5.2 %shard_map.102 = bf16[256,640]{1,0:T(8,128)(2,1)S(1)} custom-call(s32[2]{0:T(128)S(1)} %pad_add_fusion.place, bf16[64,512]{1,0:T(8,128)(2,1)S(1)} %shard_map.100.refs_0_, bf16[64,512]{1,0:T(8,128)(2,1)S(1)} %collective-permute-done.5.refs_1_, bf16[64,512]{1,0:T(8,128)(2,1)S(1)} %collective-permute-done.6.refs_2_, ...), custom_call_target="tpu_custom_call" | custom-call | flops 5000000000 | bytes 1000000 | tf_op jit(solution)/shard_map/pallas_call | solution.py:209
  81.1 0.0 collective-permute-done.11
  81.1 1.7 %collective-permute-done.9 = bf16[96,2048]{1,0:T(8,128)(2,1)S(1)} collective-permute-done((bf16[96,2048]{1,0:T(8,128)(2,1)S(1)}, bf16[96,2048]{1,0:T(8,128)(2,1)S(1)}, u32[]{:S(2)}, u32[]{:S(2)}) %collective-permute-start.9) | collective-permute-done | bytes 393248 | tf_op jit(solution)/shard_map/ppermute | solution.py:228
  82.8 0.1 maximum_bitcast_fusion
  82.9 1.6 %pad_maximum_fusion.out_mine.mine = bf16[4,192,2048]{2,1,0:T(8,128)(2,1)S(1)} fusion(bf16[1,192,2048]{2,1,0:T(8,128)(2,1)} %bitcast.14, bf16[1,192,2048]{2,1,0:T(8,128)(2,1)S(1)} %maximum_bitcast_fusion, bf16[1,192,2048]{2,1,0:T(8,128)(2,1)} %bitcast.12, bf16[1,192,2048]{2,1,0:T(8,128)(2,1)S(1)} %bitcast.23), kind=kLoop, calls=%fused_computation | loop fusion | flops 4718592 | bytes 6291456 | tf_op jit(solution)/shard_map/stack | solution.py:299
  84.4 4.6 %collective-permute-start.12 = (bf16[4,192,2048]{2,1,0:T(8,128)(2,1)S(1)}, bf16[4,192,2048]{2,1,0:T(8,128)(2,1)S(1)}, u32[]{:S(2)}, u32[]{:S(2)}) collective-permute-start(bf16[4,192,2048]{2,1,0:T(8,128)(2,1)S(1)} %pad_maximum_fusion.out_mine.mine), channel_id=1, source_target_pairs={{1,0},{0,1},{3,2},{2,3},{5,4},{4,5},{7,6},{6,7},{9,8},{8,9},{11,10... | collective-permute-start | bytes 9437192 | tf_op jit(solution)/shard_map/ppermute | solution.py:228
  89.1 2.3 %slice.30 = bf16[64,1,32,256]{3,2,1,0:T(8,128)(2,1)} slice(bf16[64,2,32,256]{3,2,1,0:T(8,128)(2,1)} %all-to-all-done.refs_4_.refs_1_), slice={[0:64], [1:2], [0:32], [0:256]} | slice | bytes 2097152 | tf_op jit(solution)/shard_map/slice | solution.py:301
  91.3 1.9 %collective-permute-start.13 = (bf16[64,1,32,256]{3,2,1,0:T(8,128)(2,1)}, bf16[64,1,32,256]{3,2,1,0:T(8,128)(2,1)}, u32[]{:S(2)}, u32[]{:S(2)}) collective-permute-start(bf16[64,1,32,256]{3,2,1,0:T(8,128)(2,1)} %slice.30), channel_id=1, source_target_pairs={{1,0},{0,1},{3,2},{2,3},{5,4},{4,5},{7,6},{6,7},{9,8},{8,9},{11,10... | collective-permute-start | bytes 3145736 | tf_op jit(solution)/shard_map/ppermute | solution.py:228
  93.2 12.4 %all_to_all.20.arrived = bf16[8,32,640]{2,1,0:T(8,128)(2,1)S(1)} all-to-all(bf16[8,32,640]{2,1,0:T(8,128)(2,1)S(1)} %bitcast.21), channel_id=1, replica_groups=mesh['z'=8,'y'=8,'x'=4,'c'=2] {'x','c'}, dimensions={0} | all-to-all | bytes 655360 | tf_op jit(solution)/shard_map/all_to_all | solution.py:294
  105.6 2.1 %shard_map.103 = (bf16[32,2048]{1,0:T(8,128)(2,1)S(1)}, bf16[32,512]{1,0:T(8,128)(2,1)S(1)}) custom-call(s32[2]{0:T(128)S(1)} %pad_add_fusion.place, bf16[8,32,640]{2,1,0:T(8,128)(2,1)S(1)} %all_to_all.20.arrived, bf16[32,2048]{1,0:T(8,128)(2,1)S(1)} %copy-done.2, f32[2,2048]{1,0:T(2,128)S(1)} %copy-done.3, f32[2,64]{1,0:T(2,128)S(1)} %copy-done.4, ...), custom_call_target="tpu_custom_call" | custom-call | flops 400000000 | bytes 1000000 | tf_op jit(solution)/shard_map/pallas_call | solution.py:209
  107.8 0.7 broadcast_in_dim.7
  108.5 3.5 %all-to-all-start.2 = ((bf16[4,32,512]{2,1,0:T(8,128)(2,1)}), bf16[4,32,512]{2,1,0:T(8,128)(2,1)S(1)}, u32[]{:S(2)}, u32[]{:S(2)}) async-start(bf16[4,32,512]{2,1,0:T(8,128)(2,1)} %broadcast_in_dim.7), calls=%async_computation.2 | async-start | bytes 262144 | tf_op jit(solution)/shard_map/all_to_all | solution.py:223
  112.0 4.6 %all-to-all-done.2.refs_0_ = bf16[4,32,512]{2,1,0:T(8,128)(2,1)S(1)} async-done(((bf16[4,32,512]{2,1,0:T(8,128)(2,1)}), bf16[4,32,512]{2,1,0:T(8,128)(2,1)S(1)}, u32[]{:S(2)}, u32[]{:S(2)}) %all-to-all-start.2) | async-done | bytes 131104 | tf_op jit(solution)/shard_map/all_to_all | solution.py:223
  116.6 6.1 %shard_map.104 = bf16[128,640]{1,0:T(8,128)(2,1)S(1)} custom-call(s32[2]{0:T(128)S(1)} %pad_add_fusion.place, bf16[4,32,512]{2,1,0:T(8,128)(2,1)S(1)} %all-to-all-done.2.refs_0_, bf16[64,2,32,256]{3,2,1,0:T(8,128)(2,1)} %all-to-all-done.refs_4_.refs_1_, bf16[64,1,32,256]{3,2,1,0:T(8,128)(2,1)} %collective-permute-done.13.refs_2_), custom_call_target="tpu_custom_call" | custom-call | flops 5000000000 | bytes 1000000 | tf_op jit(solution)/shard_map/pallas_call | solution.py:209
  122.7 7.4 %all_to_all.21.arrived = bf16[4,32,640]{2,1,0:T(8,128)(2,1)S(1)} all-to-all(bf16[4,32,640]{2,1,0:T(8,128)(2,1)S(1)} %bitcast.22), channel_id=1, replica_groups=mesh['z'=8,'y'=8,'x'=4,'c'=2] {'x'}, dimensions={0} | all-to-all | bytes 327680 | tf_op jit(solution)/shard_map/all_to_all | solution.py:294
  130.0 1.9 %shard_map.105 = bf16[32,2048]{1,0:T(8,128)(2,1)} custom-call(s32[2]{0:T(128)S(1)} %pad_add_fusion.place, bf16[4,32,640]{2,1,0:T(8,128)(2,1)S(1)} %all_to_all.21.arrived, bf16[32,2048]{1,0:T(8,128)(2,1)S(1)} %get-tuple-element.20.hidden, bf16[4,192,2048]{2,1,0:T(8,128)(2,1)S(1)} %pad_maximum_fusion.out_mine.mine, bf16[4,192,2048]{2,1,0:T(8,128)(2,1)S(1)} %copy-done.1), custom_call_target="tpu_custom_call" | custom-call | flops 200000000 | bytes 1000000 | tf_op jit(solution)/shard_map/pallas_call | solution.py:209
  (22 shorter events, 0.1 us)
Async XLA Ops:
  5.1 17.5 %copy-start.7 = (bf16[2,2048,64]{1,2,0:T(8,128)(2,1)S(1)}, bf16[2,2048,64]{1,2,0:T(8,128)(2,1)}, u32[]{:S(2)}) copy-start(bf16[2,2048,64]{1,2,0:T(8,128)(2,1)} %param.16) | copy-start | bytes 1572868
  5.1 70.8 %all-to-all-start = ((bf16[64,2,32,256]{3,2,1,0:T(8,128)(2,1)}), bf16[64,2,32,256]{3,2,1,0:T(8,128)(2,1)}, u32[]{:S(2)}, u32[]{:S(2)}) async-start(bf16[64,2,32,256]{3,2,1,0:T(8,128)(2,1)} %broadcast_in_dim.6), calls=%async_computation | async-start | bytes 4194304 | tf_op jit(solution)/shard_map/all_to_all | solution.py:223
  22.6 22.2 %copy-start.8 = (bf16[2,64,2048]{2,1,0:T(8,128)(2,1)S(1)}, bf16[2,64,2048]{2,1,0:T(8,128)(2,1)}, u32[]{:S(2)}) copy-start(bf16[2,64,2048]{2,1,0:T(8,128)(2,1)} %param.19) | copy-start | bytes 1572868
  22.7 10.7 %collective-permute-start.3 = (bf16[64,2048]{1,0:T(8,128)(2,1)S(1)}, bf16[64,2048]{1,0:T(8,128)(2,1)S(1)}, u32[]{:S(2)}, u32[]{:S(2)}) collective-permute-start(bf16[64,2048]{1,0:T(8,128)(2,1)S(1)} %get-tuple-element.24), channel_id=1, source_target_pairs={{6,0},{0,2},{2,4},{4,6},{7,1},{1,3},{3,5},{5,7},{14,8},{8,10},{10,... | collective-permute-start | bytes 786440 | tf_op jit(solution)/shard_map/ppermute | solution.py:228
  26.0 13.6 %collective-permute-start.2 = (bf16[64,2048]{1,0:T(8,128)(2,1)S(1)}, bf16[64,2048]{1,0:T(8,128)(2,1)S(1)}, u32[]{:S(2)}, u32[]{:S(2)}) collective-permute-start(bf16[64,2048]{1,0:T(8,128)(2,1)S(1)} %get-tuple-element.24), channel_id=1, source_target_pairs={{4,0},{6,2},{0,4},{2,6},{5,1},{7,3},{1,5},{3,7},{12,8},{14,10},{8,... | collective-permute-start | bytes 786440 | tf_op jit(solution)/shard_map/ppermute | solution.py:228
  30.4 10.5 %collective-permute-start.1 = (bf16[64,2048]{1,0:T(8,128)(2,1)S(1)}, bf16[64,2048]{1,0:T(8,128)(2,1)S(1)}, u32[]{:S(2)}, u32[]{:S(2)}) collective-permute-start(bf16[64,2048]{1,0:T(8,128)(2,1)S(1)} %get-tuple-element.24), channel_id=1, source_target_pairs={{2,0},{4,2},{6,4},{0,6},{3,1},{5,3},{7,5},{1,7},{10,8},{12,10},{14... | collective-permute-start | bytes 786440 | tf_op jit(solution)/shard_map/ppermute | solution.py:228
  40.8 10.7 %copy-start.2 = (bf16[32,2048]{1,0:T(8,128)(2,1)S(1)}, bf16[32,2048]{1,0:T(8,128)(2,1)}, u32[]{:S(2)}) copy-start(bf16[32,2048]{1,0:T(8,128)(2,1)} %hidden.1) | copy-start | bytes 393220
  40.8 14.1 %copy-start.3 = (f32[2,2048]{1,0:T(2,128)S(1)}, f32[2,2048]{1,0:T(2,128)}, u32[]{:S(2)}) copy-start(f32[2,2048]{1,0:T(2,128)} %gain.5) | copy-start | bytes 49156
  40.8 14.1 %copy-start.4 = (f32[2,64]{1,0:T(2,128)S(1)}, f32[2,64]{1,0:T(2,128)}, u32[]{:S(2)}) copy-start(f32[2,64]{1,0:T(2,128)} %query_gain.3) | copy-start | bytes 1540
  41.0 14.0 %collective-permute-start.4 = (bf16[4,64,2048]{2,1,0:T(8,128)(2,1)S(1)}, bf16[4,64,2048]{2,1,0:T(8,128)(2,1)S(1)}, u32[]{:S(2)}, u32[]{:S(2)}) collective-permute-start(bf16[4,64,2048]{2,1,0:T(8,128)(2,1)S(1)} %pad_maximum_fusion.1.mine), channel_id=1, source_target_pairs={{1,0},{0,1},{3,2},{2,3},{5,4},{4,5},{7,6},{6,7},{9,8},{8,9},{11,10... | collective-permute-start | bytes 3145736 | tf_op jit(solution)/shard_map/ppermute | solution.py:228
  45.0 36.1 %copy-start.5 = (bf16[192,2048]{1,0:T(8,128)(2,1)}, bf16[192,2048]{1,0:T(8,128)(2,1)S(1)}, u32[]{:S(2)}) copy-start(bf16[192,2048]{1,0:T(8,128)(2,1)S(1)} %pad_maximum_fusion.2) | copy-start | bytes 2359300
  45.0 22.3 %collective-permute-start.10 = (bf16[192,2048]{1,0:T(8,128)(2,1)S(1)}, bf16[192,2048]{1,0:T(8,128)(2,1)}, u32[]{:S(2)}, u32[]{:S(2)}) collective-permute-start(bf16[192,2048]{1,0:T(8,128)(2,1)S(1)} %pad_maximum_fusion.2), channel_id=1, source_target_pairs={{6,0},{0,2},{2,4},{4,6},{7,1},{1,3},{3,5},{5,7},{14,8},{8,10},{10,... | collective-permute-start | bytes 2359304 | tf_op jit(solution)/shard_map/ppermute | solution.py:228
  49.0 22.0 %collective-permute-start.8 = (bf16[192,2048]{1,0:T(8,128)(2,1)S(1)}, bf16[192,2048]{1,0:T(8,128)(2,1)}, u32[]{:S(2)}, u32[]{:S(2)}) collective-permute-start(bf16[192,2048]{1,0:T(8,128)(2,1)S(1)} %pad_maximum_fusion.2), channel_id=1, source_target_pairs={{2,0},{4,2},{6,4},{0,6},{3,1},{5,3},{7,5},{1,7},{10,8},{12,10},{14... | collective-permute-start | bytes 2359304 | tf_op jit(solution)/shard_map/ppermute | solution.py:228
  51.5 3.5 %collective-permute-start = (bf16[32,2048]{1,0:T(8,128)(2,1)S(1)}, bf16[32,2048]{1,0:T(8,128)(2,1)S(1)}, u32[]{:S(2)}, u32[]{:S(2)}) collective-permute-start(bf16[32,2048]{1,0:T(8,128)(2,1)S(1)} %copy-done.2), channel_id=1, source_target_pairs={{1,0},{0,1},{3,2},{2,3},{5,4},{4,5},{7,6},{6,7},{9,8},{8,9},{11,10... | collective-permute-start | bytes 393224 | tf_op jit(solution)/shard_map/ppermute | solution.py:228
  56.5 19.3 %collective-permute-start.7 = (bf16[64,512]{1,0:T(8,128)(2,1)S(1)}, bf16[64,512]{1,0:T(8,128)(2,1)S(1)}, u32[]{:S(2)}, u32[]{:S(2)}) collective-permute-start(bf16[64,512]{1,0:T(8,128)(2,1)S(1)} %shard_map.100.refs_0_), channel_id=1, source_target_pairs={{6,0},{0,2},{2,4},{4,6},{7,1},{1,3},{3,5},{5,7},{14,8},{8,10},{10,... | collective-permute-start | bytes 196616 | tf_op jit(solution)/shard_map/ppermute | solution.py:228
  59.5 16.4 %collective-permute-start.6 = (bf16[64,512]{1,0:T(8,128)(2,1)S(1)}, bf16[64,512]{1,0:T(8,128)(2,1)S(1)}, u32[]{:S(2)}, u32[]{:S(2)}) collective-permute-start(bf16[64,512]{1,0:T(8,128)(2,1)S(1)} %shard_map.100.refs_0_), channel_id=1, source_target_pairs={{4,0},{6,2},{0,4},{2,6},{5,1},{7,3},{1,5},{3,7},{12,8},{14,10},{8,... | collective-permute-start | bytes 196616 | tf_op jit(solution)/shard_map/ppermute | solution.py:228
  62.7 13.1 %collective-permute-start.5 = (bf16[64,512]{1,0:T(8,128)(2,1)S(1)}, bf16[64,512]{1,0:T(8,128)(2,1)S(1)}, u32[]{:S(2)}, u32[]{:S(2)}) collective-permute-start(bf16[64,512]{1,0:T(8,128)(2,1)S(1)} %shard_map.100.refs_0_), channel_id=1, source_target_pairs={{2,0},{4,2},{6,4},{0,6},{3,1},{5,3},{7,5},{1,7},{10,8},{12,10},{14... | collective-permute-start | bytes 196616 | tf_op jit(solution)/shard_map/ppermute | solution.py:228
  68.3 12.8 %collective-permute-start.11 = (bf16[96,2048]{1,0:T(8,128)(2,1)S(1)}, bf16[96,2048]{1,0:T(8,128)(2,1)S(1)}, u32[]{:S(2)}, u32[]{:S(2)}) collective-permute-start(bf16[96,2048]{1,0:T(8,128)(2,1)S(1)} %slice.34), channel_id=1, source_target_pairs={{6,0},{0,2},{2,4},{4,6},{7,1},{1,3},{3,5},{5,7},{14,8},{8,10},{10,... | collective-permute-start | bytes 1179656 | tf_op jit(solution)/shard_map/ppermute | solution.py:228
  72.1 10.7 %collective-permute-start.9 = (bf16[96,2048]{1,0:T(8,128)(2,1)S(1)}, bf16[96,2048]{1,0:T(8,128)(2,1)S(1)}, u32[]{:S(2)}, u32[]{:S(2)}) collective-permute-start(bf16[96,2048]{1,0:T(8,128)(2,1)S(1)} %slice.33), channel_id=1, source_target_pairs={{2,0},{4,2},{6,4},{0,6},{3,1},{5,3},{7,5},{1,7},{10,8},{12,10},{14... | collective-permute-start | bytes 1179656 | tf_op jit(solution)/shard_map/ppermute | solution.py:228
  81.1 1.7 %copy-start.6 = (bf16[192,2048]{1,0:T(8,128)(2,1)S(1)}, bf16[192,2048]{1,0:T(8,128)(2,1)}, u32[]{:S(2)}) copy-start(bf16[192,2048]{1,0:T(8,128)(2,1)} %copy-done.5) | copy-start | bytes 2359300
  84.4 21.2 %collective-permute-start.12 = (bf16[4,192,2048]{2,1,0:T(8,128)(2,1)S(1)}, bf16[4,192,2048]{2,1,0:T(8,128)(2,1)S(1)}, u32[]{:S(2)}, u32[]{:S(2)}) collective-permute-start(bf16[4,192,2048]{2,1,0:T(8,128)(2,1)S(1)} %pad_maximum_fusion.out_mine.mine), channel_id=1, source_target_pairs={{1,0},{0,1},{3,2},{2,3},{5,4},{4,5},{7,6},{6,7},{9,8},{8,9},{11,10... | collective-permute-start | bytes 9437192 | tf_op jit(solution)/shard_map/ppermute | solution.py:228
  91.3 20.7 %collective-permute-start.13 = (bf16[64,1,32,256]{3,2,1,0:T(8,128)(2,1)}, bf16[64,1,32,256]{3,2,1,0:T(8,128)(2,1)}, u32[]{:S(2)}, u32[]{:S(2)}) collective-permute-start(bf16[64,1,32,256]{3,2,1,0:T(8,128)(2,1)} %slice.30), channel_id=1, source_target_pairs={{1,0},{0,1},{3,2},{2,3},{5,4},{4,5},{7,6},{6,7},{9,8},{8,9},{11,10... | collective-permute-start | bytes 3145736 | tf_op jit(solution)/shard_map/ppermute | solution.py:228
  105.6 2.2 %copy-start = (bf16[4,192,2048]{2,1,0:T(8,128)(2,1)}, bf16[4,192,2048]{2,1,0:T(8,128)(2,1)S(1)}, u32[]{:S(2)}) copy-start(bf16[4,192,2048]{2,1,0:T(8,128)(2,1)S(1)} %collective-permute-done.12.out_other.other) | copy-start | bytes 9437188
  108.5 8.1 %all-to-all-start.2 = ((bf16[4,32,512]{2,1,0:T(8,128)(2,1)}), bf16[4,32,512]{2,1,0:T(8,128)(2,1)S(1)}, u32[]{:S(2)}, u32[]{:S(2)}) async-start(bf16[4,32,512]{2,1,0:T(8,128)(2,1)} %broadcast_in_dim.7), calls=%async_computation.2 | async-start | bytes 262144 | tf_op jit(solution)/shard_map/all_to_all | solution.py:223
  116.6 13.4 %copy-start.1 = (bf16[4,192,2048]{2,1,0:T(8,128)(2,1)S(1)}, bf16[4,192,2048]{2,1,0:T(8,128)(2,1)}, u32[]{:S(2)}) copy-start(bf16[4,192,2048]{2,1,0:T(8,128)(2,1)} %copy-done) | copy-start | bytes 9437188

commit v5 on v4

--- a/solution.py
+++ b/solution.py
@@ -58,8 +58,11 @@
         row = doubled(key_gain[layer : layer + 1, :])
         groups = head_norm(keys, row, head)
         for k, group in enumerate(groups):
-            out[layer, :, k * 2 * head : (k + 1) * 2 * head] = group.astype(BF16)
-        out[layer, :, width:] = dot(normed, value_weight[layer]).astype(BF16)
+            out[0, layer, :, k * 2 * head : (k + 1) * 2 * head] = group.astype(BF16)
+        out[0, layer, :, width:] = dot(normed, value_weight[layer]).astype(BF16)
+    result = out[0]
+    for k in range(1, out.shape[0]):
+        out[k] = result
 
 
 def project(normed, mine, other, row, head, place):
@@ -121,7 +124,9 @@
     value = now.astype(F32)
     normed = (value * rms(value) * gain[layer : layer + 1, :]).astype(BF16)
     row = doubled(query_gain[layer : layer + 1, :])
-    store_groups(out, project(normed, mine[...], other[...], row, head, place))
+    halves = project(normed, mine[...], other[...], row, head, place)
+    for copy in range(out.shape[0]):
+        store_groups(out.at[copy], halves)
 
 
 def last_kernel(heads, head, place, arrived, hidden, out_mine, out_other, hidden_out):
@@ -218,11 +223,6 @@
     )(*placed, *rest, *(part[0] for part in parts))
 
 
-def to_all(value, axis):
-    copies = jnp.broadcast_to(value, (lax.axis_size(axis), *value.shape))
-    return lax.all_to_all(copies, axis, split_axis=0, concat_axis=0, tiled=True)
-
-
 def shifted(value, axis, step):
     size = lax.axis_size(axis)
     return lax.ppermute(value, axis, [((k + step) % size, k) for k in range(size)])
@@ -249,13 +249,13 @@
 
     pairs = with_place(
         source_kernel,
-        shapes((layers, rows, 4 * head), BF16),
+        shapes((lax.axis_size(ROWS), layers, rows, 4 * head), BF16),
         (None, source, source_gain, key_gain, key_weight, value_weight),
         [],
         200000000,
         limit=63,
     )
-    plane = to_all(pairs, ROWS)
+    plane = lax.all_to_all(pairs, ROWS, split_axis=0, concat_axis=0, tiled=True)
     keys = plane.shape[0] * rows
 
     def both(stacked):
@@ -298,16 +298,18 @@
     far = jnp.concatenate(pieces[2:4], axis=0)
     rest = both(jnp.stack([pieces[0], pieces[1], far, pieces[4]]))
     rest = [[(part, k, head) for part in rest] for k in range(3)]
-    shared = shifted(second[:, 1:2], "c", 1)
+    shared = shifted(second, "c", 1)
     arrived = returned(partial, TP)
     hidden, queries = with_place(
         functools.partial(middle_kernel, 1, heads),
-        [shapes((rows, model), BF16), shapes((rows, width), BF16)],
+        [shapes((rows, model), BF16), shapes((lax.axis_size("x"), rows, width), BF16)],
         (place, arrived, target, target_gain, query_gain),
         rest[0] + rest[1],
         400000000,
-    )
-    partial = attend([to_all(queries, "x")], [(plane, 1, 1), (shared, 0, 1)], lax.axis_size("x"))
+        limit=56,
+    )
+    everyone = lax.all_to_all(queries, "x", split_axis=0, concat_axis=0, tiled=True)
+    partial = attend([everyone], [(plane, 1, 1), (shared, 1, 1)], lax.axis_size("x"))
     return with_place(
         functools.partial(last_kernel, heads, head),
         shapes((rows, model), BF16),

time: 134 us -> 139 us (1.037)
  waiting for transfers between devices: 15.9 us -> 24.2 us
  starting transfers between devices: 66.9 us -> 62 us
  local copies, waits for them, and re-layouts: 7.47 us -> 3.88 us
  Pallas kernels: 19.6 us -> 23.1 us
    ppermute x14, waiting for transfers between devices: 11.3 us -> 19.6 us  [shifted(): lax.ppermute(value, axis, [((k + step) % size, k) for k in range(size)])]
    ppermute x14, starting transfers between devices: 45.9 us -> 41 us  [shifted(): lax.ppermute(value, axis, [((k + step) % size, k) for k in range(size)])]
    pallas_call x6, Pallas kernels: 19.6 us -> 23.1 us  [with_place(): pl.pallas_call(kernel, grid=(1,), out_shape=shapes, in_specs=specs, out_s...]
    broadcast_in_dim x2 -> x0, local copies, waits for them, and re-layouts: 3.02 us -> none  [to_all(): copies = jnp.broadcast_to(value, (lax.axis_size(axis), *value.shape))]
    slice x1 -> x0, local copies, waits for them, and re-layouts: 2.26 us -> none  [decoder(): shared = shifted(second[:, 1:2], 'c', 1)]
    unnamed x18 -> x24, local copies, waits for them, and re-layouts: 0.04 us -> 1.72 us
  transfers between devices with their start and end apart: 16 -> 16, of which waited for: 6 -> 7; matrix products, arithmetic and copies ran while one was open for 4% -> 2% of each run, Pallas kernels for 7% -> 8%
where the time goes in v5:
time: 139 us; the launch traced here: 137 us
  starting transfers between devices  62 us (45%)
  waiting for transfers between devices  24.2 us (17%)
  Pallas kernels  23.1 us (17%)
  blocking collectives  20.2 us (15%)
  local copies, waits for them, and re-layouts  3.88 us (3%)
  other arithmetic  3.01 us (2%)
    ppermute x14, starting transfers between devices, shifted(): lax.ppermute(value, axis, [((k + step) % size, k) for k in range(size)])  41 us
    pallas_call x6, Pallas kernels, with_place(): pl.pallas_call(kernel, grid=(1,), out_shape=shapes, in_specs=specs, out_s...  23.1 us
    all_to_all x2, blocking collectives, returned(): lax.all_to_all(partial.reshape(-1, rows, wide), axis, split_axis=0, conca...  20.2 us
    ppermute x14, waiting for transfers between devices, shifted(): lax.ppermute(value, axis, [((k + step) % size, k) for k in range(size)])  19.6 us
    all_to_all x1, starting transfers between devices, decoder(): plane = lax.all_to_all(pairs, ROWS, split_axis=0, concat_axis=0, tiled=True)  17.5 us
    all_to_all x1, waiting for transfers between devices, decoder(): lax.all_to_all(queries, 'x', split_axis=0, concat_axis=0, tiled=True)  4.59 us
    all_to_all x1, starting transfers between devices, decoder(): lax.all_to_all(queries, 'x', split_axis=0, concat_axis=0, tiled=True)  3.5 us
  transfers between devices with their start and end apart: 16, of which 7 were waited for; matrix products, arithmetic and copies ran while one was open for 2% of the time, Pallas kernels for 8%

profile of v5, /device:TPU:1, one launch (start us, length us, event | category | flops | bytes accessed | tf_op | source)
XLA Modules:
  0.0 136.7 jit_solution(16581661573249314183)
XLA Ops:
  0.0 3.7 %shard_map.101 = bf16[64,2,32,256]{3,2,1,0:T(8,128)(2,1)} custom-call(bf16[32,2048]{1,0:T(8,128)(2,1)} %source.1, f32[2,2048]{1,0:T(2,128)} %gain.4, f32[2,64]{1,0:T(2,128)} %key_gain.1, bf16[2,2048,128]{2,1,0:T(8,128)(2,1)} %key_weight.1, bf16[2,2048,128]{2,1,0:T(8,128)(2,1)} %value_weight.1), custom_call_target="tpu_custom_call" | custom-call | flops 200000000 | bytes 1000000 | tf_op jit(solution)/shard_map/pallas_call | solution.py:214
  3.7 17.5 %all-to-all-start = ((bf16[64,2,32,256]{3,2,1,0:T(8,128)(2,1)}), bf16[64,2,32,256]{3,2,1,0:T(8,128)(2,1)}, u32[]{:S(2)}, u32[]{:S(2)}) async-start(bf16[64,2,32,256]{3,2,1,0:T(8,128)(2,1)} %shard_map.101), calls=%async_computation | async-start | bytes 4194304 | tf_op jit(solution)/shard_map/all_to_all | solution.py:258
  21.2 0.0 copy-start.11
  21.3 0.1 slice_bitcast_fusion
  21.3 4.5 %collective-permute-start.1 = (bf16[64,2048]{1,0:T(8,128)(2,1)S(1)}, bf16[64,2048]{1,0:T(8,128)(2,1)S(1)}, u32[]{:S(2)}, u32[]{:S(2)}) collective-permute-start(bf16[64,2048]{1,0:T(8,128)(2,1)S(1)} %get-tuple-element.24), channel_id=1, source_target_pairs={{2,0},{4,2},{6,4},{0,6},{3,1},{5,3},{7,5},{1,7},{10,8},{12,10},{14... | collective-permute-start | bytes 786440 | tf_op jit(solution)/shard_map/ppermute | solution.py:228
  25.9 2.4 %collective-permute-start.2 = (bf16[64,2048]{1,0:T(8,128)(2,1)S(1)}, bf16[64,2048]{1,0:T(8,128)(2,1)S(1)}, u32[]{:S(2)}, u32[]{:S(2)}) collective-permute-start(bf16[64,2048]{1,0:T(8,128)(2,1)S(1)} %get-tuple-element.24), channel_id=1, source_target_pairs={{4,0},{6,2},{0,4},{2,6},{5,1},{7,3},{1,5},{3,7},{12,8},{14,10},{8,... | collective-permute-start | bytes 786440 | tf_op jit(solution)/shard_map/ppermute | solution.py:228
  28.3 2.5 %collective-permute-start.3 = (bf16[64,2048]{1,0:T(8,128)(2,1)S(1)}, bf16[64,2048]{1,0:T(8,128)(2,1)S(1)}, u32[]{:S(2)}, u32[]{:S(2)}) collective-permute-start(bf16[64,2048]{1,0:T(8,128)(2,1)S(1)} %get-tuple-element.24), channel_id=1, source_target_pairs={{6,0},{0,2},{2,4},{4,6},{7,1},{1,3},{3,5},{5,7},{14,8},{8,10},{10,... | collective-permute-start | bytes 786440 | tf_op jit(solution)/shard_map/ppermute | solution.py:228
  30.8 0.5 collective-permute-done.1
  31.4 4.7 %collective-permute-done.2 = bf16[64,2048]{1,0:T(8,128)(2,1)S(1)} collective-permute-done((bf16[64,2048]{1,0:T(8,128)(2,1)S(1)}, bf16[64,2048]{1,0:T(8,128)(2,1)S(1)}, u32[]{:S(2)}, u32[]{:S(2)}) %collective-permute-start.2) | collective-permute-done | bytes 262176 | tf_op jit(solution)/shard_map/ppermute | solution.py:228
  36.0 7.2 %collective-permute-done.3 = bf16[64,2048]{1,0:T(8,128)(2,1)S(1)} collective-permute-done((bf16[64,2048]{1,0:T(8,128)(2,1)S(1)}, bf16[64,2048]{1,0:T(8,128)(2,1)S(1)}, u32[]{:S(2)}, u32[]{:S(2)}) %collective-permute-start.3) | collective-permute-done | bytes 262176 | tf_op jit(solution)/shard_map/ppermute | solution.py:228
  43.2 0.1 pad_maximum_fusion.1.mine
  43.3 2.3 %collective-permute-start.4 = (bf16[4,64,2048]{2,1,0:T(8,128)(2,1)S(1)}, bf16[4,64,2048]{2,1,0:T(8,128)(2,1)S(1)}, u32[]{:S(2)}, u32[]{:S(2)}) collective-permute-start(bf16[4,64,2048]{2,1,0:T(8,128)(2,1)S(1)} %pad_maximum_fusion.1.mine), channel_id=1, source_target_pairs={{1,0},{0,1},{3,2},{2,3},{5,4},{4,5},{7,6},{6,7},{9,8},{8,9},{11,10... | collective-permute-start | bytes 3145736 | tf_op jit(solution)/shard_map/ppermute | solution.py:228
  45.7 0.9 pad_maximum_fusion.2
  46.7 1.9 %collective-permute-start.10 = (bf16[192,2048]{1,0:T(8,128)(2,1)}, bf16[192,2048]{1,0:T(8,128)(2,1)}, u32[]{:S(2)}, u32[]{:S(2)}) collective-permute-start(bf16[192,2048]{1,0:T(8,128)(2,1)} %pad_maximum_fusion.2), channel_id=1, source_target_pairs={{6,0},{0,2},{2,4},{4,6},{7,1},{1,3},{3,5},{5,7},{14,8},{8,10},{10,... | collective-permute-start | bytes 2359304 | tf_op jit(solution)/shard_map/ppermute | solution.py:228
  48.6 4.6 %collective-permute-start.8 = (bf16[192,2048]{1,0:T(8,128)(2,1)}, bf16[192,2048]{1,0:T(8,128)(2,1)}, u32[]{:S(2)}, u32[]{:S(2)}) collective-permute-start(bf16[192,2048]{1,0:T(8,128)(2,1)} %pad_maximum_fusion.2), channel_id=1, source_target_pairs={{2,0},{4,2},{6,4},{0,6},{3,1},{5,3},{7,5},{1,7},{10,8},{12,10},{14... | collective-permute-start | bytes 2359304 | tf_op jit(solution)/shard_map/ppermute | solution.py:228
  53.2 2.6 %collective-permute-start = (bf16[32,2048]{1,0:T(8,128)(2,1)S(1)}, bf16[32,2048]{1,0:T(8,128)(2,1)S(1)}, u32[]{:S(2)}, u32[]{:S(2)}) collective-permute-start(bf16[32,2048]{1,0:T(8,128)(2,1)S(1)} %copy-done.4), channel_id=1, source_target_pairs={{1,0},{0,1},{3,2},{2,3},{5,4},{4,5},{7,6},{6,7},{9,8},{8,9},{11,10... | collective-permute-start | bytes 393224 | tf_op jit(solution)/shard_map/ppermute | solution.py:228
  55.8 0.1 pad_add_fusion.place
  55.8 0.9 collective-permute-done.beside
  56.7 0.0 collective-permute-done.4.other
  56.7 1.6 %shard_map.100.refs_0_ = bf16[64,512]{1,0:T(8,128)(2,1)S(1)} custom-call(s32[2]{0:T(128)S(1)} %pad_add_fusion.place, bf16[32,2048]{1,0:T(8,128)(2,1)S(1)} %copy-done.4, bf16[32,2048]{1,0:T(8,128)(2,1)S(1)} %collective-permute-done.beside, f32[2,2048]{1,0:T(2,128)S(1)} %copy-done.6, f32[2,64]{1,0:T(2,128)S(1)} %copy-done.9, ...), custom_call_target="tpu_custom_call" | custom-call | flops 200000000 | bytes 1000000 | tf_op jit(solution)/shard_map/pallas_call | solution.py:214
  58.3 1.9 %collective-permute-start.5 = (bf16[64,512]{1,0:T(8,128)(2,1)S(1)}, bf16[64,512]{1,0:T(8,128)(2,1)S(1)}, u32[]{:S(2)}, u32[]{:S(2)}) collective-permute-start(bf16[64,512]{1,0:T(8,128)(2,1)S(1)} %shard_map.100.refs_0_), channel_id=1, source_target_pairs={{2,0},{4,2},{6,4},{0,6},{3,1},{5,3},{7,5},{1,7},{10,8},{12,10},{14... | collective-permute-start | bytes 196616 | tf_op jit(solution)/shard_map/ppermute | solution.py:228
  60.2 2.2 %collective-permute-start.6 = (bf16[64,512]{1,0:T(8,128)(2,1)S(1)}, bf16[64,512]{1,0:T(8,128)(2,1)S(1)}, u32[]{:S(2)}, u32[]{:S(2)}) collective-permute-start(bf16[64,512]{1,0:T(8,128)(2,1)S(1)} %shard_map.100.refs_0_), channel_id=1, source_target_pairs={{4,0},{6,2},{0,4},{2,6},{5,1},{7,3},{1,5},{3,7},{12,8},{14,10},{8,... | collective-permute-start | bytes 196616 | tf_op jit(solution)/shard_map/ppermute | solution.py:228
  62.4 3.1 %collective-permute-start.7 = (bf16[64,512]{1,0:T(8,128)(2,1)S(1)}, bf16[64,512]{1,0:T(8,128)(2,1)S(1)}, u32[]{:S(2)}, u32[]{:S(2)}) collective-permute-start(bf16[64,512]{1,0:T(8,128)(2,1)S(1)} %shard_map.100.refs_0_), channel_id=1, source_target_pairs={{6,0},{0,2},{2,4},{4,6},{7,1},{1,3},{3,5},{5,7},{14,8},{8,10},{10,... | collective-permute-start | bytes 196616 | tf_op jit(solution)/shard_map/ppermute | solution.py:228
  65.5 4.9 %collective-permute-done.10 = bf16[192,2048]{1,0:T(8,128)(2,1)} collective-permute-done((bf16[192,2048]{1,0:T(8,128)(2,1)}, bf16[192,2048]{1,0:T(8,128)(2,1)}, u32[]{:S(2)}, u32[]{:S(2)}) %collective-permute-start.10) | collective-permute-done | bytes 786464 | tf_op jit(solution)/shard_map/ppermute | solution.py:228
  70.5 1.0 slice.30
  71.5 1.9 %collective-permute-start.11 = (bf16[96,2048]{1,0:T(8,128)(2,1)S(1)}, bf16[96,2048]{1,0:T(8,128)(2,1)S(1)}, u32[]{:S(2)}, u32[]{:S(2)}) collective-permute-start(bf16[96,2048]{1,0:T(8,128)(2,1)S(1)} %slice.30), channel_id=1, source_target_pairs={{6,0},{0,2},{2,4},{4,6},{7,1},{1,3},{3,5},{5,7},{14,8},{8,10},{10,... | collective-permute-start | bytes 1179656 | tf_op jit(solution)/shard_map/ppermute | solution.py:228
  73.4 0.0 collective-permute-done.8
  73.4 1.0 slice.29
  74.5 4.6 %collective-permute-start.9 = (bf16[96,2048]{1,0:T(8,128)(2,1)S(1)}, bf16[96,2048]{1,0:T(8,128)(2,1)S(1)}, u32[]{:S(2)}, u32[]{:S(2)}) collective-permute-start(bf16[96,2048]{1,0:T(8,128)(2,1)S(1)} %slice.29), channel_id=1, source_target_pairs={{2,0},{4,2},{6,4},{0,6},{3,1},{5,3},{7,5},{1,7},{10,8},{12,10},{14... | collective-permute-start | bytes 1179656 | tf_op jit(solution)/shard_map/ppermute | solution.py:228
  79.0 0.0 collective-permute-done.5.refs_1_
  79.1 0.0 collective-permute-done.6.refs_2_
  79.1 0.0 all-to-all-done.refs_4_.refs_1_
  79.1 5.2 %shard_map.102 = bf16[256,640]{1,0:T(8,128)(2,1)S(1)} custom-call(s32[2]{0:T(128)S(1)} %pad_add_fusion.place, bf16[64,512]{1,0:T(8,128)(2,1)S(1)} %shard_map.100.refs_0_, bf16[64,512]{1,0:T(8,128)(2,1)S(1)} %collective-permute-done.5.refs_1_, bf16[64,512]{1,0:T(8,128)(2,1)S(1)} %collective-permute-done.6.refs_2_, ...), custom_call_target="tpu_custom_call" | custom-call | flops 5000000000 | bytes 1000000 | tf_op jit(solution)/shard_map/pallas_call | solution.py:214
  84.3 1.4 %collective-permute-done.9 = bf16[96,2048]{1,0:T(8,128)(2,1)S(1)} collective-permute-done((bf16[96,2048]{1,0:T(8,128)(2,1)S(1)}, bf16[96,2048]{1,0:T(8,128)(2,1)S(1)}, u32[]{:S(2)}, u32[]{:S(2)}) %collective-permute-start.9) | collective-permute-done | bytes 393248 | tf_op jit(solution)/shard_map/ppermute | solution.py:228
  85.7 0.1 maximum_bitcast_fusion
  85.7 1.8 %pad_maximum_fusion.out_mine.mine = bf16[4,192,2048]{2,1,0:T(8,128)(2,1)S(1)} fusion(bf16[1,192,2048]{2,1,0:T(8,128)(2,1)} %bitcast.14, bf16[1,192,2048]{2,1,0:T(8,128)(2,1)S(1)} %maximum_bitcast_fusion, bf16[1,192,2048]{2,1,0:T(8,128)(2,1)} %bitcast.12, bf16[1,192,2048]{2,1,0:T(8,128)(2,1)} %bitcast.11), kind=kLoop, calls=%fused_computation | loop fusion | flops 4718592 | bytes 6291456 | tf_op jit(solution)/shard_map/stack | solution.py:299
  87.6 4.6 %collective-permute-start.12 = (bf16[4,192,2048]{2,1,0:T(8,128)(2,1)S(1)}, bf16[4,192,2048]{2,1,0:T(8,128)(2,1)S(1)}, u32[]{:S(2)}, u32[]{:S(2)}) collective-permute-start(bf16[4,192,2048]{2,1,0:T(8,128)(2,1)S(1)} %pad_maximum_fusion.out_mine.mine), channel_id=1, source_target_pairs={{1,0},{0,1},{3,2},{2,3},{5,4},{4,5},{7,6},{6,7},{9,8},{8,9},{11,10... | collective-permute-start | bytes 9437192 | tf_op jit(solution)/shard_map/ppermute | solution.py:228
  92.1 1.9 %collective-permute-start.13 = (bf16[64,2,32,256]{3,2,1,0:T(8,128)(2,1)}, bf16[64,2,32,256]{3,2,1,0:T(8,128)(2,1)}, u32[]{:S(2)}, u32[]{:S(2)}) collective-permute-start(bf16[64,2,32,256]{3,2,1,0:T(8,128)(2,1)} %all-to-all-done.refs_4_.refs_1_), channel_id=1, source_target_pairs={{1,0},{0,1},{3,2},{2,3},{5,4},{4,5},{7,6},{6,7},{9,8},{8,9},{11,10... | collective-permute-start | bytes 6291464 | tf_op jit(solution)/shard_map/ppermute | solution.py:228
  94.1 12.8 %all_to_all.20.arrived = bf16[8,32,640]{2,1,0:T(8,128)(2,1)} all-to-all(bf16[8,32,640]{2,1,0:T(8,128)(2,1)S(1)} %bitcast.21), channel_id=1, replica_groups=mesh['z'=8,'y'=8,'x'=4,'c'=2] {'x','c'}, dimensions={0} | all-to-all | bytes 655360 | tf_op jit(solution)/shard_map/all_to_all | solution.py:294
  106.9 1.7 %copy-done.2 = bf16[4,192,2048]{2,1,0:T(8,128)(2,1)} copy-done((bf16[4,192,2048]{2,1,0:T(8,128)(2,1)}, bf16[4,192,2048]{2,1,0:T(8,128)(2,1)S(1)}, u32[]{:S(2)}) %copy-start.2) | copy-done | bytes 3145752
  108.6 4.7 %shard_map.103 = (bf16[32,2048]{1,0:T(8,128)(2,1)}, bf16[4,32,512]{2,1,0:T(8,128)(2,1)}) custom-call(s32[2]{0:T(128)} %copy-done.7, bf16[8,32,640]{2,1,0:T(8,128)(2,1)} %all_to_all.20.arrived, bf16[32,2048]{1,0:T(8,128)(2,1)} %hidden.1, f32[2,2048]{1,0:T(2,128)} %gain.5, f32[2,64]{1,0:T(2,128)} %query_gain.3, bf16[4,192,2048]{2,1,0:T(8,128)(2,1)} %copy-done, ...), custom_call_target="tpu_custom_call" | custom-call | flops 400000000 | bytes 1000000 | tf_op jit(solution)/shard_map/pallas_call | solution.py:214
  113.3 3.5 %all-to-all-start.2 = ((bf16[4,32,512]{2,1,0:T(8,128)(2,1)}), bf16[4,32,512]{2,1,0:T(8,128)(2,1)S(1)}, u32[]{:S(2)}, u32[]{:S(2)}) async-start(bf16[4,32,512]{2,1,0:T(8,128)(2,1)} %get-tuple-element.18), calls=%async_computation.2 | async-start | bytes 262144 | tf_op jit(solution)/shard_map/all_to_all | solution.py:311
  116.8 0.0 copy-start.5
  116.8 0.0 collective-permute-done.13.refs_2_
  116.8 4.6 %all-to-all-done.2.refs_0_ = bf16[4,32,512]{2,1,0:T(8,128)(2,1)S(1)} async-done(((bf16[4,32,512]{2,1,0:T(8,128)(2,1)}), bf16[4,32,512]{2,1,0:T(8,128)(2,1)S(1)}, u32[]{:S(2)}, u32[]{:S(2)}) %all-to-all-start.2) | async-done | bytes 131104 | tf_op jit(solution)/shard_map/all_to_all | solution.py:311
  121.4 6.1 %shard_map.104 = bf16[128,640]{1,0:T(8,128)(2,1)S(1)} custom-call(s32[2]{0:T(128)S(1)} %copy-done.8, bf16[4,32,512]{2,1,0:T(8,128)(2,1)S(1)} %all-to-all-done.2.refs_0_, bf16[64,2,32,256]{3,2,1,0:T(8,128)(2,1)} %all-to-all-done.refs_4_.refs_1_, bf16[64,2,32,256]{3,2,1,0:T(8,128)(2,1)} %collective-permute-done.13.refs_2_), custom_call_target="tpu_custom_call" | custom-call | flops 5000000000 | bytes 1000000 | tf_op jit(solution)/shard_map/pallas_call | solution.py:214
  127.5 7.4 %all_to_all.21.arrived = bf16[4,32,640]{2,1,0:T(8,128)(2,1)S(1)} all-to-all(bf16[4,32,640]{2,1,0:T(8,128)(2,1)S(1)} %bitcast.22), channel_id=1, replica_groups=mesh['z'=8,'y'=8,'x'=4,'c'=2] {'x'}, dimensions={0} | all-to-all | bytes 327680 | tf_op jit(solution)/shard_map/all_to_all | solution.py:294
  134.9 1.9 %shard_map.105 = bf16[32,2048]{1,0:T(8,128)(2,1)} custom-call(s32[2]{0:T(128)S(1)} %copy-done.8, bf16[4,32,640]{2,1,0:T(8,128)(2,1)S(1)} %all_to_all.21.arrived, bf16[32,2048]{1,0:T(8,128)(2,1)S(1)} %copy-done.5, bf16[4,192,2048]{2,1,0:T(8,128)(2,1)S(1)} %copy-done.1, bf16[4,192,2048]{2,1,0:T(8,128)(2,1)S(1)} %copy-done.3), custom_call_target="tpu_custom_call" | custom-call | flops 200000000 | bytes 1000000 | tf_op jit(solution)/shard_map/pallas_call | solution.py:214
  (25 shorter events, 0.1 us)
Async XLA Ops:
  3.7 17.5 %copy-start.10 = (bf16[2,2048,64]{1,2,0:T(8,128)(2,1)S(1)}, bf16[2,2048,64]{1,2,0:T(8,128)(2,1)}, u32[]{:S(2)}) copy-start(bf16[2,2048,64]{1,2,0:T(8,128)(2,1)} %param.16) | copy-start | bytes 1572868
  3.7 75.4 %all-to-all-start = ((bf16[64,2,32,256]{3,2,1,0:T(8,128)(2,1)}), bf16[64,2,32,256]{3,2,1,0:T(8,128)(2,1)}, u32[]{:S(2)}, u32[]{:S(2)}) async-start(bf16[64,2,32,256]{3,2,1,0:T(8,128)(2,1)} %shard_map.101), calls=%async_computation | async-start | bytes 4194304 | tf_op jit(solution)/shard_map/all_to_all | solution.py:258
  21.2 24.4 %copy-start.11 = (bf16[2,64,2048]{2,1,0:T(8,128)(2,1)S(1)}, bf16[2,64,2048]{2,1,0:T(8,128)(2,1)}, u32[]{:S(2)}) copy-start(bf16[2,64,2048]{2,1,0:T(8,128)(2,1)} %param.19) | copy-start | bytes 1572868
  21.3 10.0 %collective-permute-start.1 = (bf16[64,2048]{1,0:T(8,128)(2,1)S(1)}, bf16[64,2048]{1,0:T(8,128)(2,1)S(1)}, u32[]{:S(2)}, u32[]{:S(2)}) collective-permute-start(bf16[64,2048]{1,0:T(8,128)(2,1)S(1)} %get-tuple-element.24), channel_id=1, source_target_pairs={{2,0},{4,2},{6,4},{0,6},{3,1},{5,3},{7,5},{1,7},{10,8},{12,10},{14... | collective-permute-start | bytes 786440 | tf_op jit(solution)/shard_map/ppermute | solution.py:228
  25.9 10.2 %collective-permute-start.2 = (bf16[64,2048]{1,0:T(8,128)(2,1)S(1)}, bf16[64,2048]{1,0:T(8,128)(2,1)S(1)}, u32[]{:S(2)}, u32[]{:S(2)}) collective-permute-start(bf16[64,2048]{1,0:T(8,128)(2,1)S(1)} %get-tuple-element.24), channel_id=1, source_target_pairs={{4,0},{6,2},{0,4},{2,6},{5,1},{7,3},{1,5},{3,7},{12,8},{14,10},{8,... | collective-permute-start | bytes 786440 | tf_op jit(solution)/shard_map/ppermute | solution.py:228
  28.3 14.9 %collective-permute-start.3 = (bf16[64,2048]{1,0:T(8,128)(2,1)S(1)}, bf16[64,2048]{1,0:T(8,128)(2,1)S(1)}, u32[]{:S(2)}, u32[]{:S(2)}) collective-permute-start(bf16[64,2048]{1,0:T(8,128)(2,1)S(1)} %get-tuple-element.24), channel_id=1, source_target_pairs={{6,0},{0,2},{2,4},{4,6},{7,1},{1,3},{3,5},{5,7},{14,8},{8,10},{10,... | collective-permute-start | bytes 786440 | tf_op jit(solution)/shard_map/ppermute | solution.py:228
  43.2 10.0 %copy-start.4 = (bf16[32,2048]{1,0:T(8,128)(2,1)S(1)}, bf16[32,2048]{1,0:T(8,128)(2,1)}, u32[]{:S(2)}) copy-start(bf16[32,2048]{1,0:T(8,128)(2,1)} %hidden.1) | copy-start | bytes 393220
  43.2 13.5 %copy-start.6 = (f32[2,2048]{1,0:T(2,128)S(1)}, f32[2,2048]{1,0:T(2,128)}, u32[]{:S(2)}) copy-start(f32[2,2048]{1,0:T(2,128)} %gain.5) | copy-start | bytes 49156
  43.2 13.5 %copy-start.9 = (f32[2,64]{1,0:T(2,128)S(1)}, f32[2,64]{1,0:T(2,128)}, u32[]{:S(2)}) copy-start(f32[2,64]{1,0:T(2,128)} %query_gain.3) | copy-start | bytes 1540
  43.3 13.4 %collective-permute-start.4 = (bf16[4,64,2048]{2,1,0:T(8,128)(2,1)S(1)}, bf16[4,64,2048]{2,1,0:T(8,128)(2,1)S(1)}, u32[]{:S(2)}, u32[]{:S(2)}) collective-permute-start(bf16[4,64,2048]{2,1,0:T(8,128)(2,1)S(1)} %pad_maximum_fusion.1.mine), channel_id=1, source_target_pairs={{1,0},{0,1},{3,2},{2,3},{5,4},{4,5},{7,6},{6,7},{9,8},{8,9},{11,10... | collective-permute-start | bytes 3145736 | tf_op jit(solution)/shard_map/ppermute | solution.py:228
  46.7 23.8 %collective-permute-start.10 = (bf16[192,2048]{1,0:T(8,128)(2,1)}, bf16[192,2048]{1,0:T(8,128)(2,1)}, u32[]{:S(2)}, u32[]{:S(2)}) collective-permute-start(bf16[192,2048]{1,0:T(8,128)(2,1)} %pad_maximum_fusion.2), channel_id=1, source_target_pairs={{6,0},{0,2},{2,4},{4,6},{7,1},{1,3},{3,5},{5,7},{14,8},{8,10},{10,... | collective-permute-start | bytes 2359304 | tf_op jit(solution)/shard_map/ppermute | solution.py:228
  48.6 24.8 %collective-permute-start.8 = (bf16[192,2048]{1,0:T(8,128)(2,1)}, bf16[192,2048]{1,0:T(8,128)(2,1)}, u32[]{:S(2)}, u32[]{:S(2)}) collective-permute-start(bf16[192,2048]{1,0:T(8,128)(2,1)} %pad_maximum_fusion.2), channel_id=1, source_target_pairs={{2,0},{4,2},{6,4},{0,6},{3,1},{5,3},{7,5},{1,7},{10,8},{12,10},{14... | collective-permute-start | bytes 2359304 | tf_op jit(solution)/shard_map/ppermute | solution.py:228
  53.2 3.5 %collective-permute-start = (bf16[32,2048]{1,0:T(8,128)(2,1)S(1)}, bf16[32,2048]{1,0:T(8,128)(2,1)S(1)}, u32[]{:S(2)}, u32[]{:S(2)}) collective-permute-start(bf16[32,2048]{1,0:T(8,128)(2,1)S(1)} %copy-done.4), channel_id=1, source_target_pairs={{1,0},{0,1},{3,2},{2,3},{5,4},{4,5},{7,6},{6,7},{9,8},{8,9},{11,10... | collective-permute-start | bytes 393224 | tf_op jit(solution)/shard_map/ppermute | solution.py:228
  55.8 28.4 %copy-start.7 = (s32[2]{0:T(128)}, s32[2]{0:T(128)S(1)}, u32[]{:S(2)}) copy-start(s32[2]{0:T(128)S(1)} %pad_add_fusion.place) | copy-start | bytes 28
  58.3 20.7 %collective-permute-start.5 = (bf16[64,512]{1,0:T(8,128)(2,1)S(1)}, bf16[64,512]{1,0:T(8,128)(2,1)S(1)}, u32[]{:S(2)}, u32[]{:S(2)}) collective-permute-start(bf16[64,512]{1,0:T(8,128)(2,1)S(1)} %shard_map.100.refs_0_), channel_id=1, source_target_pairs={{2,0},{4,2},{6,4},{0,6},{3,1},{5,3},{7,5},{1,7},{10,8},{12,10},{14... | collective-permute-start | bytes 196616 | tf_op jit(solution)/shard_map/ppermute | solution.py:228
  60.2 18.8 %collective-permute-start.6 = (bf16[64,512]{1,0:T(8,128)(2,1)S(1)}, bf16[64,512]{1,0:T(8,128)(2,1)S(1)}, u32[]{:S(2)}, u32[]{:S(2)}) collective-permute-start(bf16[64,512]{1,0:T(8,128)(2,1)S(1)} %shard_map.100.refs_0_), channel_id=1, source_target_pairs={{4,0},{6,2},{0,4},{2,6},{5,1},{7,3},{1,5},{3,7},{12,8},{14,10},{8,... | collective-permute-start | bytes 196616 | tf_op jit(solution)/shard_map/ppermute | solution.py:228
  62.4 16.6 %collective-permute-start.7 = (bf16[64,512]{1,0:T(8,128)(2,1)S(1)}, bf16[64,512]{1,0:T(8,128)(2,1)S(1)}, u32[]{:S(2)}, u32[]{:S(2)}) collective-permute-start(bf16[64,512]{1,0:T(8,128)(2,1)S(1)} %shard_map.100.refs_0_), channel_id=1, source_target_pairs={{6,0},{0,2},{2,4},{4,6},{7,1},{1,3},{3,5},{5,7},{14,8},{8,10},{10,... | collective-permute-start | bytes 196616 | tf_op jit(solution)/shard_map/ppermute | solution.py:228
  71.5 12.8 %collective-permute-start.11 = (bf16[96,2048]{1,0:T(8,128)(2,1)S(1)}, bf16[96,2048]{1,0:T(8,128)(2,1)S(1)}, u32[]{:S(2)}, u32[]{:S(2)}) collective-permute-start(bf16[96,2048]{1,0:T(8,128)(2,1)S(1)} %slice.30), channel_id=1, source_target_pairs={{6,0},{0,2},{2,4},{4,6},{7,1},{1,3},{3,5},{5,7},{14,8},{8,10},{10,... | collective-permute-start | bytes 1179656 | tf_op jit(solution)/shard_map/ppermute | solution.py:228
  74.5 11.2 %collective-permute-start.9 = (bf16[96,2048]{1,0:T(8,128)(2,1)S(1)}, bf16[96,2048]{1,0:T(8,128)(2,1)S(1)}, u32[]{:S(2)}, u32[]{:S(2)}) collective-permute-start(bf16[96,2048]{1,0:T(8,128)(2,1)S(1)} %slice.29), channel_id=1, source_target_pairs={{2,0},{4,2},{6,4},{0,6},{3,1},{5,3},{7,5},{1,7},{10,8},{12,10},{14... | collective-permute-start | bytes 1179656 | tf_op jit(solution)/shard_map/ppermute | solution.py:228
  87.6 19.4 %copy-start = (bf16[4,192,2048]{2,1,0:T(8,128)(2,1)}, bf16[4,192,2048]{2,1,0:T(8,128)(2,1)S(1)}, u32[]{:S(2)}) copy-start(bf16[4,192,2048]{2,1,0:T(8,128)(2,1)S(1)} %pad_maximum_fusion.out_mine.mine) | copy-start | bytes 9437188
  87.6 19.3 %collective-permute-start.12 = (bf16[4,192,2048]{2,1,0:T(8,128)(2,1)S(1)}, bf16[4,192,2048]{2,1,0:T(8,128)(2,1)S(1)}, u32[]{:S(2)}, u32[]{:S(2)}) collective-permute-start(bf16[4,192,2048]{2,1,0:T(8,128)(2,1)S(1)} %pad_maximum_fusion.out_mine.mine), channel_id=1, source_target_pairs={{1,0},{0,1},{3,2},{2,3},{5,4},{4,5},{7,6},{6,7},{9,8},{8,9},{11,10... | collective-permute-start | bytes 9437192 | tf_op jit(solution)/shard_map/ppermute | solution.py:228
  92.1 24.6 %collective-permute-start.13 = (bf16[64,2,32,256]{3,2,1,0:T(8,128)(2,1)}, bf16[64,2,32,256]{3,2,1,0:T(8,128)(2,1)}, u32[]{:S(2)}, u32[]{:S(2)}) collective-permute-start(bf16[64,2,32,256]{3,2,1,0:T(8,128)(2,1)} %all-to-all-done.refs_4_.refs_1_), channel_id=1, source_target_pairs={{1,0},{0,1},{3,2},{2,3},{5,4},{4,5},{7,6},{6,7},{9,8},{8,9},{11,10... | collective-permute-start | bytes 6291464 | tf_op jit(solution)/shard_map/ppermute | solution.py:228
  106.9 14.5 %copy-start.8 = (s32[2]{0:T(128)S(1)}, s32[2]{0:T(128)}, u32[]{:S(2)}) copy-start(s32[2]{0:T(128)} %copy-done.7) | copy-start | bytes 28
  106.9 1.7 %copy-start.2 = (bf16[4,192,2048]{2,1,0:T(8,128)(2,1)}, bf16[4,192,2048]{2,1,0:T(8,128)(2,1)S(1)}, u32[]{:S(2)}) copy-start(bf16[4,192,2048]{2,1,0:T(8,128)(2,1)S(1)} %collective-permute-done.12.out_other.other) | copy-start | bytes 9437188
  113.3 8.1 %all-to-all-start.2 = ((bf16[4,32,512]{2,1,0:T(8,128)(2,1)}), bf16[4,32,512]{2,1,0:T(8,128)(2,1)S(1)}, u32[]{:S(2)}, u32[]{:S(2)}) async-start(bf16[4,32,512]{2,1,0:T(8,128)(2,1)} %get-tuple-element.18), calls=%async_computation.2 | async-start | bytes 262144 | tf_op jit(solution)/shard_map/all_to_all | solution.py:311
  116.8 18.1 %copy-start.5 = (bf16[32,2048]{1,0:T(8,128)(2,1)S(1)}, bf16[32,2048]{1,0:T(8,128)(2,1)}, u32[]{:S(2)}) copy-start(bf16[32,2048]{1,0:T(8,128)(2,1)} %get-tuple-element.20.hidden) | copy-start | bytes 393220
  121.4 13.5 %copy-start.1 = (bf16[4,192,2048]{2,1,0:T(8,128)(2,1)S(1)}, bf16[4,192,2048]{2,1,0:T(8,128)(2,1)}, u32[]{:S(2)}) copy-start(bf16[4,192,2048]{2,1,0:T(8,128)(2,1)} %copy-done) | copy-start | bytes 9437188
  121.4 13.5 %copy-start.3 = (bf16[4,192,2048]{2,1,0:T(8,128)(2,1)S(1)}, bf16[4,192,2048]{2,1,0:T(8,128)(2,1)}, u32[]{:S(2)}) copy-start(bf16[4,192,2048]{2,1,0:T(8,128)(2,1)} %copy-done.2) | copy-start | bytes 9437188

commit v6 on v5

--- a/solution.py
+++ b/solution.py
@@ -296,8 +296,10 @@
     partial = attend(everyone, [(plane, 0, 1)], lax.axis_size(TP))
     pieces, second, _ = lax.optimization_barrier((pieces, plane, partial))
     far = jnp.concatenate(pieces[2:4], axis=0)
-    rest = both(jnp.stack([pieces[0], pieces[1], far, pieces[4]]))
-    rest = [[(part, k, head) for part in rest] for k in range(3)]
+    beside = [pieces[0], pieces[1], far, pieces[4]]
+    near = both(jnp.stack([part[: 2 * head] for part in beside]))
+    late = both(jnp.stack([part[2 * head :] for part in beside]))
+    rest = [[(part, k, head) for part in near] for k in range(2)] + [[(part, 0, head) for part in late]]
     shared = shifted(second, "c", 1)
     arrived = returned(partial, TP)
     hidden, queries = with_place(

time: 139 us -> 140 us (level)
  starting transfers between devices: 62 us -> 72.7 us
  blocking collectives: 20.2 us -> 12.1 us
  waiting for transfers between devices: 24.2 us -> 20.9 us
  local copies, waits for them, and re-layouts: 3.88 us -> 6.67 us
    ppermute x14 -> x15, waiting for transfers between devices: 19.6 us -> 11.3 us  [shifted(): lax.ppermute(value, axis, [((k + step) % size, k) for k in range(size)])]
    all_to_all x2 -> x1, blocking collectives: 20.2 us -> 12.1 us  [returned(): lax.all_to_all(partial.reshape(-1, rows, wide), axis, split_axis=0, conca...]
    ppermute x14 -> x15, starting transfers between devices: 41 us -> 48.3 us  [shifted(): lax.ppermute(value, axis, [((k + step) % size, k) for k in range(size)])]
    all_to_all x0 -> x1, waiting for transfers between devices: none -> 4.96 us  [returned(): lax.all_to_all(partial.reshape(-1, rows, wide), axis, split_axis=0, conca...]
    all_to_all x0 -> x1, starting transfers between devices: none -> 3.34 us  [returned(): lax.all_to_all(partial.reshape(-1, rows, wide), axis, split_axis=0, conca...]
    another operation x0 -> x3, local copies, waits for them, and re-layouts: none -> 3.08 us  [the longest x2 1.97 us: decoder(): late = both(jnp.stack([part[2 * head:] for part in beside]))]
  transfers between devices with their start and end apart: 16 -> 18, of which waited for: 7 -> 7; matrix products, arithmetic and copies ran while one was open for 2% -> 3% of each run, Pallas kernels for 8% -> 13%
where the time goes in v6:
time: 140 us; the launch traced here: 138 us
  starting transfers between devices  72.7 us (52%)
  Pallas kernels  23.6 us (17%)
  waiting for transfers between devices  20.9 us (15%)
  blocking collectives  12.1 us (9%)
  local copies, waits for them, and re-layouts  6.67 us (5%)
  other arithmetic  1.8 us (1%)
    ppermute x15, starting transfers between devices, shifted(): lax.ppermute(value, axis, [((k + step) % size, k) for k in range(size)])  48.3 us
    pallas_call x6, Pallas kernels, with_place(): pl.pallas_call(kernel, grid=(1,), out_shape=shapes, in_specs=specs, out_s...  23.6 us
    all_to_all x1, starting transfers between devices, decoder(): plane = lax.all_to_all(pairs, ROWS, split_axis=0, concat_axis=0, tiled=True)  17.5 us
    all_to_all x1, blocking collectives, returned(): lax.all_to_all(partial.reshape(-1, rows, wide), axis, split_axis=0, conca...  12.1 us
    ppermute x15, waiting for transfers between devices, shifted(): lax.ppermute(value, axis, [((k + step) % size, k) for k in range(size)])  11.3 us
    all_to_all x1, waiting for transfers between devices, returned(): lax.all_to_all(partial.reshape(-1, rows, wide), axis, split_axis=0, conca...  4.96 us
    all_to_all x1, waiting for transfers between devices, decoder(): lax.all_to_all(queries, 'x', split_axis=0, concat_axis=0, tiled=True)  4.59 us
    all_to_all x1, starting transfers between devices, decoder(): lax.all_to_all(queries, 'x', split_axis=0, concat_axis=0, tiled=True)  3.5 us
  transfers between devices with their start and end apart: 18, of which 7 were waited for; matrix products, arithmetic and copies ran while one was open for 3% of the time, Pallas kernels for 13%

profile of v6, /device:TPU:1, one launch (start us, length us, event | category | flops | bytes accessed | tf_op | source)
XLA Modules:
  0.0 138.1 jit_solution(14430162323330041488)
XLA Ops:
  0.0 3.7 %shard_map.101 = bf16[64,2,32,256]{3,2,1,0:T(8,128)(2,1)} custom-call(bf16[32,2048]{1,0:T(8,128)(2,1)} %source.1, f32[2,2048]{1,0:T(2,128)} %gain.4, f32[2,64]{1,0:T(2,128)} %key_gain.1, bf16[2,2048,128]{2,1,0:T(8,128)(2,1)} %key_weight.1, bf16[2,2048,128]{2,1,0:T(8,128)(2,1)} %value_weight.1), custom_call_target="tpu_custom_call" | custom-call | flops 200000000 | bytes 1000000 | tf_op jit(solution)/shard_map/pallas_call | solution.py:214
  3.7 17.5 %all-to-all-start = ((bf16[64,2,32,256]{3,2,1,0:T(8,128)(2,1)}), bf16[64,2,32,256]{3,2,1,0:T(8,128)(2,1)}, u32[]{:S(2)}, u32[]{:S(2)}) async-start(bf16[64,2,32,256]{3,2,1,0:T(8,128)(2,1)} %shard_map.101), calls=%async_computation | async-start | bytes 4194304 | tf_op jit(solution)/shard_map/all_to_all | solution.py:258
  21.2 0.0 copy-start.9
  21.2 0.1 slice_bitcast_fusion.3
  21.3 3.3 %collective-permute-start.3 = (bf16[64,2048]{1,0:T(8,128)(2,1)S(1)}, bf16[64,2048]{1,0:T(8,128)(2,1)S(1)}, u32[]{:S(2)}, u32[]{:S(2)}) collective-permute-start(bf16[64,2048]{1,0:T(8,128)(2,1)S(1)} %get-tuple-element.24), channel_id=1, source_target_pairs={{6,0},{0,2},{2,4},{4,6},{7,1},{1,3},{3,5},{5,7},{14,8},{8,10},{10,... | collective-permute-start | bytes 786440 | tf_op jit(solution)/shard_map/ppermute | solution.py:228
  24.6 4.4 %collective-permute-start.2 = (bf16[64,2048]{1,0:T(8,128)(2,1)S(1)}, bf16[64,2048]{1,0:T(8,128)(2,1)S(1)}, u32[]{:S(2)}, u32[]{:S(2)}) collective-permute-start(bf16[64,2048]{1,0:T(8,128)(2,1)S(1)} %get-tuple-element.24), channel_id=1, source_target_pairs={{4,0},{6,2},{0,4},{2,6},{5,1},{7,3},{1,5},{3,7},{12,8},{14,10},{8,... | collective-permute-start | bytes 786440 | tf_op jit(solution)/shard_map/ppermute | solution.py:228
  28.9 3.1 %collective-permute-start.1 = (bf16[64,2048]{1,0:T(8,128)(2,1)S(1)}, bf16[64,2048]{1,0:T(8,128)(2,1)S(1)}, u32[]{:S(2)}, u32[]{:S(2)}) collective-permute-start(bf16[64,2048]{1,0:T(8,128)(2,1)S(1)} %get-tuple-element.24), channel_id=1, source_target_pairs={{2,0},{4,2},{6,4},{0,6},{3,1},{5,3},{7,5},{1,7},{10,8},{12,10},{14... | collective-permute-start | bytes 786440 | tf_op jit(solution)/shard_map/ppermute | solution.py:228
  32.0 6.1 %collective-permute-done.2 = bf16[64,2048]{1,0:T(8,128)(2,1)S(1)} collective-permute-done((bf16[64,2048]{1,0:T(8,128)(2,1)S(1)}, bf16[64,2048]{1,0:T(8,128)(2,1)S(1)}, u32[]{:S(2)}, u32[]{:S(2)}) %collective-permute-start.2) | collective-permute-done | bytes 262176 | tf_op jit(solution)/shard_map/ppermute | solution.py:228
  38.2 1.2 collective-permute-done.1
  39.4 0.1 pad_maximum_fusion.1.mine
  39.5 3.9 %collective-permute-start.4 = (bf16[4,64,2048]{2,1,0:T(8,128)(2,1)S(1)}, bf16[4,64,2048]{2,1,0:T(8,128)(2,1)S(1)}, u32[]{:S(2)}, u32[]{:S(2)}) collective-permute-start(bf16[4,64,2048]{2,1,0:T(8,128)(2,1)S(1)} %pad_maximum_fusion.1.mine), channel_id=1, source_target_pairs={{1,0},{0,1},{3,2},{2,3},{5,4},{4,5},{7,6},{6,7},{9,8},{8,9},{11,10... | collective-permute-start | bytes 3145736 | tf_op jit(solution)/shard_map/ppermute | solution.py:228
  43.5 0.1 pad_maximum_fusion.3
  43.6 4.0 %collective-permute-start.10 = (bf16[192,2048]{1,0:T(8,128)(2,1)S(1)}, bf16[192,2048]{1,0:T(8,128)(2,1)}, u32[]{:S(2)}, u32[]{:S(2)}) collective-permute-start(bf16[192,2048]{1,0:T(8,128)(2,1)S(1)} %pad_maximum_fusion.3), channel_id=1, source_target_pairs={{6,0},{0,2},{2,4},{4,6},{7,1},{1,3},{3,5},{5,7},{14,8},{8,10},{10,... | collective-permute-start | bytes 2359304 | tf_op jit(solution)/shard_map/ppermute | solution.py:228
  47.6 2.4 %collective-permute-start.8 = (bf16[192,2048]{1,0:T(8,128)(2,1)S(1)}, bf16[192,2048]{1,0:T(8,128)(2,1)}, u32[]{:S(2)}, u32[]{:S(2)}) collective-permute-start(bf16[192,2048]{1,0:T(8,128)(2,1)S(1)} %pad_maximum_fusion.3), channel_id=1, source_target_pairs={{2,0},{4,2},{6,4},{0,6},{3,1},{5,3},{7,5},{1,7},{10,8},{12,10},{14... | collective-permute-start | bytes 2359304 | tf_op jit(solution)/shard_map/ppermute | solution.py:228
  50.1 2.5 %collective-permute-start = (bf16[32,2048]{1,0:T(8,128)(2,1)S(1)}, bf16[32,2048]{1,0:T(8,128)(2,1)S(1)}, u32[]{:S(2)}, u32[]{:S(2)}) collective-permute-start(bf16[32,2048]{1,0:T(8,128)(2,1)S(1)} %copy-done), channel_id=1, source_target_pairs={{1,0},{0,1},{3,2},{2,3},{5,4},{4,5},{7,6},{6,7},{9,8},{8,9},{11,10... | collective-permute-start | bytes 393224 | tf_op jit(solution)/shard_map/ppermute | solution.py:228
  52.6 0.1 pad_add_fusion.place
  52.7 0.9 collective-permute-done.beside
  53.6 1.6 %shard_map.100.refs_0_ = bf16[64,512]{1,0:T(8,128)(2,1)S(1)} custom-call(s32[2]{0:T(128)S(1)} %pad_add_fusion.place, bf16[32,2048]{1,0:T(8,128)(2,1)S(1)} %copy-done, bf16[32,2048]{1,0:T(8,128)(2,1)S(1)} %collective-permute-done.beside, f32[2,2048]{1,0:T(2,128)S(1)} %copy-done.2, f32[2,64]{1,0:T(2,128)S(1)} %copy-done.5, ...), custom_call_target="tpu_custom_call" | custom-call | flops 200000000 | bytes 1000000 | tf_op jit(solution)/shard_map/pallas_call | solution.py:214
  55.1 2.9 %collective-permute-start.7 = (bf16[64,512]{1,0:T(8,128)(2,1)S(1)}, bf16[64,512]{1,0:T(8,128)(2,1)S(1)}, u32[]{:S(2)}, u32[]{:S(2)}) collective-permute-start(bf16[64,512]{1,0:T(8,128)(2,1)S(1)} %shard_map.100.refs_0_), channel_id=1, source_target_pairs={{6,0},{0,2},{2,4},{4,6},{7,1},{1,3},{3,5},{5,7},{14,8},{8,10},{10,... | collective-permute-start | bytes 196616 | tf_op jit(solution)/shard_map/ppermute | solution.py:228
  58.1 3.2 %collective-permute-start.6 = (bf16[64,512]{1,0:T(8,128)(2,1)S(1)}, bf16[64,512]{1,0:T(8,128)(2,1)S(1)}, u32[]{:S(2)}, u32[]{:S(2)}) collective-permute-start(bf16[64,512]{1,0:T(8,128)(2,1)S(1)} %shard_map.100.refs_0_), channel_id=1, source_target_pairs={{4,0},{6,2},{0,4},{2,6},{5,1},{7,3},{1,5},{3,7},{12,8},{14,10},{8,... | collective-permute-start | bytes 196616 | tf_op jit(solution)/shard_map/ppermute | solution.py:228
  61.3 3.2 %collective-permute-start.5 = (bf16[64,512]{1,0:T(8,128)(2,1)S(1)}, bf16[64,512]{1,0:T(8,128)(2,1)S(1)}, u32[]{:S(2)}, u32[]{:S(2)}) collective-permute-start(bf16[64,512]{1,0:T(8,128)(2,1)S(1)} %shard_map.100.refs_0_), channel_id=1, source_target_pairs={{2,0},{4,2},{6,4},{0,6},{3,1},{5,3},{7,5},{1,7},{10,8},{12,10},{14... | collective-permute-start | bytes 196616 | tf_op jit(solution)/shard_map/ppermute | solution.py:228
  64.5 1.3 collective-permute-done.10
  65.9 1.0 slice.62
  66.9 2.7 %collective-permute-start.11 = (bf16[96,2048]{1,0:T(8,128)(2,1)S(1)}, bf16[96,2048]{1,0:T(8,128)(2,1)S(1)}, u32[]{:S(2)}, u32[]{:S(2)}) collective-permute-start(bf16[96,2048]{1,0:T(8,128)(2,1)S(1)} %slice.62), channel_id=1, source_target_pairs={{6,0},{0,2},{2,4},{4,6},{7,1},{1,3},{3,5},{5,7},{14,8},{8,10},{10,... | collective-permute-start | bytes 1179656 | tf_op jit(solution)/shard_map/ppermute | solution.py:228
  69.6 0.0 collective-permute-done.8
  69.6 1.0 slice.61
  70.7 3.8 %collective-permute-start.9 = (bf16[96,2048]{1,0:T(8,128)(2,1)S(1)}, bf16[96,2048]{1,0:T(8,128)(2,1)S(1)}, u32[]{:S(2)}, u32[]{:S(2)}) collective-permute-start(bf16[96,2048]{1,0:T(8,128)(2,1)S(1)} %slice.61), channel_id=1, source_target_pairs={{2,0},{4,2},{6,4},{0,6},{3,1},{5,3},{7,5},{1,7},{10,8},{12,10},{14... | collective-permute-start | bytes 1179656 | tf_op jit(solution)/shard_map/ppermute | solution.py:228
  74.5 5.2 %shard_map.102 = bf16[256,640]{1,0:T(8,128)(2,1)S(1)} custom-call(s32[2]{0:T(128)S(1)} %pad_add_fusion.place, bf16[64,512]{1,0:T(8,128)(2,1)S(1)} %shard_map.100.refs_0_, bf16[64,512]{1,0:T(8,128)(2,1)S(1)} %collective-permute-done.5.refs_1_, bf16[64,512]{1,0:T(8,128)(2,1)S(1)} %collective-permute-done.6.refs_2_, ...), custom_call_target="tpu_custom_call" | custom-call | flops 5000000000 | bytes 1000000 | tf_op jit(solution)/shard_map/pallas_call | solution.py:214
  79.7 1.7 %collective-permute-done.9 = bf16[96,2048]{1,0:T(8,128)(2,1)S(1)} collective-permute-done((bf16[96,2048]{1,0:T(8,128)(2,1)S(1)}, bf16[96,2048]{1,0:T(8,128)(2,1)S(1)}, u32[]{:S(2)}, u32[]{:S(2)}) %collective-permute-start.9) | collective-permute-done | bytes 393248 | tf_op jit(solution)/shard_map/ppermute | solution.py:228
  81.4 1.1 slice_bitcast_fusion.1
  82.5 1.1 fusion
  83.6 0.3 pad_maximum_fusion.out_mine.mine
  83.9 4.6 %collective-permute-start.12 = (bf16[4,128,2048]{2,1,0:T(8,128)(2,1)S(1)}, bf16[4,128,2048]{2,1,0:T(8,128)(2,1)S(1)}, u32[]{:S(2)}, u32[]{:S(2)}) collective-permute-start(bf16[4,128,2048]{2,1,0:T(8,128)(2,1)S(1)} %pad_maximum_fusion.out_mine.mine), channel_id=1, source_target_pairs={{1,0},{0,1},{3,2},{2,3},{5,4},{4,5},{7,6},{6,7},{9,8},{8,9},{11,10... | collective-permute-start | bytes 6291464 | tf_op jit(solution)/shard_map/ppermute | solution.py:228
  88.5 1.9 %collective-permute-start.13 = (bf16[64,2,32,256]{3,2,1,0:T(8,128)(2,1)}, bf16[64,2,32,256]{3,2,1,0:T(8,128)(2,1)}, u32[]{:S(2)}, u32[]{:S(2)}) collective-permute-start(bf16[64,2,32,256]{3,2,1,0:T(8,128)(2,1)} %all-to-all-done.refs_4_.refs_1_), channel_id=1, source_target_pairs={{1,0},{0,1},{3,2},{2,3},{5,4},{4,5},{7,6},{6,7},{9,8},{8,9},{11,10... | collective-permute-start | bytes 6291464 | tf_op jit(solution)/shard_map/ppermute | solution.py:228
  90.5 1.0 slice_bitcast_fusion.6
  91.4 1.0 slice_bitcast_fusion.4
  92.4 0.1 pad_maximum_fusion.2.out_mine
  92.6 2.4 %collective-permute-start.14 = (bf16[4,64,2048]{2,1,0:T(8,128)(2,1)S(1)}, bf16[4,64,2048]{2,1,0:T(8,128)(2,1)S(1)}, u32[]{:S(2)}, u32[]{:S(2)}) collective-permute-start(bf16[4,64,2048]{2,1,0:T(8,128)(2,1)S(1)} %pad_maximum_fusion.2.out_mine), channel_id=1, source_target_pairs={{1,0},{0,1},{3,2},{2,3},{5,4},{4,5},{7,6},{6,7},{9,8},{8,9},{11,10... | collective-permute-start | bytes 3145736 | tf_op jit(solution)/shard_map/ppermute | solution.py:228
  95.0 12.1 %all_to_all.20.arrived = bf16[8,32,640]{2,1,0:T(8,128)(2,1)} all-to-all(bf16[8,32,640]{2,1,0:T(8,128)(2,1)S(1)} %bitcast.32), channel_id=1, replica_groups=mesh['z'=8,'y'=8,'x'=4,'c'=2] {'x','c'}, dimensions={0} | all-to-all | bytes 655360 | tf_op jit(solution)/shard_map/all_to_all | solution.py:294
  107.1 1.4 %copy-done.7 = bf16[4,128,2048]{2,1,0:T(8,128)(2,1)} copy-done((bf16[4,128,2048]{2,1,0:T(8,128)(2,1)}, bf16[4,128,2048]{2,1,0:T(8,128)(2,1)S(1)}, u32[]{:S(2)}) %copy-start.7) | copy-done | bytes 2097176
  108.5 4.6 %shard_map.103 = (bf16[32,2048]{1,0:T(8,128)(2,1)}, bf16[4,32,512]{2,1,0:T(8,128)(2,1)}) custom-call(s32[2]{0:T(128)} %copy-done.3, bf16[8,32,640]{2,1,0:T(8,128)(2,1)} %all_to_all.20.arrived, bf16[32,2048]{1,0:T(8,128)(2,1)} %hidden.1, f32[2,2048]{1,0:T(2,128)} %gain.5, f32[2,64]{1,0:T(2,128)} %query_gain.3, bf16[4,128,2048]{2,1,0:T(8,128)(2,1)} %copy-done.6, ...), custom_call_target="tpu_custom_call" | custom-call | flops 400000000 | bytes 1000000 | tf_op jit(solution)/shard_map/pallas_call | solution.py:214
  113.2 3.5 %all-to-all-start.2 = ((bf16[4,32,512]{2,1,0:T(8,128)(2,1)}), bf16[4,32,512]{2,1,0:T(8,128)(2,1)S(1)}, u32[]{:S(2)}, u32[]{:S(2)}) async-start(bf16[4,32,512]{2,1,0:T(8,128)(2,1)} %get-tuple-element.18), calls=%async_computation.2 | async-start | bytes 262144 | tf_op jit(solution)/shard_map/all_to_all | solution.py:313
  116.7 0.0 copy-start.1
  116.7 4.6 %all-to-all-done.2.refs_0_ = bf16[4,32,512]{2,1,0:T(8,128)(2,1)S(1)} async-done(((bf16[4,32,512]{2,1,0:T(8,128)(2,1)}), bf16[4,32,512]{2,1,0:T(8,128)(2,1)S(1)}, u32[]{:S(2)}, u32[]{:S(2)}) %all-to-all-start.2) | async-done | bytes 131104 | tf_op jit(solution)/shard_map/all_to_all | solution.py:313
  121.3 6.6 %shard_map.104 = bf16[128,640]{1,0:T(8,128)(2,1)} custom-call(s32[2]{0:T(128)S(1)} %copy-done.4, bf16[4,32,512]{2,1,0:T(8,128)(2,1)S(1)} %all-to-all-done.2.refs_0_, bf16[64,2,32,256]{3,2,1,0:T(8,128)(2,1)} %all-to-all-done.refs_4_.refs_1_, bf16[64,2,32,256]{3,2,1,0:T(8,128)(2,1)} %collective-permute-done.13.refs_2_), custom_call_target="tpu_custom_call" | custom-call | flops 5000000000 | bytes 1000000 | tf_op jit(solution)/shard_map/pallas_call | solution.py:214
  127.9 3.3 %all-to-all-start.3 = ((bf16[4,32,640]{2,1,0:T(8,128)(2,1)}), bf16[4,32,640]{2,1,0:T(8,128)(2,1)S(1)}, u32[]{:S(2)}, u32[]{:S(2)}) async-start(bf16[4,32,640]{2,1,0:T(8,128)(2,1)} %bitcast.15), calls=%async_computation.3 | async-start | bytes 327680 | tf_op jit(solution)/shard_map/all_to_all | solution.py:294
  131.2 5.0 %all-to-all-done.3.arrived = bf16[4,32,640]{2,1,0:T(8,128)(2,1)S(1)} async-done(((bf16[4,32,640]{2,1,0:T(8,128)(2,1)}), bf16[4,32,640]{2,1,0:T(8,128)(2,1)S(1)}, u32[]{:S(2)}, u32[]{:S(2)}) %all-to-all-start.3) | async-done | bytes 163872 | tf_op jit(solution)/shard_map/all_to_all | solution.py:294
  136.2 1.9 %shard_map.105 = bf16[32,2048]{1,0:T(8,128)(2,1)} custom-call(s32[2]{0:T(128)S(1)} %copy-done.4, bf16[4,32,640]{2,1,0:T(8,128)(2,1)S(1)} %all-to-all-done.3.arrived, bf16[32,2048]{1,0:T(8,128)(2,1)S(1)} %copy-done.1, bf16[4,64,2048]{2,1,0:T(8,128)(2,1)S(1)} %pad_maximum_fusion.2.out_mine, bf16[4,64,2048]{2,1,0:T(8,128)(2,1)S(1)} %collective-permute-done.14.out_other), custom_call_target="tpu_custom_call" | custom-call | flops 200000000 | bytes 1000000 | tf_op jit(solution)/shard_map/pallas_call | solution.py:214
  (28 shorter events, 0.1 us)
Async XLA Ops:
  3.7 17.5 %copy-start.8 = (bf16[2,2048,64]{1,2,0:T(8,128)(2,1)S(1)}, bf16[2,2048,64]{1,2,0:T(8,128)(2,1)}, u32[]{:S(2)}) copy-start(bf16[2,2048,64]{1,2,0:T(8,128)(2,1)} %param.16) | copy-start | bytes 1572868
  3.7 70.8 %all-to-all-start = ((bf16[64,2,32,256]{3,2,1,0:T(8,128)(2,1)}), bf16[64,2,32,256]{3,2,1,0:T(8,128)(2,1)}, u32[]{:S(2)}, u32[]{:S(2)}) async-start(bf16[64,2,32,256]{3,2,1,0:T(8,128)(2,1)} %shard_map.101), calls=%async_computation | async-start | bytes 4194304 | tf_op jit(solution)/shard_map/all_to_all | solution.py:258
  21.2 22.2 %copy-start.9 = (bf16[2,64,2048]{2,1,0:T(8,128)(2,1)S(1)}, bf16[2,64,2048]{2,1,0:T(8,128)(2,1)}, u32[]{:S(2)}) copy-start(bf16[2,64,2048]{2,1,0:T(8,128)(2,1)} %param.19) | copy-start | bytes 1572868
  21.3 10.7 %collective-permute-start.3 = (bf16[64,2048]{1,0:T(8,128)(2,1)S(1)}, bf16[64,2048]{1,0:T(8,128)(2,1)S(1)}, u32[]{:S(2)}, u32[]{:S(2)}) collective-permute-start(bf16[64,2048]{1,0:T(8,128)(2,1)S(1)} %get-tuple-element.24), channel_id=1, source_target_pairs={{6,0},{0,2},{2,4},{4,6},{7,1},{1,3},{3,5},{5,7},{14,8},{8,10},{10,... | collective-permute-start | bytes 786440 | tf_op jit(solution)/shard_map/ppermute | solution.py:228
  24.6 13.6 %collective-permute-start.2 = (bf16[64,2048]{1,0:T(8,128)(2,1)S(1)}, bf16[64,2048]{1,0:T(8,128)(2,1)S(1)}, u32[]{:S(2)}, u32[]{:S(2)}) collective-permute-start(bf16[64,2048]{1,0:T(8,128)(2,1)S(1)} %get-tuple-element.24), channel_id=1, source_target_pairs={{4,0},{6,2},{0,4},{2,6},{5,1},{7,3},{1,5},{3,7},{12,8},{14,10},{8,... | collective-permute-start | bytes 786440 | tf_op jit(solution)/shard_map/ppermute | solution.py:228
  28.9 10.5 %collective-permute-start.1 = (bf16[64,2048]{1,0:T(8,128)(2,1)S(1)}, bf16[64,2048]{1,0:T(8,128)(2,1)S(1)}, u32[]{:S(2)}, u32[]{:S(2)}) collective-permute-start(bf16[64,2048]{1,0:T(8,128)(2,1)S(1)} %get-tuple-element.24), channel_id=1, source_target_pairs={{2,0},{4,2},{6,4},{0,6},{3,1},{5,3},{7,5},{1,7},{10,8},{12,10},{14... | collective-permute-start | bytes 786440 | tf_op jit(solution)/shard_map/ppermute | solution.py:228
  39.4 10.7 %copy-start = (bf16[32,2048]{1,0:T(8,128)(2,1)S(1)}, bf16[32,2048]{1,0:T(8,128)(2,1)}, u32[]{:S(2)}) copy-start(bf16[32,2048]{1,0:T(8,128)(2,1)} %hidden.1) | copy-start | bytes 393220
  39.4 14.2 %copy-start.2 = (f32[2,2048]{1,0:T(2,128)S(1)}, f32[2,2048]{1,0:T(2,128)}, u32[]{:S(2)}) copy-start(f32[2,2048]{1,0:T(2,128)} %gain.5) | copy-start | bytes 49156
  39.4 14.2 %copy-start.5 = (f32[2,64]{1,0:T(2,128)S(1)}, f32[2,64]{1,0:T(2,128)}, u32[]{:S(2)}) copy-start(f32[2,64]{1,0:T(2,128)} %query_gain.3) | copy-start | bytes 1540
  39.5 14.0 %collective-permute-start.4 = (bf16[4,64,2048]{2,1,0:T(8,128)(2,1)S(1)}, bf16[4,64,2048]{2,1,0:T(8,128)(2,1)S(1)}, u32[]{:S(2)}, u32[]{:S(2)}) collective-permute-start(bf16[4,64,2048]{2,1,0:T(8,128)(2,1)S(1)} %pad_maximum_fusion.1.mine), channel_id=1, source_target_pairs={{1,0},{0,1},{3,2},{2,3},{5,4},{4,5},{7,6},{6,7},{9,8},{8,9},{11,10... | collective-permute-start | bytes 3145736 | tf_op jit(solution)/shard_map/ppermute | solution.py:228
  43.6 22.3 %collective-permute-start.10 = (bf16[192,2048]{1,0:T(8,128)(2,1)S(1)}, bf16[192,2048]{1,0:T(8,128)(2,1)}, u32[]{:S(2)}, u32[]{:S(2)}) collective-permute-start(bf16[192,2048]{1,0:T(8,128)(2,1)S(1)} %pad_maximum_fusion.3), channel_id=1, source_target_pairs={{6,0},{0,2},{2,4},{4,6},{7,1},{1,3},{3,5},{5,7},{14,8},{8,10},{10,... | collective-permute-start | bytes 2359304 | tf_op jit(solution)/shard_map/ppermute | solution.py:228
  47.6 22.0 %collective-permute-start.8 = (bf16[192,2048]{1,0:T(8,128)(2,1)S(1)}, bf16[192,2048]{1,0:T(8,128)(2,1)}, u32[]{:S(2)}, u32[]{:S(2)}) collective-permute-start(bf16[192,2048]{1,0:T(8,128)(2,1)S(1)} %pad_maximum_fusion.3), channel_id=1, source_target_pairs={{2,0},{4,2},{6,4},{0,6},{3,1},{5,3},{7,5},{1,7},{10,8},{12,10},{14... | collective-permute-start | bytes 2359304 | tf_op jit(solution)/shard_map/ppermute | solution.py:228
  50.1 3.5 %collective-permute-start = (bf16[32,2048]{1,0:T(8,128)(2,1)S(1)}, bf16[32,2048]{1,0:T(8,128)(2,1)S(1)}, u32[]{:S(2)}, u32[]{:S(2)}) collective-permute-start(bf16[32,2048]{1,0:T(8,128)(2,1)S(1)} %copy-done), channel_id=1, source_target_pairs={{1,0},{0,1},{3,2},{2,3},{5,4},{4,5},{7,6},{6,7},{9,8},{8,9},{11,10... | collective-permute-start | bytes 393224 | tf_op jit(solution)/shard_map/ppermute | solution.py:228
  52.7 27.0 %copy-start.3 = (s32[2]{0:T(128)}, s32[2]{0:T(128)S(1)}, u32[]{:S(2)}) copy-start(s32[2]{0:T(128)S(1)} %pad_add_fusion.place) | copy-start | bytes 28
  55.1 19.3 %collective-permute-start.7 = (bf16[64,512]{1,0:T(8,128)(2,1)S(1)}, bf16[64,512]{1,0:T(8,128)(2,1)S(1)}, u32[]{:S(2)}, u32[]{:S(2)}) collective-permute-start(bf16[64,512]{1,0:T(8,128)(2,1)S(1)} %shard_map.100.refs_0_), channel_id=1, source_target_pairs={{6,0},{0,2},{2,4},{4,6},{7,1},{1,3},{3,5},{5,7},{14,8},{8,10},{10,... | collective-permute-start | bytes 196616 | tf_op jit(solution)/shard_map/ppermute | solution.py:228
  58.1 16.4 %collective-permute-start.6 = (bf16[64,512]{1,0:T(8,128)(2,1)S(1)}, bf16[64,512]{1,0:T(8,128)(2,1)S(1)}, u32[]{:S(2)}, u32[]{:S(2)}) collective-permute-start(bf16[64,512]{1,0:T(8,128)(2,1)S(1)} %shard_map.100.refs_0_), channel_id=1, source_target_pairs={{4,0},{6,2},{0,4},{2,6},{5,1},{7,3},{1,5},{3,7},{12,8},{14,10},{8,... | collective-permute-start | bytes 196616 | tf_op jit(solution)/shard_map/ppermute | solution.py:228
  61.3 13.1 %collective-permute-start.5 = (bf16[64,512]{1,0:T(8,128)(2,1)S(1)}, bf16[64,512]{1,0:T(8,128)(2,1)S(1)}, u32[]{:S(2)}, u32[]{:S(2)}) collective-permute-start(bf16[64,512]{1,0:T(8,128)(2,1)S(1)} %shard_map.100.refs_0_), channel_id=1, source_target_pairs={{2,0},{4,2},{6,4},{0,6},{3,1},{5,3},{7,5},{1,7},{10,8},{12,10},{14... | collective-permute-start | bytes 196616 | tf_op jit(solution)/shard_map/ppermute | solution.py:228
  66.9 12.8 %collective-permute-start.11 = (bf16[96,2048]{1,0:T(8,128)(2,1)S(1)}, bf16[96,2048]{1,0:T(8,128)(2,1)S(1)}, u32[]{:S(2)}, u32[]{:S(2)}) collective-permute-start(bf16[96,2048]{1,0:T(8,128)(2,1)S(1)} %slice.62), channel_id=1, source_target_pairs={{6,0},{0,2},{2,4},{4,6},{7,1},{1,3},{3,5},{5,7},{14,8},{8,10},{10,... | collective-permute-start | bytes 1179656 | tf_op jit(solution)/shard_map/ppermute | solution.py:228
  70.7 10.7 %collective-permute-start.9 = (bf16[96,2048]{1,0:T(8,128)(2,1)S(1)}, bf16[96,2048]{1,0:T(8,128)(2,1)S(1)}, u32[]{:S(2)}, u32[]{:S(2)}) collective-permute-start(bf16[96,2048]{1,0:T(8,128)(2,1)S(1)} %slice.61), channel_id=1, source_target_pairs={{2,0},{4,2},{6,4},{0,6},{3,1},{5,3},{7,5},{1,7},{10,8},{12,10},{14... | collective-permute-start | bytes 1179656 | tf_op jit(solution)/shard_map/ppermute | solution.py:228
  83.9 8.7 %copy-start.6 = (bf16[4,128,2048]{2,1,0:T(8,128)(2,1)}, bf16[4,128,2048]{2,1,0:T(8,128)(2,1)S(1)}, u32[]{:S(2)}) copy-start(bf16[4,128,2048]{2,1,0:T(8,128)(2,1)S(1)} %pad_maximum_fusion.out_mine.mine) | copy-start | bytes 6291460
  83.9 23.2 %collective-permute-start.12 = (bf16[4,128,2048]{2,1,0:T(8,128)(2,1)S(1)}, bf16[4,128,2048]{2,1,0:T(8,128)(2,1)S(1)}, u32[]{:S(2)}, u32[]{:S(2)}) collective-permute-start(bf16[4,128,2048]{2,1,0:T(8,128)(2,1)S(1)} %pad_maximum_fusion.out_mine.mine), channel_id=1, source_target_pairs={{1,0},{0,1},{3,2},{2,3},{5,4},{4,5},{7,6},{6,7},{9,8},{8,9},{11,10... | collective-permute-start | bytes 6291464 | tf_op jit(solution)/shard_map/ppermute | solution.py:228
  88.5 28.2 %collective-permute-start.13 = (bf16[64,2,32,256]{3,2,1,0:T(8,128)(2,1)}, bf16[64,2,32,256]{3,2,1,0:T(8,128)(2,1)}, u32[]{:S(2)}, u32[]{:S(2)}) collective-permute-start(bf16[64,2,32,256]{3,2,1,0:T(8,128)(2,1)} %all-to-all-done.refs_4_.refs_1_), channel_id=1, source_target_pairs={{1,0},{0,1},{3,2},{2,3},{5,4},{4,5},{7,6},{6,7},{9,8},{8,9},{11,10... | collective-permute-start | bytes 6291464 | tf_op jit(solution)/shard_map/ppermute | solution.py:228
  92.6 38.7 %collective-permute-start.14 = (bf16[4,64,2048]{2,1,0:T(8,128)(2,1)S(1)}, bf16[4,64,2048]{2,1,0:T(8,128)(2,1)S(1)}, u32[]{:S(2)}, u32[]{:S(2)}) collective-permute-start(bf16[4,64,2048]{2,1,0:T(8,128)(2,1)S(1)} %pad_maximum_fusion.2.out_mine), channel_id=1, source_target_pairs={{1,0},{0,1},{3,2},{2,3},{5,4},{4,5},{7,6},{6,7},{9,8},{8,9},{11,10... | collective-permute-start | bytes 3145736 | tf_op jit(solution)/shard_map/ppermute | solution.py:228
  107.1 14.2 %copy-start.4 = (s32[2]{0:T(128)S(1)}, s32[2]{0:T(128)}, u32[]{:S(2)}) copy-start(s32[2]{0:T(128)} %copy-done.3) | copy-start | bytes 28
  107.1 1.4 %copy-start.7 = (bf16[4,128,2048]{2,1,0:T(8,128)(2,1)}, bf16[4,128,2048]{2,1,0:T(8,128)(2,1)S(1)}, u32[]{:S(2)}) copy-start(bf16[4,128,2048]{2,1,0:T(8,128)(2,1)S(1)} %collective-permute-done.12.out_other.other) | copy-start | bytes 6291460
  113.2 8.1 %all-to-all-start.2 = ((bf16[4,32,512]{2,1,0:T(8,128)(2,1)}), bf16[4,32,512]{2,1,0:T(8,128)(2,1)S(1)}, u32[]{:S(2)}, u32[]{:S(2)}) async-start(bf16[4,32,512]{2,1,0:T(8,128)(2,1)} %get-tuple-element.18), calls=%async_computation.2 | async-start | bytes 262144 | tf_op jit(solution)/shard_map/all_to_all | solution.py:313
  116.7 19.5 %copy-start.1 = (bf16[32,2048]{1,0:T(8,128)(2,1)S(1)}, bf16[32,2048]{1,0:T(8,128)(2,1)}, u32[]{:S(2)}) copy-start(bf16[32,2048]{1,0:T(8,128)(2,1)} %get-tuple-element.20.hidden) | copy-start | bytes 393220
  127.9 8.3 %all-to-all-start.3 = ((bf16[4,32,640]{2,1,0:T(8,128)(2,1)}), bf16[4,32,640]{2,1,0:T(8,128)(2,1)S(1)}, u32[]{:S(2)}, u32[]{:S(2)}) async-start(bf16[4,32,640]{2,1,0:T(8,128)(2,1)} %bitcast.15), calls=%async_computation.3 | async-start | bytes 327680 | tf_op jit(solution)/shard_map/all_to_all | solution.py:294
